TPU v7x, 1024 devices: a whole 4x4x32 slice. The times are simulated.
1024 devices in a mesh: fs: 256 (over z, x, core), tp: 4 (over y).
Axes of the slice: x: 4, y: 4, z: 32, core: 2. Of those that a mesh axis runs over, the one named last changes fastest.
Arguments:
- normed_input: bfloat16 [131072, 2048], P('fs'), may hold values from -6 to 6
- value_cotangent: bfloat16 [131072, 2048], P('fs', 'tp'), may hold values from -6 to 6
- gated_output: bfloat16 [131072, 2048], P('fs', 'tp'), may hold values from -6 to 6
- layer_cotangent: bfloat16 [131072, 2048], P('fs'), may hold values from -6 to 6
- factor_value: bfloat16 [2048, 256], P('fs'), may hold values from -4 to 4, as said below
- factor_output: bfloat16 [2048, 256], P('fs'), may hold values from -4 to 4, as said below
- weight_value: float32 [2048, 2048], P('fs', 'tp'), may hold values from -0.125 to 0.125
- weight_output: float32 [2048, 2048], P('tp', 'fs'), may hold values from -0.125 to 0.125
- first_value: float32 [256, 2048], P('fs', 'tp'), may hold values from -8192 to 8192
- second_value: float32 [256, 2048], P('fs', 'tp'), may hold values from 524288 to 8388608
- first_output: float32 [256, 2048], P('fs', 'tp'), may hold values from -8192 to 8192
- second_output: float32 [256, 2048], P('fs', 'tp'), may hold values from 524288 to 8388608
Outputs:
- step_value: float32 [2048, 2048], P('fs', 'tp')
- step_output: float32 [2048, 2048], P('tp', 'fs')
- next_weight_value: float32 [2048, 2048], P('fs', 'tp')
- next_weight_output: float32 [2048, 2048], P('tp', 'fs')
- next_first_value: float32 [256, 2048], P('fs', 'tp')
- next_second_value: float32 [256, 2048], P('fs', 'tp')
- next_first_output: float32 [256, 2048], P('fs', 'tp')
- next_second_output: float32 [256, 2048], P('fs', 'tp')
- copy_value: bfloat16 [2048, 2048], P(None, 'tp')
- copy_output: bfloat16 [2048, 2048], P('tp')
Inputs may be any that keep to these rules, and one draw needn't show every extreme that they name: factor_value has full rank. factor_output has full rank.
All inputs are finite; a program needn't handle non-finite values.
Results may differ from a plain program's by a relative error of at most 0.0039.
Values may be sent and summed in bfloat16 or wider, within the bound.
No kernel may reach another device: no remote copies, remote signals or barrier semaphores. Data moves between devices by JAX's collectives and lax.ppermute only.
A program may use at most 64 MiB of HBM per device.

v0:
```python
import jax
import jax.numpy as jnp
from jax import lax
from jax.sharding import Mesh
from jax.sharding import PartitionSpec as P

D = 2048
WIDTH = 2048
FS = ("fs_0", "fs_1", "fs_2")


def joined_along(pieces, dim):
    dims = list(pieces.shape[1:])
    dims[dim] *= pieces.shape[0]
    return jnp.moveaxis(pieces, 0, dim).reshape(dims)


def stacked_from(shard, axes, turns):
    pieces = shard
    for k in turns:
        pieces = lax.all_gather(pieces, axes[k])
    done = turns[::-1]
    back = [done.index(k) for k in range(len(axes))]
    pieces = pieces.transpose(*back, *range(len(axes), pieces.ndim))
    return pieces.reshape(-1, *shard.shape)


def whole_of(shard, axes, turns, dim):
    return joined_along(stacked_from(shard, axes, turns), dim)


def sum_in_order(pieces, axes, turns):
    inside = pieces.shape[1:]
    pieces = pieces.reshape(*(lax.axis_size(a) for a in axes), *inside)
    pieces = jnp.moveaxis(pieces, turns, range(len(axes))).reshape(-1, *inside)
    for k in turns:
        pieces = lax.psum_scatter(pieces, axes[k], scatter_dimension=0, tiled=True)
    return pieces[0]


def cut_along(shard, dim, devices):
    dims = shard.shape
    pieces = shard.reshape(*dims[:dim], devices, dims[dim] // devices, *dims[dim + 1 :])
    return jnp.moveaxis(pieces, dim, 0)


def summed_rows(shard, axes, turns, dim):
    devices = lax.axis_size(axes)
    return sum_in_order(cut_along(shard, dim, devices), axes, turns)


def in_one_piece(arrays, axis, dim, along):
    ends, at = ([], 0)
    for a in arrays[:-1]:
        at += a.shape[along]
        ends.append(at)
    both = jnp.concatenate(arrays, axis=along)
    return tuple(jnp.split(lax.all_gather(both, axis, axis=dim, tiled=True), ends, axis=along))


def sent_to_all(shard, axis):
    copies = jnp.broadcast_to(shard, (lax.axis_size(axis), *shard.shape))
    return lax.all_to_all(copies, axis, split_axis=0, concat_axis=0, tiled=True)


def taken_together(shard, axis):
    return sent_to_all(shard, axis).sum(axis=0)


def packed_total(arrays, axis):
    ravelled, at, done = (jnp.concatenate([a.reshape(-1) for a in arrays]), 0, [])
    running = taken_together(ravelled, axis)
    for a in arrays:
        done.append(running[at : at + a.size].reshape(a.shape))
        at += a.size
    return tuple(done)


def rows_first(arrays, axis, dims):
    turned = [jnp.moveaxis(a, dim, 0) for a, dim in zip(arrays, dims)]
    widths = [t[0].size for t in turned]
    both = jnp.concatenate([t.reshape(-1, w) for t, w in zip(turned, widths)], axis=1)
    out = lax.all_gather(both, axis, axis=0, tiled=True)
    pieces = jnp.split(out, [sum(widths[:k]) for k in range(1, len(widths))], axis=1)
    return tuple(
        (
            jnp.moveaxis(b.reshape(-1, *t.shape[1:]), 0, dim)
            for b, t, dim in zip(pieces, turned, dims)
        )
    )


def gram_times(gram_matrix, directions):
    gram_high = gram_matrix.astype(jnp.bfloat16)
    gram_low = (gram_matrix - gram_high.astype(jnp.float32)).astype(jnp.bfloat16)
    return jnp.dot(gram_high, directions, preferred_element_type=jnp.float32) + jnp.dot(
        gram_low, directions, preferred_element_type=jnp.float32
    )


def body(
    normed_input,
    value_cotangent,
    gated_output,
    layer_cotangent,
    factor_value,
    factor_output,
    weight_value,
    weight_output,
    first_value,
    second_value,
    first_output,
    second_output,
):
    col_count = value_cotangent.shape[1]
    inner = (((0,), (0,)), ((), ()))
    pieces = (whole_of(factor_value, FS, (0, 1, 2), 0), whole_of(factor_output, FS, (0, 1, 2), 0))
    piece_value, piece_output = pieces
    span_input = normed_input
    span_cotan = layer_cotangent
    gram_value = lax.dot_general(pieces[0], pieces[0], inner, preferred_element_type=jnp.float32)
    gram_output = lax.dot_general(pieces[1], pieces[1], inner, preferred_element_type=jnp.float32)
    projected_input = jnp.dot(span_input, piece_value, preferred_element_type=jnp.float32).astype(
        jnp.bfloat16
    )
    projected_cotangent = jnp.dot(
        span_cotan, piece_output, preferred_element_type=jnp.float32
    ).astype(jnp.bfloat16)
    span_input = projected_input
    span_cotan = projected_cotangent
    term_value = lax.dot_general(
        span_input, value_cotangent, inner, preferred_element_type=jnp.float32
    )
    term_output = lax.dot_general(
        span_cotan, gated_output, inner, preferred_element_type=jnp.float32
    )
    low_rank = summed_rows(jnp.concatenate([term_value, term_output], axis=1), FS, (2, 0, 1), 0)
    low_value = low_rank[:, :col_count]
    low_output = low_rank[:, col_count:]
    next_first_value = 0.9 * first_value + 0.1 * low_value
    next_second_value = 0.95 * second_value + 0.05 * low_value * low_value
    next_first_output = 0.9 * first_output + 0.1 * low_output
    next_second_output = 0.95 * second_output + 0.05 * low_output * low_output
    direction_value = (next_first_value * lax.rsqrt(next_second_value)).astype(jnp.bfloat16)
    direction_output = (next_first_output * lax.rsqrt(next_second_output)).astype(jnp.bfloat16)
    gathered_value, gathered_output = in_one_piece((direction_value, direction_output), FS, 0, 1)
    update_value = jnp.dot(factor_value, gathered_value, preferred_element_type=jnp.float32)
    update_output = lax.dot_general(
        gathered_output, factor_output, (((0,), (1,)), ((), ())), preferred_element_type=jnp.float32
    )
    square_value = jnp.sum(
        gathered_value.astype(jnp.float32) * gram_times(gram_value, gathered_value)
    )
    square_output = jnp.sum(
        gathered_output.astype(jnp.float32) * gram_times(gram_output, gathered_output)
    )
    total_value, total_output = packed_total((square_value, square_output), "tp")
    entries = D * WIDTH
    step_value = update_value * lax.rsqrt(total_value / entries + 1e-06)
    step_output = update_output * lax.rsqrt(total_output / entries + 1e-06)
    next_weight_value = weight_value - 0.02 * step_value
    next_weight_output = weight_output - 0.02 * step_output
    half_value = next_weight_value.astype(jnp.bfloat16)
    half_output = next_weight_output.astype(jnp.bfloat16)
    copy_value, copy_output = rows_first((half_value, half_output), FS, (0, 1))
    return (
        step_value,
        step_output,
        next_weight_value,
        next_weight_output,
        next_first_value,
        next_second_value,
        next_first_output,
        next_second_output,
        copy_value,
        copy_output,
    )


def solution(mesh):
    torus = Mesh(mesh.devices.reshape(32, 4, 2, mesh.shape["tp"]), ("fs_0", "fs_1", "fs_2", "tp"))
    placed = (
        P(FS, None),
        P(FS, "tp"),
        P(FS, "tp"),
        P(FS, None),
        P(FS, None),
        P(FS, None),
        P(FS, "tp"),
        P("tp", FS),
        P(FS, "tp"),
        P(FS, "tp"),
        P(FS, "tp"),
        P(FS, "tp"),
    )
    return jax.shard_map(
        body,
        mesh=torus,
        in_specs=placed,
        out_specs=(
            P(FS, "tp"),
            P("tp", FS),
            P(FS, "tp"),
            P("tp", FS),
            P(FS, "tp"),
            P(FS, "tp"),
            P(FS, "tp"),
            P(FS, "tp"),
            P(None, "tp"),
            P("tp", None),
        ),
        check_vma=False,
    )
```

profile of v0, /device:TPU:1, one launch (start us, length us, event | category | flops | bytes accessed | tf_op | source)
XLA Modules:
  0.0 995.8 jit_solution(733296162595097203)
XLA Ops:
  7.2 55.9 %all-gather.3 = bf16[256,256]{1,0:T(8,128)(2,1)S(1)} all-gather(bf16[8,256]{1,0:T(8,128)(2,1)} %param.17), channel_id=5, replica_groups=mesh['fs_0'=32,'fs_1'=4,'fs_2'=2,'tp'=4] {'fs_0'}, dimensions={0}, use_global_device_ids=true | all-gather | bytes 135168 | tf_op jit(solution)/shard_map/all_gather | solution.py:21
  63.1 11.0 %all-gather.4 = bf16[128,8,256]{2,1,0:T(8,128)(2,1)} all-gather(bf16[32,8,256]{2,1,0:T(8,128)(2,1)S(1)} %bitcast.70), channel_id=6, replica_groups=mesh['fs_0'=32,'fs_1'=4,'fs_2'=2,'tp'=4] {'fs_1'}, dimensions={0}, use_global_device_ids=true | all-gather | bytes 655360 | tf_op jit(solution)/shard_map/all_gather | solution.py:21
  74.2 38.7 %all-gather = bf16[256,256]{1,0:T(8,128)(2,1)S(1)} all-gather(bf16[8,256]{1,0:T(8,128)(2,1)} %param.16), channel_id=2, replica_groups=mesh['fs_0'=32,'fs_1'=4,'fs_2'=2,'tp'=4] {'fs_0'}, dimensions={0}, use_global_device_ids=true | all-gather | bytes 135168 | tf_op jit(solution)/shard_map/all_gather | solution.py:21
  112.9 10.7 %all-gather.1 = bf16[128,8,256]{2,1,0:T(8,128)(2,1)} all-gather(bf16[32,8,256]{2,1,0:T(8,128)(2,1)S(1)} %bitcast.71), channel_id=3, replica_groups=mesh['fs_0'=32,'fs_1'=4,'fs_2'=2,'tp'=4] {'fs_1'}, dimensions={0}, use_global_device_ids=true | all-gather | bytes 655360 | tf_op jit(solution)/shard_map/all_gather | solution.py:21
  123.7 1.3 copy.42
  125.0 56.5 %all-gather.13.cloned.1.call-done = bf16[8,32,8,256]{3,2,1,0:T(8,128)(2,1)} async-done(((bf16[4,32,8,256]{3,2,1,0:T(8,128)(2,1)}), bf16[8,32,8,256]{3,2,1,0:T(8,128)(2,1)}) %all-gather.13.cloned.1.call-update) | async-done | bytes 1048592 | tf_op jit(solution)/shard_map/all_gather | solution.py:21
  181.5 2.3 copy.41
  183.8 3.0 fusion.3
  186.9 4.0 fusion.2
  190.9 1.3 pad_maximum_fusion
  192.2 1.6 reshape_reshape.11
  193.7 3.3 copy.43
  197.1 1.3 dynamic-slice.4
  198.4 1.3 dynamic-slice.2
  199.6 1.3 dynamic-slice
  202.2 2.1 convolution_bitcast_fusion
  204.4 55.3 %all-reduce.6.cloned.1.call-done = f32[256,1,1024]{2,1,0:T(1,128)} async-done(((f32[256,1,1024]{2,1,0:T(1,128)}), f32[256,1,1024]{2,1,0:T(1,128)}) %all-reduce.6.cloned.1.call-update) | async-done | bytes 1048592
  259.7 1.9 constant_dynamic-slice_fusion.1
  261.7 1.2 convolution_bitcast_fusion.1
  263.0 244.3 %all-reduce.8.cloned.1.call-done = f32[128,1,1024]{2,1,0:T(1,128)} async-done(((f32[128,1,1024]{2,1,0:T(1,128)}), f32[128,1,1024]{2,1,0:T(1,128)}) %all-reduce.8.cloned.1.call-update) | async-done | bytes 524304
  507.2 0.7 constant_dynamic-slice_fusion
  507.9 13.9 %all-reduce.2 = f32[4,1,1024]{2,1,0:T(1,128)S(1)} all-reduce(f32[4,1,1024]{2,1,0:T(1,128)S(1)} %constant_dynamic-slice_fusion), channel_id=10, replica_groups=mesh['fs_0'=32,'fs_1'=4,'fs_2'=2,'tp'=4] {'fs_1'}, use_global_device_ids=true, to_apply=%region_2.0.clone | all-reduce | flops 4096 | bytes 32768
  521.9 0.6 dynamic-slice_bitcast_fusion
  523.2 182.6 %all-gather.6 = bf16[256,1,1024]{2,1,0:T(2,128)(2,1)S(1)} all-gather(bf16[1,1,1024]{2,1,0:T(2,128)(2,1)S(1)} %maximum_bitcast_fusion), channel_id=1, replica_groups=mesh['fs_0'=32,'fs_1'=4,'fs_2'=2,'tp'=4] {'fs_0','fs_1','fs_2'}, dimensions={0}, use_global_device_ids=true | all-gather | bytes 526336 | tf_op jit(solution)/shard_map/all_gather | solution.py:58
  706.3 0.9 fusion.7
  707.4 0.9 fusion.8
  708.3 1.4 pad_maximum_fusion.2
  709.7 7.9 all_to_all.6
  719.8 0.8 fusion.25
  721.8 259.0 %all-gather.11.cloned.1.call-done = bf16[2048,1024]{1,0:T(8,128)(2,1)} async-done(((bf16[8,1024]{1,0:T(8,128)(2,1)}), bf16[2048,1024]{1,0:T(8,128)(2,1)}) %all-gather.11.cloned.1.call-update) | async-done | bytes 4194320 | tf_op jit(solution)/shard_map/all_gather | solution.py:83
  980.8 4.5 slice_bitcast_fusion
  985.3 3.9 copy.45
  (46 shorter events, 3.6 us)
Async XLA Ops:
  7.2 176.6 %copy-start = (bf16[512,2048]{1,0:T(8,128)(2,1)S(1)}, bf16[512,2048]{1,0:T(8,128)(2,1)}, u32[]{:S(2)}) copy-start(bf16[512,2048]{1,0:T(8,128)(2,1)} %param.15) | copy-start | bytes 6291460
  7.2 116.5 %all-gather.15.cloned.1.call-start = ((), (), s32[]{:S(2)}) async-start(), calls=%async_computation.3 | async-start | bytes 1572864 | tf_op jit(solution)/shard_map/all_gather | solution.py:21
  74.1 107.4 %all-gather.13.cloned.1.call-start = ((), (), s32[]{:S(2)}) async-start(), calls=%async_computation.2 | async-start | bytes 1572864 | tf_op jit(solution)/shard_map/all_gather | solution.py:21
  123.6 136.1 %all-reduce.6.cloned.1.call-start = ((), (), s32[]{:S(2)}) async-start(), calls=%async_computation.4 | async-start | bytes 2097152
  197.0 310.2 %all-reduce.8.cloned.1.call-start = ((), (), s32[]{:S(2)}) async-start(), calls=%async_computation.5 | async-start | bytes 1048576
  202.2 59.5 %copy-start.1 = (bf16[8,32,8,256]{3,2,1,0:T(8,128)(2,1)S(1)}, bf16[8,32,8,256]{3,2,1,0:T(8,128)(2,1)}, u32[]{:S(2)}) copy-start(bf16[8,32,8,256]{3,2,1,0:T(8,128)(2,1)} %all-gather.13.cloned.1.call-done) | copy-start | bytes 3145732
  261.6 260.9 %copy-start.7 = (f32[1,512]{1,0:T(1,128)S(1)}, f32[1,512]{1,0:T(1,128)}, u32[]{:S(2)}) copy-start(f32[1,512]{1,0:T(1,128)} %param.21) | copy-start | bytes 6148
  261.6 260.9 %copy-start.8 = (f32[1,512]{1,0:T(1,128)S(1)}, f32[1,512]{1,0:T(1,128)}, u32[]{:S(2)}) copy-start(f32[1,512]{1,0:T(1,128)} %param.20) | copy-start | bytes 6148
  261.6 260.9 %copy-start.9 = (f32[1,512]{1,0:T(1,128)S(1)}, f32[1,512]{1,0:T(1,128)}, u32[]{:S(2)}) copy-start(f32[1,512]{1,0:T(1,128)} %param.23) | copy-start | bytes 6148
  261.7 260.9 %copy-start.10 = (f32[1,512]{1,0:T(1,128)S(1)}, f32[1,512]{1,0:T(1,128)}, u32[]{:S(2)}) copy-start(f32[1,512]{1,0:T(1,128)} %param.22) | copy-start | bytes 6148
  261.7 719.1 %all-gather.11.cloned.1.call-start = ((), (), s32[]{:S(2)}) async-start(), calls=%async_computation.1 | async-start | bytes 4210688 | tf_op jit(solution)/shard_map/all_gather | solution.py:83
  263.0 443.0 %copy-start.2 = (f32[256,256]{1,0:T(8,128)S(1)}, f32[256,256]{1,0:T(8,128)}, u32[]{:S(2)}) copy-start(f32[256,256]{1,0:T(8,128)} %convolution_bitcast_fusion.1) | copy-start | bytes 786436
  706.0 13.6 %copy-start.5 = (bf16[8,256]{1,0:T(8,128)(2,1)S(1)}, bf16[8,256]{1,0:T(8,128)(2,1)}, u32[]{:S(2)}) copy-start(bf16[8,256]{1,0:T(8,128)(2,1)} %param.17) | copy-start | bytes 12292
  706.0 13.8 %copy-start.6 = (bf16[8,256]{1,0:T(8,128)(2,1)S(1)}, bf16[8,256]{1,0:T(8,128)(2,1)}, u32[]{:S(2)}) copy-start(bf16[8,256]{1,0:T(8,128)(2,1)} %param.16) | copy-start | bytes 12292
  706.0 13.8 %copy-start.11 = (f32[8,512]{1,0:T(8,128)S(1)}, f32[8,512]{1,0:T(8,128)}, u32[]{:S(2)}) copy-start(f32[8,512]{1,0:T(8,128)} %param.18) | copy-start | bytes 49156
  706.3 14.3 %copy-start.3 = (f32[512,8]{0,1:T(8,128)S(1)}, f32[512,8]{0,1:T(8,128)}, u32[]{:S(2)}) copy-start(f32[512,8]{0,1:T(8,128)} %param.19) | copy-start | bytes 49156
  719.8 265.5 %copy-start.4 = (f32[512,8]{0,1:T(8,128)}, f32[512,8]{0,1:T(8,128)S(1)}, u32[]{:S(2)}) copy-start(f32[512,8]{0,1:T(8,128)S(1)} %convolution_multiply_fusion) | copy-start | bytes 49156
Sparse Core Ops, SparseCore 0:
  74.2 40.6 all-gather.14
  123.7 57.7 all-gather.12
  197.2 62.5 all-reduce.5
  262.5 244.6 all-reduce.7
  721.9 258.8 all-gather.10
where the time goes:
time: 997 us; the launch traced here: 996 us
  waiting for transfers between devices  615 us (62%)
  blocking collectives  321 us (32%)
  local copies, waits for them, and re-layouts  24.8 us (2%)
  between operations  16.7 us (2%)
  matrix products  13.6 us (1%)
    unnamed x7, waiting for transfers between devices  300 us
    all_gather x1, waiting for transfers between devices, rows_first(): out = lax.all_gather(both, axis, axis=0, tiled=True)  259 us
    all_gather x1, blocking collectives, in_one_piece(): lax.all_gather(both, axis, axis=dim, tiled=True)  183 us
    all_gather x4, blocking collectives, stacked_from(): pieces = lax.all_gather(pieces, axes[k])  116 us
    all_gather x2, waiting for transfers between devices, stacked_from(): pieces = lax.all_gather(pieces, axes[k])  56.5 us
  transfers between devices with their start and end apart: 5, of which 4 were waited for; matrix products, arithmetic and copies ran while one was open for 1% of the time, Pallas kernels for 0%

commit v1 on v0

v1 whole, which is shorter than its diff:
```python
import jax
import jax.numpy as jnp
from jax import lax
from jax.sharding import Mesh
from jax.sharding import PartitionSpec as P

D = 2048
WIDTH = 2048
R = 256
FS = ("z", "x", "c")


def exchange(blocks, axes):
    return lax.all_to_all(blocks, axes, split_axis=0, concat_axis=0, tiled=True)


def to_all(block, axes):
    copies = jnp.broadcast_to(block[None], (lax.axis_size(axes), *block.shape))
    return exchange(copies, axes)


def body(
    normed_input,
    value_cotangent,
    gated_output,
    layer_cotangent,
    factor_value,
    factor_output,
    weight_value,
    weight_output,
    first_value,
    second_value,
    first_output,
    second_output,
):
    nz, nx, nc, ny = (lax.axis_size(a) for a in ("z", "x", "c", "tp"))
    rows = factor_value.shape[0]
    cols = value_cotangent.shape[1]
    quarter = lax.axis_index("tp")
    inner = (((0,), (0,)), ((), ()))

    half_value = weight_value.astype(jnp.bfloat16)
    half_output = weight_output.astype(jnp.bfloat16).T
    halves = jnp.concatenate([half_value, half_output], axis=1)
    with jax.named_scope("wz"):
        w = to_all(halves, "z")
    with jax.named_scope("wx"):
        w = to_all(w, "x")
    with jax.named_scope("wc"):
        w = to_all(w, "c")
    w = w.transpose(2, 1, 0, 3, 4).reshape(D, 2 * cols)

    place = jnp.arange(R).reshape(nz, nx * nc).T.reshape(R)
    turn = (jnp.arange(R)[:, None] == place[None, :]).astype(jnp.bfloat16)
    both = jnp.concatenate([factor_value, factor_output], axis=0)
    both = jnp.dot(both, turn, preferred_element_type=jnp.float32).astype(jnp.bfloat16)
    both = both.reshape(2, rows, 2, R // 2).transpose(0, 2, 1, 3).reshape(ny, rows, R // 2)
    mine = lax.dynamic_index_in_dim(both, quarter, 0, keepdims=False)
    with jax.named_scope("fz"):
        f = to_all(mine, "z")
    with jax.named_scope("fxy"):
        f = to_all(f, ("x", "tp"))
    with jax.named_scope("fc"):
        f = to_all(f, "c")
    f = f.reshape(nc, nx, 2, 2, nz, rows, R // 2).transpose(2, 4, 1, 0, 5, 3, 6).reshape(2, D, R)
    whole_value, whole_output = f[0], f[1]

    projected_input = jnp.dot(
        normed_input, whole_value, preferred_element_type=jnp.float32
    ).astype(jnp.bfloat16)
    projected_cotangent = jnp.dot(
        layer_cotangent, whole_output, preferred_element_type=jnp.float32
    ).astype(jnp.bfloat16)
    term_value = lax.dot_general(
        projected_input, value_cotangent, inner, preferred_element_type=jnp.float32
    )
    term_output = lax.dot_general(
        projected_cotangent, gated_output, inner, preferred_element_type=jnp.float32
    )
    terms = jnp.concatenate([term_value, term_output], axis=1).astype(jnp.bfloat16)
    with jax.named_scope("sxc"):
        t = exchange(terms.reshape(nx * nc, nz, 2 * cols), ("x", "c"))
    t = t.astype(jnp.float32).sum(axis=0).astype(jnp.bfloat16)
    with jax.named_scope("sz"):
        t = exchange(t.reshape(nz, 8, 2 * cols // 8), "z")
    low = t.astype(jnp.float32).sum(axis=0)
    low_value = low[:4].reshape(1, cols)
    low_output = low[4:].reshape(1, cols)

    next_first_value = 0.9 * first_value + 0.1 * low_value
    next_second_value = 0.95 * second_value + 0.05 * low_value * low_value
    next_first_output = 0.9 * first_output + 0.1 * low_output
    next_second_output = 0.95 * second_output + 0.05 * low_output * low_output
    direction_value = (next_first_value * lax.rsqrt(next_second_value)).astype(jnp.bfloat16)
    direction_output = (next_first_output * lax.rsqrt(next_second_output)).astype(jnp.bfloat16)
    d = jnp.concatenate([direction_value.reshape(4, -1), direction_output.reshape(4, -1)], axis=0)
    with jax.named_scope("dz"):
        d = to_all(d, "z")
    with jax.named_scope("dxc"):
        d = to_all(d, ("x", "c"))
    d = d.reshape(R, 2 * cols)
    d_value, d_output = d[:, :cols], d[:, cols:]

    update_value = jnp.dot(whole_value, d_value, preferred_element_type=jnp.float32)
    update_output = lax.dot_general(
        d_output, whole_output, (((0,), (1,)), ((), ())), preferred_element_type=jnp.float32
    )
    squares = jnp.stack([jnp.sum(update_value * update_value), jnp.sum(update_output * update_output)])
    with jax.named_scope("tot"):
        totals = to_all(jnp.broadcast_to(squares[:, None, None], (2, 8, 128)), "tp").sum(axis=0)
    entries = D * WIDTH
    scale_value = lax.rsqrt(totals[0, 0, 0] / entries + 1e-06)
    scale_output = lax.rsqrt(totals[1, 0, 0] / entries + 1e-06)

    at = lax.axis_index(FS) * rows
    own_value = jnp.dot(factor_value, jnp.dot(turn, d_value, preferred_element_type=jnp.float32).astype(jnp.bfloat16), preferred_element_type=jnp.float32)
    own_output = lax.dot_general(
        jnp.dot(turn, d_output, preferred_element_type=jnp.float32).astype(jnp.bfloat16), factor_output, (((0,), (1,)), ((), ())), preferred_element_type=jnp.float32
    )
    step_value = own_value * scale_value
    step_output = own_output * scale_output
    next_weight_value = weight_value - 0.02 * step_value
    next_weight_output = weight_output - 0.02 * step_output
    copy_value = (w[:, :cols] - (0.02 * scale_value) * update_value).astype(jnp.bfloat16)
    copy_output = (w[:, cols:].T - (0.02 * scale_output) * update_output).astype(jnp.bfloat16)
    return (
        step_value,
        step_output,
        next_weight_value,
        next_weight_output,
        next_first_value,
        next_second_value,
        next_first_output,
        next_second_output,
        copy_value,
        copy_output,
    )


def solution(mesh):
    torus = Mesh(mesh.devices.reshape(32, 4, 2, mesh.shape["tp"]), ("z", "x", "c", "tp"))
    placed = (
        P(FS, None),
        P(FS, "tp"),
        P(FS, "tp"),
        P(FS, None),
        P(FS, None),
        P(FS, None),
        P(FS, "tp"),
        P("tp", FS),
        P(FS, "tp"),
        P(FS, "tp"),
        P(FS, "tp"),
        P(FS, "tp"),
    )
    return jax.shard_map(
        body,
        mesh=torus,
        in_specs=placed,
        out_specs=(
            P(FS, "tp"),
            P("tp", FS),
            P(FS, "tp"),
            P("tp", FS),
            P(FS, "tp"),
            P(FS, "tp"),
            P(FS, "tp"),
            P(FS, "tp"),
            P(None, "tp"),
            P("tp", None),
        ),
        check_vma=False,
    )
```

time: 997 us -> 322 us (0.32)
  waiting for transfers between devices: 615 us -> 15.5 us
  blocking collectives: 321 us -> 249 us
  between operations: 16.7 us -> 2.27 us
    all_gather x3 -> x0, waiting for transfers between devices: 315 us -> none  [the longest x1 259 us: rows_first(): out = lax.all_gather(both, axis, axis=0, tiled=True)]
    unnamed x7 -> x0, waiting for transfers between devices: 300 us -> none
    all_gather x5 -> x0, blocking collectives: 299 us -> none  [the longest x1 183 us: in_one_piece(): lax.all_gather(both, axis, axis=dim, tiled=True)]
    all_to_all x1 -> x10, blocking collectives: 7.92 us -> 249 us  [exchange(): return lax.all_to_all(blocks, axes, split_axis=0, concat_axis=0, tiled=True)]
    all_to_all x0 -> x1, waiting for transfers between devices: none -> 15.5 us  [exchange(): return lax.all_to_all(blocks, axes, split_axis=0, concat_axis=0, tiled=True)]
    unnamed x1 -> x0, blocking collectives: 13.9 us -> none
  transfers between devices with their start and end apart: 5 -> 1, of which waited for: 4 -> 1; matrix products, arithmetic and copies ran while one was open for 1% -> 2% of each run, Pallas kernels for 0% -> 0%
where the time goes in v1:
time: 322 us; the launch traced here: 321 us
  blocking collectives  249 us (77%)
  local copies, waits for them, and re-layouts  20.4 us (6%)
  matrix products  17.3 us (5%)
  waiting for transfers between devices  15.5 us (5%)
  other arithmetic  11.8 us (4%)
  starting transfers between devices  4.47 us (1%)
    all_to_all x10, blocking collectives, exchange(): return lax.all_to_all(blocks, axes, split_axis=0, concat_axis=0, tiled=True)  249 us
    all_to_all x1, waiting for transfers between devices, exchange(): return lax.all_to_all(blocks, axes, split_axis=0, concat_axis=0, tiled=True)  15.5 us
    unnamed x31, local copies, waits for them, and re-layouts  6.94 us
  transfers between devices with their start and end apart: 1, of which 1 were waited for; matrix products, arithmetic and copies ran while one was open for 2% of the time, Pallas kernels for 0%

profile of v1, /device:TPU:1, one launch (start us, length us, event | category | flops | bytes accessed | tf_op | source)
XLA Modules:
  0.0 320.7 jit_solution(4238916515911516527)
XLA Ops:
  0.8 1.0 convolution_convert_fusion.6
  1.8 53.2 %all_to_all.55 = bf16[32,8,128]{2,1,0:T(8,128)(2,1)S(1)} all-to-all(bf16[32,8,128]{2,1,0:T(8,128)(2,1)S(1)} %broadcast_in_dim.21), channel_id=1, replica_groups=mesh['z'=32,'x'=4,'c'=2,'tp'=4] {'z'}, dimensions={0} | all-to-all | bytes 131072 | tf_op jit(solution)/shard_map/fz/all_to_all | solution.py:14
  55.1 19.7 %all_to_all.56 = bf16[16,32,8,128]{3,2,1,0:T(8,128)(2,1)S(1)} all-to-all(bf16[16,32,8,128]{3,2,1,0:T(8,128)(2,1)S(1)} %broadcast_in_dim.22), channel_id=1, replica_groups=mesh['z'=32,'x'=4,'c'=2,'tp'=4] {'x','tp'}, dimensions={0} | all-to-all | bytes 2097152 | tf_op jit(solution)/shard_map/fxy/all_to_all | solution.py:14
  75.4 10.0 %all_to_all.57 = bf16[2,16,32,8,128]{4,3,2,1,0:T(8,128)(2,1)S(1)} all-to-all(bf16[2,16,32,8,128]{4,3,2,1,0:T(8,128)(2,1)S(1)} %broadcast_in_dim.23), channel_id=1, replica_groups=mesh['z'=32,'x'=4,'c'=2,'tp'=4] {'c'}, dimensions={0} | all-to-all | bytes 4194304 | tf_op jit(solution)/shard_map/fc/all_to_all | solution.py:14
  85.9 1.3 copy.37
  87.2 2.0 convolution_convert_fusion.4
  89.2 3.6 %convolution_convert_fusion.2 = bf16[256,512]{1,0:T(8,128)(2,1)} fusion(bf16[512,512]{1,0:T(8,128)(2,1)} %param.14, bf16[2048,256]{1,0:T(8,128)(2,1)} %bitcast.55, bf16[512,2048]{1,0:T(8,128)(2,1)} %param.15), kind=kOutput, calls=%fused_computation.7 | convolution fusion | flops 671350784 | bytes 3932160 | tf_op jit(solution)/shard_map/dot_general | solution.py:77
  92.8 1.0 pad_maximum_fusion
  93.9 12.8 %all_to_all.58 = bf16[8,32,1024]{2,1,0:T(8,128)(2,1)} all-to-all(bf16[8,32,1024]{2,1,0:T(8,128)(2,1)S(1)} %pad_maximum_fusion), channel_id=1, replica_groups=mesh['z'=32,'x'=4,'c'=2,'tp'=4] {'x','c'}, dimensions={0} | all-to-all | bytes 1048576 | tf_op jit(solution)/shard_map/sxc/all_to_all | solution.py:14
  106.7 1.1 reduce_sum.48
  107.8 27.1 %all_to_all.59 = bf16[32,8,128]{2,1,0:T(8,128)(2,1)S(1)} all-to-all(bf16[32,8,128]{2,1,0:T(8,128)(2,1)S(1)} %bitcast.62), channel_id=1, replica_groups=mesh['z'=32,'x'=4,'c'=2,'tp'=4] {'z'}, dimensions={0} | all-to-all | bytes 131072 | tf_op jit(solution)/shard_map/sz/all_to_all | solution.py:14
  135.7 27.1 %all_to_all.60 = bf16[32,8,128]{2,1,0:T(8,128)(2,1)S(1)} all-to-all(bf16[32,8,128]{2,1,0:T(8,128)(2,1)S(1)} %broadcast_in_dim.24), channel_id=1, replica_groups=mesh['z'=32,'x'=4,'c'=2,'tp'=4] {'z'}, dimensions={0} | all-to-all | bytes 131072 | tf_op jit(solution)/shard_map/dz/all_to_all | solution.py:14
  162.9 15.3 %all_to_all.61 = bf16[8,32,8,128]{3,2,1,0:T(8,128)(2,1)S(1)} all-to-all(bf16[8,32,8,128]{3,2,1,0:T(8,128)(2,1)S(1)} %broadcast_in_dim.25), channel_id=1, replica_groups=mesh['z'=32,'x'=4,'c'=2,'tp'=4] {'x','c'}, dimensions={0} | all-to-all | bytes 1048576 | tf_op jit(solution)/shard_map/dxc/all_to_all | solution.py:14
  178.3 3.7 %multiply_reduce_fusion.1 = (f32[]{:T(128)}, f32[2048,512]{1,0:T(8,128)}) fusion(bf16[2048,256]{1,0:T(8,128)(2,1)S(1)} %bitcast.54, bf16[256,1024]{1,0:T(8,128)(2,1)S(1)} %bitcast.57), kind=kOutput, calls=%fused_computation.4 | convolution fusion | flops 538968064 | bytes 5505028 | tf_op jit(solution)/shard_map/dot_general | solution.py:104
  182.1 3.8 %multiply_reduce_fusion = (f32[]{:T(128)}, f32[512,2048]{1,0:T(8,128)}) fusion(bf16[2048,256]{1,0:T(8,128)(2,1)S(1)} %bitcast.56, bf16[256,1024]{1,0:T(8,128)(2,1)S(1)} %bitcast.58), kind=kOutput, calls=%fused_computation.3 | convolution fusion | flops 538968064 | bytes 5505028 | tf_op jit(solution)/shard_map/dot_general | solution.py:105
  185.8 1.4 pad_maximum_fusion.3
  187.3 6.6 %all_to_all.62 = f32[4,2,8,128]{3,2,1,0:T(8,128)S(1)} all-to-all(f32[4,2,8,128]{3,2,1,0:T(8,128)S(1)} %broadcast_in_dim.26), channel_id=1, replica_groups=mesh['z'=32,'x'=4,'c'=2,'tp'=4] {'tp'}, dimensions={0} | all-to-all | bytes 65536 | tf_op jit(solution)/shard_map/tot/all_to_all | solution.py:14
  195.8 1.3 fusion.3
  197.1 1.9 fusion.28
  199.7 63.9 %all_to_all.63 = bf16[32,8,1024]{2,1,0:T(8,128)(2,1)S(1)} all-to-all(bf16[32,8,1024]{2,1,0:T(8,128)(2,1)S(1)} %broadcast_in_dim.27), channel_id=1, replica_groups=mesh['z'=32,'x'=4,'c'=2,'tp'=4] {'z'}, dimensions={0} | all-to-all | bytes 1048576 | tf_op jit(solution)/shard_map/wz/all_to_all | solution.py:14
  263.6 1.6 broadcast_in_dim.28
  265.2 4.5 %all-to-all-start.9 = ((bf16[4,32,8,1024]{3,2,1,0:T(8,128)(2,1)}), bf16[4,32,8,1024]{3,2,1,0:T(8,128)(2,1)}, u32[]{:S(2)}, u32[]{:S(2)}) async-start(bf16[4,32,8,1024]{3,2,1,0:T(8,128)(2,1)} %broadcast_in_dim.28), calls=%async_computation.9 | async-start | bytes 4194304 | tf_op jit(solution)/shard_map/wx/all_to_all | solution.py:14
  269.7 5.4 %copy.40 = f32[512,2048]{0,1:T(8,128)} copy(f32[512,2048]{1,0:T(8,128)} %get-tuple-element.77) | data formatting | bytes 8388608 | tf_op jit(solution)/shard_map/dot_general | solution.py:105
  275.1 15.5 %all-to-all-done.9 = bf16[4,32,8,1024]{3,2,1,0:T(8,128)(2,1)} async-done(((bf16[4,32,8,1024]{3,2,1,0:T(8,128)(2,1)}), bf16[4,32,8,1024]{3,2,1,0:T(8,128)(2,1)}, u32[]{:S(2)}, u32[]{:S(2)}) %all-to-all-start.9) | async-done | bytes 2097184 | tf_op jit(solution)/shard_map/wx/all_to_all | solution.py:14
  290.5 1.8 copy.38
  293.0 13.2 %all_to_all.64 = bf16[2,4,32,8,1024]{4,3,1,2,0:T(8,128)(2,1)S(1)} all-to-all(bf16[2,4,32,8,1024]{4,3,1,2,0:T(8,128)(2,1)S(1)} %broadcast_in_dim.29), channel_id=1, replica_groups=mesh['z'=32,'x'=4,'c'=2,'tp'=4] {'c'}, dimensions={0} | all-to-all | bytes 8388608 | tf_op jit(solution)/shard_map/wc/all_to_all | solution.py:14
  306.2 0.7 copy.39
  306.9 2.1 copy-done.2
  309.0 0.8 copy-done.1
  309.8 2.1 fusion
  311.9 3.9 %copy.41 = bf16[512,2048]{1,0:T(8,128)(2,1)} copy(bf16[512,2048]{0,1:T(8,128)(2,1)} %fusion) | data formatting | bytes 4194304
  315.8 4.9 %subtract_convert_fusion = bf16[2048,512]{1,0:T(8,128)(2,1)} fusion(f32[2048,512]{1,0:T(8,128)} %get-tuple-element.79, bf16[2048,1024]{1,0:T(8,128)(2,1)} %bitcast.51, f32[]{:T(128)S(6)} %mul.158), kind=kLoop, calls=%fused_computation.2 | loop fusion | flops 4194304 | bytes 8388612 | tf_op jit(solution)/shard_map/convert_element_type | solution.py:124
  (49 shorter events, 4.2 us)
Async XLA Ops:
  0.6 86.5 %copy-start = (bf16[512,2048]{1,0:T(8,128)(2,1)S(1)}, bf16[512,2048]{1,0:T(8,128)(2,1)}, u32[]{:S(2)}) copy-start(bf16[512,2048]{1,0:T(8,128)(2,1)} %param.12) | copy-start | bytes 6291460
  92.8 42.2 %copy-start.7 = (f32[1,512]{1,0:T(1,128)S(1)}, f32[1,512]{1,0:T(1,128)}, u32[]{:S(2)}) copy-start(f32[1,512]{1,0:T(1,128)} %param.23) | copy-start | bytes 6148
  92.8 42.2 %copy-start.8 = (f32[1,512]{1,0:T(1,128)S(1)}, f32[1,512]{1,0:T(1,128)}, u32[]{:S(2)}) copy-start(f32[1,512]{1,0:T(1,128)} %param.22) | copy-start | bytes 6148
  92.8 42.2 %copy-start.9 = (f32[1,512]{1,0:T(1,128)S(1)}, f32[1,512]{1,0:T(1,128)}, u32[]{:S(2)}) copy-start(f32[1,512]{1,0:T(1,128)} %param.21) | copy-start | bytes 6148
  92.8 42.2 %copy-start.10 = (f32[1,512]{1,0:T(1,128)S(1)}, f32[1,512]{1,0:T(1,128)}, u32[]{:S(2)}) copy-start(f32[1,512]{1,0:T(1,128)} %param.20) | copy-start | bytes 6148
  178.3 3.7 %copy-start.4 = (bf16[32,8,8,128]{3,1,2,0:T(8,128)(2,1)}, bf16[32,8,8,128]{3,1,2,0:T(8,128)(2,1)S(1)}, u32[]{:S(2)}) copy-start(bf16[32,8,8,128]{3,1,2,0:T(8,128)(2,1)S(1)} %copy.45) | copy-start | bytes 1572868
  178.3 3.7 %copy-start.3 = (bf16[1,32,4,2,8,2,128]{6,4,5,3,2,1,0:T(8,128)(2,1)S(1)}, bf16[1,32,4,2,8,2,128]{6,4,5,3,2,1,0:T(8,128)(2,1)}, u32[]{:S(2)}) copy-start(bf16[1,32,4,2,8,2,128]{6,4,5,3,2,1,0:T(8,128)(2,1)} %copy.37) | copy-start | bytes 3145732
  182.0 13.8 %copy-start.12 = (bf16[8,256]{1,0:T(8,128)(2,1)S(1)}, bf16[8,256]{1,0:T(8,128)(2,1)}, u32[]{:S(2)}) copy-start(bf16[8,256]{1,0:T(8,128)(2,1)} %param.17) | copy-start | bytes 12292
  182.1 15.1 %copy-start.11 = (f32[8,512]{1,0:T(8,128)S(1)}, f32[8,512]{1,0:T(8,128)}, u32[]{:S(2)}) copy-start(f32[8,512]{1,0:T(8,128)} %param.18) | copy-start | bytes 49156
  182.1 15.1 %copy-start.13 = (bf16[8,256]{1,0:T(8,128)(2,1)S(1)}, bf16[8,256]{1,0:T(8,128)(2,1)}, u32[]{:S(2)}) copy-start(bf16[8,256]{1,0:T(8,128)(2,1)} %param.16) | copy-start | bytes 12292
  182.1 17.0 %copy-start.5 = (f32[512,8]{0,1:T(8,128)S(1)}, f32[512,8]{0,1:T(8,128)}, u32[]{:S(2)}) copy-start(f32[512,8]{0,1:T(8,128)} %param.19) | copy-start | bytes 49156
  197.1 68.1 %copy-start.6 = (f32[512,8]{0,1:T(8,128)}, f32[512,8]{0,1:T(8,128)S(1)}, u32[]{:S(2)}) copy-start(f32[512,8]{0,1:T(8,128)S(1)} %fusion.3) | copy-start | bytes 49156
  265.2 25.3 %all-to-all-start.9 = ((bf16[4,32,8,1024]{3,2,1,0:T(8,128)(2,1)}), bf16[4,32,8,1024]{3,2,1,0:T(8,128)(2,1)}, u32[]{:S(2)}, u32[]{:S(2)}) async-start(bf16[4,32,8,1024]{3,2,1,0:T(8,128)(2,1)} %broadcast_in_dim.28), calls=%async_computation.9 | async-start | bytes 4194304 | tf_op jit(solution)/shard_map/wx/all_to_all | solution.py:14
  306.2 3.6 %copy-start.1 = (f32[512,2048]{0,1:T(8,128)S(1)}, f32[512,2048]{0,1:T(8,128)}, u32[]{:S(2)}) copy-start(f32[512,2048]{0,1:T(8,128)} %copy.40) | copy-start | bytes 12582916
  306.9 2.1 copy-start.2

commit v2 on v1

v2 whole, which is shorter than its diff:
```python
import jax
import jax.numpy as jnp
from jax import lax
from jax.experimental import pallas as pl
from jax.experimental.pallas import tpu as pltpu
from jax.sharding import Mesh
from jax.sharding import PartitionSpec as P

D = 2048
WIDTH = 2048
R = 256
FS = ("zh", "zl", "x", "c")
Z = ("zh", "zl")
LANES = 128
NT = (((1,), (1,)), ((), ()))
TN = (((0,), (0,)), ((), ()))


VMEM = pl.BlockSpec(memory_space=pltpu.VMEM)
SMEM = pl.BlockSpec(memory_space=pltpu.SMEM)
HBM = pl.BlockSpec(memory_space=pltpu.HBM)


def far(*arrays):
    return [pltpu.with_memory_space_constraint(a, pltpu.HBM) for a in arrays]


def params(mib):
    return pltpu.CompilerParams(vmem_limit_bytes=mib << 20)


def cost(flops, bytes_accessed):
    return pl.CostEstimate(flops=flops, bytes_accessed=bytes_accessed, transcendentals=0)


def dot(a, b, dims=(((1,), (0,)), ((), ()))):
    return lax.dot_general(a, b, dims, preferred_element_type=jnp.float32)


def eye(n):
    i = lax.broadcasted_iota(jnp.int32, (n, n), 0)
    return (i == lax.broadcasted_iota(jnp.int32, (n, n), 1)).astype(jnp.bfloat16)


def exchange(blocks, axes):
    return lax.all_to_all(blocks, axes, split_axis=0, concat_axis=0, tiled=True)


def to_all(block, axes):
    copies = jnp.broadcast_to(block[None], (lax.axis_size(axes), *block.shape))
    return exchange(copies, axes)


def moved(block, axis, by):
    n = lax.axis_size(axis)
    return lax.ppermute(block, axis, [(i, (i + by) % n) for i in range(n)])


def swapped(block, axis, bit):
    return lax.ppermute(block, axis, [(i, i ^ bit) for i in range(lax.axis_size(axis))])


def pack_kernel(place, fv, fo, wv, wo, out, fv_in, fo_in, wv_in, wo_in, sems):
    copies = [
        pltpu.make_async_copy(src, dst, sems.at[i])
        for i, (src, dst) in enumerate(((fv, fv_in), (fo, fo_in), (wv, wv_in), (wo, wo_in)))
    ]
    for copy in copies:
        copy.start()
    n = R // 8
    y = place[0]
    j = lax.broadcasted_iota(jnp.int32, (R, R), 0)
    k = lax.broadcasted_iota(jnp.int32, (R, R), 1)
    turn = (j == (k % n) * 8 + k // n).astype(jnp.bfloat16)
    for copy in copies:
        copy.wait()
    factor = jnp.where(y < 2, fv_in[...].astype(jnp.float32), fo_in[...].astype(jnp.float32))
    factor = dot(factor.astype(jnp.bfloat16), turn)
    tile = jnp.where(y % 2 == 0, factor[:, :LANES], factor[:, LANES:]).astype(jnp.bfloat16)
    tiles = [tile]
    for w in (wv_in, wo_in):
        half = w[...].astype(jnp.bfloat16)
        tiles += [half[:, t : t + LANES] for t in range(0, half.shape[1], LANES)]
    for t, tile in enumerate(tiles):
        out[:, t] = jnp.broadcast_to(tile[None], (out.shape[0], *tile.shape))


def packed(count, place, fv, fo, wv, wo):
    rows, cols = wv.shape
    tiles = 1 + 2 * cols // LANES
    return pl.pallas_call(
        pack_kernel,
        out_shape=jax.ShapeDtypeStruct((count, tiles, rows, LANES), jnp.bfloat16),
        in_specs=[SMEM, HBM, HBM, HBM, HBM],
        out_specs=VMEM,
        scratch_shapes=[
            pltpu.VMEM(fv.shape, fv.dtype),
            pltpu.VMEM(fo.shape, fo.dtype),
            pltpu.VMEM(wv.shape, wv.dtype),
            pltpu.VMEM(wo.shape, wo.dtype),
            pltpu.SemaphoreType.DMA((4,)),
        ],
        name="packed",
        compiler_params=params(4),
        cost_estimate=cost(2 * 8 * R * R, 200_000),
    )(place, *far(fv, fo, wv, wo))


def project_kernel(
    place, mine, other, xv, vv, xo, vo, out, fv, fo, whole, x_in, v_in, sems
):
    c = place[2]
    reads = [
        pltpu.make_async_copy(src, dst.at[f], sems.at[2 * f + k])
        for f, pair in enumerate(((xv, vv), (xo, vo)))
        for k, (src, dst) in enumerate(zip(pair, (x_in, v_in)))
    ]
    for copy in reads:
        copy.start()
    nzl, nx = whole.shape[2:4]
    half = R // LANES
    writes = []
    for f, target in enumerate((fv, fo)):
        for src, at in ((mine, c), (other, 1 - c)):
            for x in range(nx):
                for h in range(half):
                    for zl in range(nzl):
                        whole[f, :, zl, x, at, :, h * LANES : (h + 1) * LANES] = src[
                            x * 2 * half + f * half + h, zl
                        ]
        writes.append(pltpu.make_async_copy(whole.at[f], target, sems.at[4 + f]))
        writes[f].start()
    cols = vv.shape[1]
    for f in range(2):
        reads[2 * f].wait()
        projected = dot(x_in[f], whole[f].reshape(D, R)).astype(jnp.bfloat16)
        reads[2 * f + 1].wait()
        term = dot(projected, v_in[f], TN).astype(jnp.bfloat16)
        out[:, :, f * cols : (f + 1) * cols] = term.reshape(out.shape[0], out.shape[1], cols)
    for copy in writes:
        copy.wait()


def projected_terms(place, mine, other, xv, vv, xo, vo, sizes):
    nzh, nzl, nx, nc = sizes
    shape = (nzh, nzl, nx, nc, D // (nzh * nzl * nx * nc), R)
    whole = pltpu.HBM(shape, jnp.bfloat16)
    cols = vv.shape[1]
    tokens = xv.shape[0]
    return pl.pallas_call(
        project_kernel,
        out_shape=(
            jax.ShapeDtypeStruct((nx * nc, nzh * nzl, 2 * cols), jnp.bfloat16),
            whole,
            whole,
        ),
        in_specs=[SMEM, VMEM, VMEM, HBM, HBM, HBM, HBM],
        out_specs=(VMEM, HBM, HBM),
        scratch_shapes=[
            pltpu.VMEM((2, *shape), jnp.bfloat16),
            pltpu.VMEM((2, *xv.shape), jnp.bfloat16),
            pltpu.VMEM((2, *vv.shape), jnp.bfloat16),
            pltpu.SemaphoreType.DMA((6,)),
        ],
        name="project",
        compiler_params=params(20),
        cost_estimate=cost(4 * tokens * R * (D + cols), 10_000_000),
    )(place, mine, other, *far(xv, vv, xo, vo))


def summed_kernel(t, out, lines):
    total = jnp.sum(t[...].astype(jnp.float32), axis=0)
    nz, tiles, _ = out.shape
    for k in range(tiles):
        lines[pl.ds(k, nz, stride=tiles), :] = total[:, k * LANES : (k + 1) * LANES]
    out[...] = lines[...].reshape(out.shape).astype(jnp.bfloat16)


def summed(t):
    _, nz, width = t.shape
    tiles = width // LANES
    return pl.pallas_call(
        summed_kernel,
        out_shape=jax.ShapeDtypeStruct((nz, tiles, LANES), jnp.bfloat16),
        in_specs=[VMEM],
        out_specs=VMEM,
        scratch_shapes=[pltpu.VMEM((nz * tiles, LANES), jnp.float32)],
        name="summed",
        compiler_params=params(2),
        cost_estimate=cost(t.size, 600_000),
    )(t)


def gram_kernel(fv, fo, out, factors, grams, sems):
    reads = [
        pltpu.make_async_copy(src, factors.at[f], sems.at[f]) for f, src in enumerate((fv, fo))
    ]
    for copy in reads:
        copy.start()
    for f, copy in enumerate(reads):
        copy.wait()
        factor = factors[f].reshape(D, R)
        gram = dot(factor, factor, TN)
        high = gram.astype(jnp.bfloat16)
        grams[f, 0] = high
        grams[f, 1] = (gram - high.astype(jnp.float32)).astype(jnp.bfloat16)
    write = pltpu.make_async_copy(grams, out, sems.at[2])
    write.start()
    write.wait()


def gram_of(fv, fo):
    shape = (2, 2, R, R)
    return pl.pallas_call(
        gram_kernel,
        out_shape=pltpu.HBM(shape, jnp.bfloat16),
        in_specs=[HBM, HBM],
        out_specs=HBM,
        scratch_shapes=[
            pltpu.VMEM((2, *fv.shape), jnp.bfloat16),
            pltpu.VMEM(shape, jnp.bfloat16),
            pltpu.SemaphoreType.DMA((3,)),
        ],
        name="gram",
        compiler_params=params(8),
        cost_estimate=cost(4 * D * R * R, 3_000_000),
    )(*far(fv, fo))


def moments_kernel(t, fv, sv, fo, so, out, nfv, nsv, nfo, nso):
    low = jnp.sum(t[...].astype(jnp.float32), axis=0)
    half = low.shape[0] // 2
    directions = []
    for part, first, second, next_first, next_second in (
        (low[:half], fv, sv, nfv, nsv),
        (low[half:], fo, so, nfo, nso),
    ):
        a = 0.9 * first[...] + 0.1 * part
        b = 0.95 * second[...] + 0.05 * part * part
        next_first[...] = a
        next_second[...] = b
        directions.append(a * lax.rsqrt(b))
    d = jnp.concatenate(directions, axis=0).astype(jnp.bfloat16)
    out[...] = jnp.broadcast_to(d[None], out.shape)


def moments(t, *state):
    shape = jax.ShapeDtypeStruct(state[0].shape, jnp.float32)
    return pl.pallas_call(
        moments_kernel,
        out_shape=(jax.ShapeDtypeStruct(t.shape, jnp.bfloat16), shape, shape, shape, shape),
        in_specs=[VMEM] * 5,
        out_specs=(VMEM,) * 5,
        name="moments",
        compiler_params=params(2),
        cost_estimate=cost(100_000, 150_000),
    )(t, *state)


def total_kernel(d, gram, out, dv, turned, gram_in, lines, whole, across, sems):
    read = pltpu.make_async_copy(gram, gram_in, sems.at[0])
    read.start()
    tiles = d.shape[1]
    lines[...] = d[...].astype(jnp.float32).reshape(lines.shape)
    for k in range(tiles):
        part = lines[pl.ds(k, R, stride=tiles), :].astype(jnp.bfloat16)
        whole[k // (tiles // 2), :, pl.ds(k % (tiles // 2) * LANES, LANES)] = part
    write_v = pltpu.make_async_copy(whole.at[0], dv, sems.at[1])
    write_v.start()
    across[...] = dot(eye(across.shape[0]), whole[1], NT).astype(jnp.bfloat16)
    write_o = pltpu.make_async_copy(across, turned, sems.at[2])
    write_o.start()
    read.wait()
    rows = out.shape[1] // 2
    for f in range(2):
        part = whole[f]
        square = part.astype(jnp.float32) * (dot(gram_in[f, 0], part) + dot(gram_in[f, 1], part))
        out[:, f * rows : (f + 1) * rows] = jnp.full(
            (out.shape[0], rows, LANES), jnp.sum(square)
        )
    write_v.wait()
    write_o.wait()


def totals_of(count, d, gram):
    _, tiles, _ = d.shape
    cols = tiles // 2 * LANES
    return pl.pallas_call(
        total_kernel,
        out_shape=(
            jax.ShapeDtypeStruct((count, 8, LANES), jnp.float32),
            pltpu.HBM((R, cols), jnp.bfloat16),
            pltpu.HBM((cols, R), jnp.bfloat16),
        ),
        in_specs=[VMEM, HBM],
        out_specs=(VMEM, HBM, HBM),
        scratch_shapes=[
            pltpu.VMEM(gram.shape, jnp.bfloat16),
            pltpu.VMEM((R * tiles, LANES), jnp.float32),
            pltpu.VMEM((2, R, cols), jnp.bfloat16),
            pltpu.VMEM((cols, R), jnp.bfloat16),
            pltpu.SemaphoreType.DMA((3,)),
        ],
        name="totals",
        compiler_params=params(6),
        cost_estimate=cost(8 * R * R * cols, 2_000_000),
    )(d, *far(gram))


def assemble_kernel(place, *refs):
    parts, (value, output, tiles_in, turned, sems) = refs[:-5], refs[-5:]
    zl, x, c = place[1], place[3], place[2]
    nx = len(parts) // 2
    nzl, nzh = parts[0].shape[:2]
    half = (parts[0].shape[2] - 1) // 2
    reads = []
    for f in range(2):
        for k, part in enumerate(parts):
            px = lax.rem(x + nx - k % nx, nx)
            pc = c if k < nx else 1 - c
            for s in range(nzl):
                reads.append(
                    pltpu.make_async_copy(
                        part.at[s, :, pl.ds(1 + f * half, half)],
                        tiles_in.at[f, :, lax.bitwise_xor(zl, s), px, pc],
                        sems.at[f],
                    )
                )
    for copy in reads:
        copy.start()
    for copy in reads[: len(reads) // 2]:
        copy.wait()
    write_v = pltpu.make_async_copy(tiles_in.at[0], value, sems.at[2])
    write_v.start()
    for copy in reads[len(reads) // 2 :]:
        copy.wait()
    chunk = D // nzh
    one = eye(half * LANES)
    for i in range(nzh):
        w = tiles_in[1, i]
        w = jnp.concatenate(
            [w[:, :, :, t].reshape(chunk, LANES) for t in range(half)], axis=1
        )
        turned[:, i * chunk : (i + 1) * chunk] = dot(one, w, NT).astype(jnp.bfloat16)
    write_o = pltpu.make_async_copy(turned, output, sems.at[3])
    write_o.start()
    write_v.wait()
    write_o.wait()


def assembled(place, parts, sizes):
    nzh, nzl, nx, nc = sizes
    _, _, tiles, rows, _ = parts[0].shape
    half = (tiles - 1) // 2
    cols = half * LANES
    shape = (nzh, nzl, nx, nc, half, rows, LANES)
    value, output = pl.pallas_call(
        assemble_kernel,
        out_shape=(
            pltpu.HBM(shape, jnp.bfloat16),
            pltpu.HBM((cols, D), jnp.bfloat16),
        ),
        in_specs=[SMEM] + [HBM] * len(parts),
        out_specs=(HBM, HBM),
        scratch_shapes=[
            pltpu.VMEM((2, *shape), jnp.bfloat16),
            pltpu.VMEM((cols, D), jnp.bfloat16),
            pltpu.SemaphoreType.DMA((4,)),
        ],
        name="assemble",
        compiler_params=params(12),
        cost_estimate=cost(2 * cols * cols * D, 9_000_000),
    )(place, *far(*parts))
    return value.reshape(D // rows, half, rows, LANES), output


def final_kernel(place, totals, dv, turned, fv, fo, wv, wo, ov, oo, own_v, own_o, copy_v, copy_o, sv, so, nv, no):
    entries = D * WIDTH
    sums = jnp.sum(totals[...], axis=0)
    scale = lax.rsqrt(sums / entries + 1e-06)
    scale_v, scale_o = scale[:1, :1], scale[4:5, :1]
    chunk = copy_v.shape[0]

    @pl.when(pl.program_id(0) == 0)
    def _():
        step_v = dot(own_v[0], dv[...]) * scale_v
        step_o = dot(own_o[0], turned[...], NT) * scale_o
        sv[...] = step_v
        so[...] = step_o
        nv[...] = ov[...] - 0.02 * step_v
        no[...] = oo[...] - 0.02 * step_o

    whole_v = fv[...].reshape(chunk, R)
    whole_o = fo[...].reshape(chunk, R)
    update = dot(whole_v, dv[...]) * (0.02 * scale_v)
    for t in range(wv.shape[1]):
        lanes = slice(t * LANES, (t + 1) * LANES)
        copy_v[:, lanes] = (
            wv[:, t].astype(jnp.float32).reshape(chunk, LANES) - update[:, lanes]
        ).astype(jnp.bfloat16)
    copy_o[...] = (
        wo[...].astype(jnp.float32) - dot(turned[...], whole_o, NT) * (0.02 * scale_o)
    ).astype(jnp.bfloat16)


def final(place, totals, dv, turned, fv, fo, wv, wo, ov, oo):
    cols = turned.shape[0]
    rows = ov.shape[0]
    steps = 8
    chunk = D // steps
    own = pltpu.HBM(ov.shape, jnp.float32)
    factor = pl.BlockSpec((chunk // rows, rows, R), lambda i, p: (i, 0, 0))
    mine = pl.BlockSpec((1, rows, R), lambda i, p: (p[4], 0, 0))
    down = pl.BlockSpec((chunk, cols), lambda i, p: (i, 0))
    across = pl.BlockSpec((cols, chunk), lambda i, p: (0, i))
    blocks = pl.BlockSpec((chunk // rows, wv.shape[1], rows, LANES), lambda i, p: (i, 0, 0, 0))

    def same(a):
        return pl.BlockSpec(a.shape, lambda i, p: (0,) * a.ndim)

    return pl.pallas_call(
        final_kernel,
        out_shape=(
            pltpu.HBM((D, cols), jnp.bfloat16),
            pltpu.HBM((cols, D), jnp.bfloat16),
            own,
            own,
            own,
            own,
        ),
        grid_spec=pltpu.PrefetchScalarGridSpec(
            num_scalar_prefetch=1,
            grid=(steps,),
            in_specs=[same(totals), same(dv), same(turned), factor, factor, blocks, across]
            + [same(ov), same(oo), mine, mine],
            out_specs=(down, across, same(ov), same(ov), same(ov), same(ov)),
        ),
        name="final",
        compiler_params=params(60),
        cost_estimate=cost(4 * D * cols * R, 10_000_000),
    )(place, totals, *far(dv, turned, fv, fo, wv, wo, ov, oo, fv, fo))


def step(
    normed_input,
    value_cotangent,
    gated_output,
    layer_cotangent,
    factor_value,
    factor_output,
    weight_value,
    weight_output,
    first_value,
    second_value,
    first_output,
    second_output,
):
    sizes = tuple(lax.axis_size(a) for a in FS)
    nzh, _, _, _ = sizes
    ny = lax.axis_size("tp")
    rows, cols = weight_value.shape

    at = [lax.axis_index(a) for a in ("tp", "zl", "c", "x", FS)]
    place = jnp.stack(at).astype(jnp.int32)
    turned_weight = weight_output.T
    w = exchange(packed(nzh, place, factor_value, factor_output, weight_value, turned_weight), "zh")
    f = to_all(w[:, 0], "zl")
    f = to_all(f, ("x", "tp"))
    other = moved(f, "c", 1)

    wa = swapped(w, "zl", 1)
    wa = jnp.stack([w, wa])
    wb = swapped(wa, "zl", 2)
    w0 = jnp.concatenate([wa, wb])

    terms, whole_value, whole_output = projected_terms(
        place, f, other, normed_input, value_cotangent, layer_cotangent, gated_output, sizes
    )
    t = exchange(terms, ("x", "c"))
    t = summed(t)
    t = exchange(t, Z)

    w1 = moved(w0, "x", 1)
    w3 = moved(w0, "x", 3)
    v0 = moved(w0, "c", 1)

    narrow = (2 * cols // (8 * LANES) * 4, LANES)
    d, *state = moments(
        t, *(s.reshape(narrow) for s in (first_value, second_value, first_output, second_output))
    )
    next_first_value, next_second_value, next_first_output, next_second_output = (
        s.reshape(1, cols) for s in state
    )
    d = exchange(d, Z)

    w2 = moved(w1, "x", 1)
    v1 = moved(w1, "c", 1)
    v3 = moved(w3, "c", 1)

    d = to_all(d, ("x", "c"))
    v2 = moved(w2, "c", 1)
    totals, dv, turned = totals_of(
        ny, d.reshape(R, *d.shape[2:]), gram_of(whole_value, whole_output)
    )
    totals = exchange(totals, "tp")

    all_value, all_output = assembled(place, (w0, w1, w2, w3, v0, v1, v2, v3), sizes)
    blocks = (D // rows, rows, R)
    copy_value, copy_output, step_value, step_output, next_value, next_output = final(
        place,
        totals,
        dv,
        turned,
        whole_value.reshape(blocks),
        whole_output.reshape(blocks),
        all_value,
        all_output,
        weight_value,
        turned_weight,
    )
    return (
        step_value,
        step_output.T,
        next_value,
        next_output.T,
        next_first_value,
        next_second_value,
        next_first_output,
        next_second_output,
        copy_value,
        copy_output,
    )


def solution(mesh):
    torus = Mesh(
        mesh.devices.reshape(8, 4, 4, 2, mesh.shape["tp"]), ("zh", "zl", "x", "c", "tp")
    )
    placed = (
        P(FS, None),
        P(FS, "tp"),
        P(FS, "tp"),
        P(FS, None),
        P(FS, None),
        P(FS, None),
        P(FS, "tp"),
        P("tp", FS),
        P(FS, "tp"),
        P(FS, "tp"),
        P(FS, "tp"),
        P(FS, "tp"),
    )
    return jax.shard_map(
        step,
        mesh=torus,
        in_specs=placed,
        out_specs=(
            P(FS, "tp"),
            P("tp", FS),
            P(FS, "tp"),
            P("tp", FS),
            P(FS, "tp"),
            P(FS, "tp"),
            P(FS, "tp"),
            P(FS, "tp"),
            P(None, "tp"),
            P("tp", None),
        ),
        check_vma=False,
    )
```

time: 322 us -> 226 us (0.70)
  blocking collectives: 249 us -> 87.9 us
  starting transfers between devices: 4.47 us -> 53.2 us
  waiting for transfers between devices: 15.5 us -> 48.8 us
  Pallas kernels: 0 us -> 30.7 us
  local copies, waits for them, and re-layouts: 20.4 us -> 2.63 us
  matrix products: 17.3 us -> 0 us
  other arithmetic: 11.8 us -> 0.09 us
    all_to_all x10 -> x3, blocking collectives: 249 us -> 87.9 us  [exchange(): return lax.all_to_all(blocks, axes, split_axis=0, concat_axis=0, tiled=True)]
    pallas_call x0 -> x8, Pallas kernels: none -> 30.7 us  [the longest x1 9.15 us: final(): pl.pallas_call(final_kernel, out_shape=(pltpu.HBM((D, cols), jnp.bfloat16...]
    ppermute x0 -> x10, starting transfers between devices: none -> 28.4 us  [the longest x8 23.2 us: moved(): return lax.ppermute(block, axis, [(i, (i + by) % n) for i in range(n)])]
    all_to_all x1 -> x5, waiting for transfers between devices: 15.5 us -> 36.8 us  [exchange(): return lax.all_to_all(blocks, axes, split_axis=0, concat_axis=0, tiled=True)]
    all_to_all x1 -> x5, starting transfers between devices: 4.47 us -> 24.9 us  [exchange(): return lax.all_to_all(blocks, axes, split_axis=0, concat_axis=0, tiled=True)]
    dot_general x7 -> x0, matrix products: 17.3 us -> none  [the longest x1 3.75 us: body(): lax.dot_general(d_output, whole_output, (((0,), (1,)), ((), ())), preferr...]
    ppermute x0 -> x10, waiting for transfers between devices: none -> 12 us  [the longest x2 7.92 us: swapped(): lax.ppermute(block, axis, [(i, i ^ bit) for i in range(lax.axis_size(axis...]
    convert_element_type x3 -> x0, other arithmetic: 7.63 us -> none  [the longest x1 4.91 us: body(): (w[:, :cols] - 0.02 * scale_value * update_value).astype(jnp.bfloat16)]
  transfers between devices with their start and end apart: 1 -> 15, of which waited for: 1 -> 7; matrix products, arithmetic and copies ran while one was open for 2% -> 0% of each run, Pallas kernels for 0% -> 9%
where the time goes in v2:
time: 226 us; the launch traced here: 224 us
  blocking collectives  87.9 us (39%)
  starting transfers between devices  53.2 us (24%)
  waiting for transfers between devices  48.8 us (22%)
  Pallas kernels  30.7 us (14%)
  local copies, waits for them, and re-layouts  2.63 us (1%)
    all_to_all x3, blocking collectives, exchange(): return lax.all_to_all(blocks, axes, split_axis=0, concat_axis=0, tiled=True)  87.9 us
    all_to_all x5, waiting for transfers between devices, exchange(): return lax.all_to_all(blocks, axes, split_axis=0, concat_axis=0, tiled=True)  36.8 us
    all_to_all x5, starting transfers between devices, exchange(): return lax.all_to_all(blocks, axes, split_axis=0, concat_axis=0, tiled=True)  24.9 us
    ppermute x8, starting transfers between devices, moved(): return lax.ppermute(block, axis, [(i, (i + by) % n) for i in range(n)])  23.2 us
    pallas_call x1, Pallas kernels, final(): pl.pallas_call(final_kernel, out_shape=(pltpu.HBM((D, cols), jnp.bfloat16...  9.15 us
    ppermute x2, waiting for transfers between devices, swapped(): lax.ppermute(block, axis, [(i, i ^ bit) for i in range(lax.axis_size(axis...  7.92 us
    pallas_call x1, Pallas kernels, projected_terms(): pl.pallas_call(project_kernel, out_shape=(jax.ShapeDtypeStruct((nx * nc,...  7.08 us
    pallas_call x1, Pallas kernels, assembled(): pl.pallas_call(assemble_kernel, out_shape=(pltpu.HBM(shape, jnp.bfloat16)...  5.43 us
  transfers between devices with their start and end apart: 15, of which 7 were waited for; matrix products, arithmetic and copies ran while one was open for 0% of the time, Pallas kernels for 9%

profile of v2, /device:TPU:1, one launch (start us, length us, event | category | flops | bytes accessed | tf_op | source)
XLA Modules:
  0.0 224.3 jit_solution(16375716583517500938)
XLA Ops:
  0.7 1.5 packed.1
  2.2 55.1 %all_to_all.40 = bf16[8,9,8,128]{3,2,1,0:T(8,128)(2,1)S(1)} all-to-all(bf16[8,9,8,128]{3,2,1,0:T(8,128)(2,1)S(1)} %packed.1), channel_id=1, replica_groups=mesh['zh'=8,'zl'=4,'x'=4,'c'=2,'tp'=4] {'zh'}, dimensions={0} | all-to-all | bytes 294912 | tf_op jit(solution)/shard_map/all_to_all | solution.py:46
  57.4 11.5 %all_to_all.41 = bf16[4,8,8,128]{3,2,1,0:T(8,128)(2,1)S(1)} all-to-all(bf16[4,8,8,128]{3,2,1,0:T(8,128)(2,1)S(1)} %broadcast_in_dim.9), channel_id=1, replica_groups=mesh['zh'=8,'zl'=4,'x'=4,'c'=2,'tp'=4] {'zl'}, dimensions={0} | all-to-all | bytes 131072 | tf_op jit(solution)/shard_map/all_to_all | solution.py:46
  69.1 21.3 %all_to_all.42.mine = bf16[16,4,8,8,128]{4,3,2,1,0:T(8,128)(2,1)S(1)} all-to-all(bf16[16,4,8,8,128]{4,3,2,1,0:T(8,128)(2,1)S(1)} %broadcast_in_dim.10), channel_id=1, replica_groups=mesh['zh'=8,'zl'=4,'x'=4,'c'=2,'tp'=4] {'x','tp'}, dimensions={0} | all-to-all | bytes 2097152 | tf_op jit(solution)/shard_map/all_to_all | solution.py:46
  90.4 5.2 %collective-permute-start = (bf16[16,4,8,8,128]{4,3,2,1,0:T(8,128)(2,1)S(1)}, bf16[16,4,8,8,128]{4,3,2,1,0:T(8,128)(2,1)S(1)}, u32[]{:S(2)}, u32[]{:S(2)}) collective-permute-start(bf16[16,4,8,8,128]{4,3,2,1,0:T(8,128)(2,1)S(1)} %all_to_all.42.mine), channel_id=1, source_target_pairs={{0,4},{4,0},{1,5},{5,1},{2,6},{6,2},{3,7},{7,3},{8,12},{12,8},{9,1... | collective-permute-start | bytes 3145736 | tf_op jit(solution)/shard_map/ppermute | solution.py:56
  95.6 2.5 %collective-permute-start.1 = (bf16[8,9,8,128]{3,2,1,0:T(8,128)(2,1)S(1)}, bf16[8,9,8,128]{3,2,1,0:T(8,128)(2,1)S(1)}, u32[]{:S(2)}, u32[]{:S(2)}) collective-permute-start(bf16[8,9,8,128]{3,2,1,0:T(8,128)(2,1)S(1)} %all_to_all.40), channel_id=1, source_target_pairs={{0,32},{32,0},{64,96},{96,64},{1,33},{33,1},{65,97},{97,65},{2,34}... | collective-permute-start | bytes 442376 | tf_op jit(solution)/shard_map/ppermute | solution.py:60
  98.2 4.7 %collective-permute-done.1 = bf16[8,9,8,128]{3,2,1,0:T(8,128)(2,1)S(1)} collective-permute-done((bf16[8,9,8,128]{3,2,1,0:T(8,128)(2,1)S(1)}, bf16[8,9,8,128]{3,2,1,0:T(8,128)(2,1)S(1)}, u32[]{:S(2)}, u32[]{:S(2)}) %collective-permute-start.1) | collective-permute-done | bytes 147488 | tf_op jit(solution)/shard_map/ppermute | solution.py:60
  102.9 2.7 %collective-permute-start.2 = (bf16[2,8,9,8,128]{4,3,2,1,0:T(8,128)(2,1)S(1)}, bf16[2,8,9,8,128]{4,3,2,1,0:T(8,128)(2,1)S(1)}, u32[]{:S(2)}, u32[]{:S(2)}) collective-permute-start(bf16[2,8,9,8,128]{4,3,2,1,0:T(8,128)(2,1)S(1)} %pad_maximum_fusion.1), channel_id=1, source_target_pairs={{0,64},{32,96},{64,0},{96,32},{1,65},{33,97},{65,1},{97,33},{2,66}... | collective-permute-start | bytes 884744 | tf_op jit(solution)/shard_map/ppermute | solution.py:60
  105.6 7.1 %project.1 = (bf16[8,32,1024]{2,1,0:T(8,128)(2,1)}, bf16[8,4,4,2,8,256]{5,4,3,2,1,0:T(8,128)(2,1)}, bf16[8,4,4,2,8,256]{5,4,3,2,1,0:T(8,128)(2,1)}) custom-call(s32[5]{0:T(128)S(1)} %stack.32.place, bf16[16,4,8,8,128]{4,3,2,1,0:T(8,128)(2,1)S(1)} %all_to_all.42.mine, bf16[16,4,8,8,128]{4,3,2,1,0:T(8,128)(2,1)S(1)} %collective-permute-done.other, ...), custom_call_target="tpu_custom_call" | custom-call | flops 1342177280 | bytes 10000000 | tf_op jit(solution)/shard_map/project/pallas_call | solution.py:150
  112.8 4.7 %all-to-all-start.3 = ((bf16[8,32,1024]{2,1,0:T(8,128)(2,1)}), bf16[8,32,1024]{2,1,0:T(8,128)(2,1)S(1)}, u32[]{:S(2)}, u32[]{:S(2)}) async-start(bf16[8,32,1024]{2,1,0:T(8,128)(2,1)} %get-tuple-element.29), calls=%async_computation.3 | async-start | bytes 1048576 | tf_op jit(solution)/shard_map/all_to_all | solution.py:46
  117.4 3.2 %collective-permute-done.2 = bf16[2,8,9,8,128]{4,3,2,1,0:T(8,128)(2,1)S(1)} collective-permute-done((bf16[2,8,9,8,128]{4,3,2,1,0:T(8,128)(2,1)S(1)}, bf16[2,8,9,8,128]{4,3,2,1,0:T(8,128)(2,1)S(1)}, u32[]{:S(2)}, u32[]{:S(2)}) %collective-permute-start.2) | collective-permute-done | bytes 294944 | tf_op jit(solution)/shard_map/ppermute | solution.py:60
  120.7 1.9 collective-permute-start.3
  122.6 4.2 %all-to-all-done.3.t = bf16[8,32,1024]{2,1,0:T(8,128)(2,1)S(1)} async-done(((bf16[8,32,1024]{2,1,0:T(8,128)(2,1)}), bf16[8,32,1024]{2,1,0:T(8,128)(2,1)S(1)}, u32[]{:S(2)}, u32[]{:S(2)}) %all-to-all-start.3) | async-done | bytes 524320 | tf_op jit(solution)/shard_map/all_to_all | solution.py:46
  127.5 5.1 %all-to-all-start.4 = ((bf16[32,8,128]{2,1,0:T(8,128)(2,1)}), bf16[32,8,128]{2,1,0:T(8,128)(2,1)S(1)}, u32[]{:S(2)}, u32[]{:S(2)}) async-start(bf16[32,8,128]{2,1,0:T(8,128)(2,1)} %summed.1), calls=%async_computation.4 | async-start | bytes 131072 | tf_op jit(solution)/shard_map/all_to_all | solution.py:46
  132.7 2.8 %collective-permute-start.5 = (bf16[4,8,9,8,128]{4,3,2,1,0:T(8,128)(2,1)S(1)}, bf16[4,8,9,8,128]{4,3,2,1,0:T(8,128)(2,1)S(1)}, u32[]{:S(2)}, u32[]{:S(2)}) collective-permute-start(bf16[4,8,9,8,128]{4,3,2,1,0:T(8,128)(2,1)S(1)} %pad_maximum_fusion.refs_0_), channel_id=1, source_target_pairs={{0,24},{8,0},{16,8},{24,16},{1,25},{9,1},{17,9},{25,17},{2,26},{10... | collective-permute-start | bytes 1769480 | tf_op jit(solution)/shard_map/ppermute | solution.py:56
  135.5 4.1 %collective-permute-done.3.refs_1_ = bf16[4,8,9,8,128]{4,3,2,1,0:T(8,128)(2,1)S(1)} collective-permute-done((bf16[4,8,9,8,128]{4,3,2,1,0:T(8,128)(2,1)S(1)}, bf16[4,8,9,8,128]{4,3,2,1,0:T(8,128)(2,1)S(1)}, u32[]{:S(2)}, u32[]{:S(2)}) %collective-permute-start.3) | collective-permute-done | bytes 589856 | tf_op jit(solution)/shard_map/ppermute | solution.py:56
  139.5 1.9 collective-permute-start.4
  141.5 14.7 %all-to-all-done.4.t = bf16[32,8,128]{2,1,0:T(8,128)(2,1)S(1)} async-done(((bf16[32,8,128]{2,1,0:T(8,128)(2,1)}), bf16[32,8,128]{2,1,0:T(8,128)(2,1)S(1)}, u32[]{:S(2)}, u32[]{:S(2)}) %all-to-all-start.4) | async-done | bytes 65568 | tf_op jit(solution)/shard_map/all_to_all | solution.py:46
  156.9 4.1 %all-to-all-start.5 = ((bf16[32,8,128]{2,1,0:T(8,128)(2,1)}), bf16[32,8,128]{2,1,0:T(8,128)(2,1)S(1)}, u32[]{:S(2)}, u32[]{:S(2)}) async-start(bf16[32,8,128]{2,1,0:T(8,128)(2,1)} %get-tuple-element.30), calls=%async_computation.5 | async-start | bytes 131072 | tf_op jit(solution)/shard_map/all_to_all | solution.py:46
  161.0 5.0 %collective-permute-start.6 = (bf16[4,8,9,8,128]{4,3,2,1,0:T(8,128)(2,1)S(1)}, bf16[4,8,9,8,128]{4,3,2,1,0:T(8,128)(2,1)S(1)}, u32[]{:S(2)}, u32[]{:S(2)}) collective-permute-start(bf16[4,8,9,8,128]{4,3,2,1,0:T(8,128)(2,1)S(1)} %pad_maximum_fusion.refs_0_), channel_id=1, source_target_pairs={{0,4},{4,0},{1,5},{5,1},{2,6},{6,2},{3,7},{7,3},{8,12},{12,8},{9,1... | collective-permute-start | bytes 1769480 | tf_op jit(solution)/shard_map/ppermute | solution.py:56
  166.0 1.9 collective-permute-start.7
  168.0 2.4 %collective-permute-start.9 = (bf16[4,8,9,8,128]{4,3,2,1,0:T(8,128)(2,1)S(1)}, bf16[4,8,9,8,128]{4,3,2,1,0:T(8,128)(2,1)}, u32[]{:S(2)}, u32[]{:S(2)}) collective-permute-start(bf16[4,8,9,8,128]{4,3,2,1,0:T(8,128)(2,1)S(1)} %collective-permute-done.5.refs_3_), channel_id=1, source_target_pairs={{0,4},{4,0},{1,5},{5,1},{2,6},{6,2},{3,7},{7,3},{8,12},{12,8},{9,1... | collective-permute-start | bytes 1769480 | tf_op jit(solution)/shard_map/ppermute | solution.py:56
  170.4 1.9 collective-permute-start.8
  172.3 12.0 %all-to-all-done.5 = bf16[32,8,128]{2,1,0:T(8,128)(2,1)S(1)} async-done(((bf16[32,8,128]{2,1,0:T(8,128)(2,1)}), bf16[32,8,128]{2,1,0:T(8,128)(2,1)S(1)}, u32[]{:S(2)}, u32[]{:S(2)}) %all-to-all-start.5) | async-done | bytes 65568 | tf_op jit(solution)/shard_map/all_to_all | solution.py:46
  184.3 0.9 broadcast_in_dim.22
  185.2 7.7 %all-to-all-start.6 = ((bf16[8,32,8,128]{3,2,1,0:T(8,128)(2,1)}), bf16[8,32,8,128]{3,2,1,0:T(8,128)(2,1)S(1)}, u32[]{:S(2)}, u32[]{:S(2)}) async-start(bf16[8,32,8,128]{3,2,1,0:T(8,128)(2,1)} %broadcast_in_dim.22), calls=%async_computation.6 | async-start | bytes 1048576 | tf_op jit(solution)/shard_map/all_to_all | solution.py:46
  192.9 3.5 %gram.1 = bf16[2,2,256,256]{3,2,1,0:T(8,128)(2,1)} custom-call(bf16[8,4,4,2,8,256]{5,4,3,2,1,0:T(8,128)(2,1)} %get-tuple-element.31.fv, bf16[8,4,4,2,8,256]{5,4,3,2,1,0:T(8,128)(2,1)} %get-tuple-element.32.fo), custom_call_target="tpu_custom_call" | custom-call | flops 536870912 | bytes 3000000 | tf_op jit(solution)/shard_map/gram/pallas_call | solution.py:214
  196.4 5.9 %all-to-all-done.6 = bf16[8,32,8,128]{3,2,1,0:T(8,128)(2,1)S(1)} async-done(((bf16[8,32,8,128]{3,2,1,0:T(8,128)(2,1)}), bf16[8,32,8,128]{3,2,1,0:T(8,128)(2,1)S(1)}, u32[]{:S(2)}, u32[]{:S(2)}) %all-to-all-start.6) | async-done | bytes 524320 | tf_op jit(solution)/shard_map/all_to_all | solution.py:46
  202.3 2.7 %totals.1 = (f32[4,8,128]{2,1,0:T(8,128)}, bf16[256,512]{1,0:T(8,128)(2,1)}, bf16[512,256]{1,0:T(8,128)(2,1)}) custom-call(bf16[256,8,128]{2,1,0:T(8,128)(2,1)S(1)} %bitcast.24, bf16[2,2,256,256]{3,2,1,0:T(8,128)(2,1)} %gram.1), custom_call_target="tpu_custom_call" | custom-call | flops 268435456 | bytes 2000000 | tf_op jit(solution)/shard_map/totals/pallas_call | solution.py:288
  205.0 3.3 %all-to-all-start.7 = ((f32[4,8,128]{2,1,0:T(8,128)}), f32[4,8,128]{2,1,0:T(8,128)S(1)}, u32[]{:S(2)}, u32[]{:S(2)}) async-start(f32[4,8,128]{2,1,0:T(8,128)} %get-tuple-element.33), calls=%async_computation.7 | async-start | bytes 32768 | tf_op jit(solution)/shard_map/all_to_all | solution.py:46
  209.1 5.4 %assemble.1 = (bf16[8,4,4,2,4,8,128]{6,5,4,3,2,1,0:T(8,128)(2,1)}, bf16[512,2048]{1,0:T(8,128)(2,1)}) custom-call(s32[5]{0:T(128)S(1)} %stack.32.place, bf16[4,8,9,8,128]{4,3,2,1,0:T(8,128)(2,1)} %copy-done.5, bf16[4,8,9,8,128]{4,3,2,1,0:T(8,128)(2,1)} %copy-done.6, bf16[4,8,9,8,128]{4,3,2,1,0:T(8,128)(2,1)} %copy-done.8, ...), custom_call_target="tpu_custom_call" | custom-call | flops 1073741824 | bytes 9000000 | tf_op jit(solution)/shard_map/assemble/pallas_call | solution.py:357
  215.2 9.1 %final.1 = (bf16[2048,512]{1,0:T(8,128)(2,1)}, bf16[512,2048]{1,0:T(8,128)(2,1)}, f32[8,512]{1,0:T(8,128)}, f32[8,512]{1,0:T(8,128)}, f32[8,512]{1,0:T(8,128)}, /*index=5*/f32[8,512]{1,0:T(8,128)}) custom-call(s32[5]{0:T(128)} %copy-done, f32[4,8,128]{2,1,0:T(8,128)} %copy-done.10, bf16[256,512]{1,0:T(8,128)(2,1)} %get-tuple-element.34.dv, ...), custom_call_target="tpu_custom_call" | custom-call | flops 1073741824 | bytes 10000000 | tf_op jit(solution)/shard_map/final/pallas_call | solution.py:421
  (38 shorter events, 3.3 us)
Async XLA Ops:
  0.7 207.6 %copy-start = (s32[5]{0:T(128)}, s32[5]{0:T(128)S(1)}, u32[]{:S(2)}) copy-start(s32[5]{0:T(128)S(1)} %stack.32.place) | copy-start | bytes 64
  90.4 15.2 %collective-permute-start = (bf16[16,4,8,8,128]{4,3,2,1,0:T(8,128)(2,1)S(1)}, bf16[16,4,8,8,128]{4,3,2,1,0:T(8,128)(2,1)S(1)}, u32[]{:S(2)}, u32[]{:S(2)}) collective-permute-start(bf16[16,4,8,8,128]{4,3,2,1,0:T(8,128)(2,1)S(1)} %all_to_all.42.mine), channel_id=1, source_target_pairs={{0,4},{4,0},{1,5},{5,1},{2,6},{6,2},{3,7},{7,3},{8,12},{12,8},{9,1... | collective-permute-start | bytes 3145736 | tf_op jit(solution)/shard_map/ppermute | solution.py:56
  95.6 7.3 %collective-permute-start.1 = (bf16[8,9,8,128]{3,2,1,0:T(8,128)(2,1)S(1)}, bf16[8,9,8,128]{3,2,1,0:T(8,128)(2,1)S(1)}, u32[]{:S(2)}, u32[]{:S(2)}) collective-permute-start(bf16[8,9,8,128]{3,2,1,0:T(8,128)(2,1)S(1)} %all_to_all.40), channel_id=1, source_target_pairs={{0,32},{32,0},{64,96},{96,64},{1,33},{33,1},{65,97},{97,65},{2,34}... | collective-permute-start | bytes 442376 | tf_op jit(solution)/shard_map/ppermute | solution.py:60
  102.9 17.7 %collective-permute-start.2 = (bf16[2,8,9,8,128]{4,3,2,1,0:T(8,128)(2,1)S(1)}, bf16[2,8,9,8,128]{4,3,2,1,0:T(8,128)(2,1)S(1)}, u32[]{:S(2)}, u32[]{:S(2)}) collective-permute-start(bf16[2,8,9,8,128]{4,3,2,1,0:T(8,128)(2,1)S(1)} %pad_maximum_fusion.1), channel_id=1, source_target_pairs={{0,64},{32,96},{64,0},{96,32},{1,65},{33,97},{65,1},{97,33},{2,66}... | collective-permute-start | bytes 884744 | tf_op jit(solution)/shard_map/ppermute | solution.py:60
  112.7 43.5 %copy-start.1 = (f32[1,512]{1,0:T(1,128)S(1)}, f32[1,512]{1,0:T(1,128)}, u32[]{:S(2)}) copy-start(f32[1,512]{1,0:T(1,128)} %param.20) | copy-start | bytes 6148
  112.7 43.4 %copy-start.2 = (f32[1,512]{1,0:T(1,128)S(1)}, f32[1,512]{1,0:T(1,128)}, u32[]{:S(2)}) copy-start(f32[1,512]{1,0:T(1,128)} %param.21) | copy-start | bytes 6148
  112.7 43.4 %copy-start.3 = (f32[1,512]{1,0:T(1,128)S(1)}, f32[1,512]{1,0:T(1,128)}, u32[]{:S(2)}) copy-start(f32[1,512]{1,0:T(1,128)} %param.22) | copy-start | bytes 6148
  112.7 43.4 %copy-start.4 = (f32[1,512]{1,0:T(1,128)S(1)}, f32[1,512]{1,0:T(1,128)}, u32[]{:S(2)}) copy-start(f32[1,512]{1,0:T(1,128)} %param.23) | copy-start | bytes 6148
  112.8 14.1 %all-to-all-start.3 = ((bf16[8,32,1024]{2,1,0:T(8,128)(2,1)}), bf16[8,32,1024]{2,1,0:T(8,128)(2,1)S(1)}, u32[]{:S(2)}, u32[]{:S(2)}) async-start(bf16[8,32,1024]{2,1,0:T(8,128)(2,1)} %get-tuple-element.29), calls=%async_computation.3 | async-start | bytes 1048576 | tf_op jit(solution)/shard_map/all_to_all | solution.py:46
  120.7 75.7 %copy-start.5 = (bf16[4,8,9,8,128]{4,3,2,1,0:T(8,128)(2,1)}, bf16[4,8,9,8,128]{4,3,2,1,0:T(8,128)(2,1)S(1)}, u32[]{:S(2)}) copy-start(bf16[4,8,9,8,128]{4,3,2,1,0:T(8,128)(2,1)S(1)} %pad_maximum_fusion.refs_0_) | copy-start | bytes 1769476
  120.7 18.8 %collective-permute-start.3 = (bf16[4,8,9,8,128]{4,3,2,1,0:T(8,128)(2,1)S(1)}, bf16[4,8,9,8,128]{4,3,2,1,0:T(8,128)(2,1)S(1)}, u32[]{:S(2)}, u32[]{:S(2)}) collective-permute-start(bf16[4,8,9,8,128]{4,3,2,1,0:T(8,128)(2,1)S(1)} %pad_maximum_fusion.refs_0_), channel_id=1, source_target_pairs={{0,8},{8,16},{16,24},{24,0},{1,9},{9,17},{17,25},{25,1},{2,10},{10... | collective-permute-start | bytes 1769480 | tf_op jit(solution)/shard_map/ppermute | solution.py:56
  127.5 28.6 %all-to-all-start.4 = ((bf16[32,8,128]{2,1,0:T(8,128)(2,1)}), bf16[32,8,128]{2,1,0:T(8,128)(2,1)S(1)}, u32[]{:S(2)}, u32[]{:S(2)}) async-start(bf16[32,8,128]{2,1,0:T(8,128)(2,1)} %summed.1), calls=%async_computation.4 | async-start | bytes 131072 | tf_op jit(solution)/shard_map/all_to_all | solution.py:46
  132.7 35.3 %collective-permute-start.5 = (bf16[4,8,9,8,128]{4,3,2,1,0:T(8,128)(2,1)S(1)}, bf16[4,8,9,8,128]{4,3,2,1,0:T(8,128)(2,1)S(1)}, u32[]{:S(2)}, u32[]{:S(2)}) collective-permute-start(bf16[4,8,9,8,128]{4,3,2,1,0:T(8,128)(2,1)S(1)} %pad_maximum_fusion.refs_0_), channel_id=1, source_target_pairs={{0,24},{8,0},{16,8},{24,16},{1,25},{9,1},{17,9},{25,17},{2,26},{10... | collective-permute-start | bytes 1769480 | tf_op jit(solution)/shard_map/ppermute | solution.py:56
  139.5 56.8 %copy-start.6 = (bf16[4,8,9,8,128]{4,3,2,1,0:T(8,128)(2,1)}, bf16[4,8,9,8,128]{4,3,2,1,0:T(8,128)(2,1)S(1)}, u32[]{:S(2)}) copy-start(bf16[4,8,9,8,128]{4,3,2,1,0:T(8,128)(2,1)S(1)} %collective-permute-done.3.refs_1_) | copy-start | bytes 1769476
  139.5 30.8 %collective-permute-start.4 = (bf16[4,8,9,8,128]{4,3,2,1,0:T(8,128)(2,1)S(1)}, bf16[4,8,9,8,128]{4,3,2,1,0:T(8,128)(2,1)S(1)}, u32[]{:S(2)}, u32[]{:S(2)}) collective-permute-start(bf16[4,8,9,8,128]{4,3,2,1,0:T(8,128)(2,1)S(1)} %collective-permute-done.3.refs_1_), channel_id=1, source_target_pairs={{0,8},{8,16},{16,24},{24,0},{1,9},{9,17},{17,25},{25,1},{2,10},{10... | collective-permute-start | bytes 1769480 | tf_op jit(solution)/shard_map/ppermute | solution.py:56
  156.9 27.5 %all-to-all-start.5 = ((bf16[32,8,128]{2,1,0:T(8,128)(2,1)}), bf16[32,8,128]{2,1,0:T(8,128)(2,1)S(1)}, u32[]{:S(2)}, u32[]{:S(2)}) async-start(bf16[32,8,128]{2,1,0:T(8,128)(2,1)} %get-tuple-element.30), calls=%async_computation.5 | async-start | bytes 131072 | tf_op jit(solution)/shard_map/all_to_all | solution.py:46
  161.0 47.3 %collective-permute-start.6 = (bf16[4,8,9,8,128]{4,3,2,1,0:T(8,128)(2,1)S(1)}, bf16[4,8,9,8,128]{4,3,2,1,0:T(8,128)(2,1)S(1)}, u32[]{:S(2)}, u32[]{:S(2)}) collective-permute-start(bf16[4,8,9,8,128]{4,3,2,1,0:T(8,128)(2,1)S(1)} %pad_maximum_fusion.refs_0_), channel_id=1, source_target_pairs={{0,4},{4,0},{1,5},{5,1},{2,6},{6,2},{3,7},{7,3},{8,12},{12,8},{9,1... | collective-permute-start | bytes 1769480 | tf_op jit(solution)/shard_map/ppermute | solution.py:56
  166.0 42.3 %collective-permute-start.7 = (bf16[4,8,9,8,128]{4,3,2,1,0:T(8,128)(2,1)S(1)}, bf16[4,8,9,8,128]{4,3,2,1,0:T(8,128)(2,1)}, u32[]{:S(2)}, u32[]{:S(2)}) collective-permute-start(bf16[4,8,9,8,128]{4,3,2,1,0:T(8,128)(2,1)S(1)} %collective-permute-done.3.refs_1_), channel_id=1, source_target_pairs={{0,4},{4,0},{1,5},{5,1},{2,6},{6,2},{3,7},{7,3},{8,12},{12,8},{9,1... | collective-permute-start | bytes 1769480 | tf_op jit(solution)/shard_map/ppermute | solution.py:56
  168.0 28.4 %copy-start.7 = (bf16[4,8,9,8,128]{4,3,2,1,0:T(8,128)(2,1)}, bf16[4,8,9,8,128]{4,3,2,1,0:T(8,128)(2,1)S(1)}, u32[]{:S(2)}) copy-start(bf16[4,8,9,8,128]{4,3,2,1,0:T(8,128)(2,1)S(1)} %collective-permute-done.5.refs_3_) | copy-start | bytes 1769476
  168.0 40.4 %collective-permute-start.9 = (bf16[4,8,9,8,128]{4,3,2,1,0:T(8,128)(2,1)S(1)}, bf16[4,8,9,8,128]{4,3,2,1,0:T(8,128)(2,1)}, u32[]{:S(2)}, u32[]{:S(2)}) collective-permute-start(bf16[4,8,9,8,128]{4,3,2,1,0:T(8,128)(2,1)S(1)} %collective-permute-done.5.refs_3_), channel_id=1, source_target_pairs={{0,4},{4,0},{1,5},{5,1},{2,6},{6,2},{3,7},{7,3},{8,12},{12,8},{9,1... | collective-permute-start | bytes 1769480 | tf_op jit(solution)/shard_map/ppermute | solution.py:56
  170.4 26.0 %copy-start.8 = (bf16[4,8,9,8,128]{4,3,2,1,0:T(8,128)(2,1)}, bf16[4,8,9,8,128]{4,3,2,1,0:T(8,128)(2,1)S(1)}, u32[]{:S(2)}) copy-start(bf16[4,8,9,8,128]{4,3,2,1,0:T(8,128)(2,1)S(1)} %collective-permute-done.4.refs_2_) | copy-start | bytes 1769476
  170.4 37.9 %collective-permute-start.8 = (bf16[4,8,9,8,128]{4,3,2,1,0:T(8,128)(2,1)S(1)}, bf16[4,8,9,8,128]{4,3,2,1,0:T(8,128)(2,1)}, u32[]{:S(2)}, u32[]{:S(2)}) collective-permute-start(bf16[4,8,9,8,128]{4,3,2,1,0:T(8,128)(2,1)S(1)} %collective-permute-done.4.refs_2_), channel_id=1, source_target_pairs={{0,4},{4,0},{1,5},{5,1},{2,6},{6,2},{3,7},{7,3},{8,12},{12,8},{9,1... | collective-permute-start | bytes 1769480 | tf_op jit(solution)/shard_map/ppermute | solution.py:56
  185.2 17.1 %all-to-all-start.6 = ((bf16[8,32,8,128]{3,2,1,0:T(8,128)(2,1)}), bf16[8,32,8,128]{3,2,1,0:T(8,128)(2,1)S(1)}, u32[]{:S(2)}, u32[]{:S(2)}) async-start(bf16[8,32,8,128]{3,2,1,0:T(8,128)(2,1)} %broadcast_in_dim.22), calls=%async_computation.6 | async-start | bytes 1048576 | tf_op jit(solution)/shard_map/all_to_all | solution.py:46
  205.0 9.5 %all-to-all-start.7 = ((f32[4,8,128]{2,1,0:T(8,128)}), f32[4,8,128]{2,1,0:T(8,128)S(1)}, u32[]{:S(2)}, u32[]{:S(2)}) async-start(f32[4,8,128]{2,1,0:T(8,128)} %get-tuple-element.33), calls=%async_computation.7 | async-start | bytes 32768 | tf_op jit(solution)/shard_map/all_to_all | solution.py:46
  208.3 0.8 copy-start.9
  214.6 0.6 copy-start.10

commit v3 on v2

v3 whole, which is shorter than its diff:
```python
import jax
import jax.numpy as jnp
from jax import lax
from jax.experimental import pallas as pl
from jax.experimental.pallas import tpu as pltpu
from jax.sharding import Mesh
from jax.sharding import PartitionSpec as P

D = 2048
WIDTH = 2048
R = 256
FS = ("zh", "zl", "x", "c")
Z = ("zh", "zl")
LANES = 128
TN = (((0,), (0,)), ((), ()))


VMEM = pl.BlockSpec(memory_space=pltpu.VMEM)
SMEM = pl.BlockSpec(memory_space=pltpu.SMEM)
HBM = pl.BlockSpec(memory_space=pltpu.HBM)


def far(*arrays):
    return [pltpu.with_memory_space_constraint(a, pltpu.HBM) for a in arrays]


def near(*arrays):
    return [pltpu.with_memory_space_constraint(a, pltpu.VMEM) for a in arrays]


def params(mib):
    return pltpu.CompilerParams(vmem_limit_bytes=mib << 20)


def cost(flops, bytes_accessed):
    return pl.CostEstimate(flops=flops, bytes_accessed=bytes_accessed, transcendentals=0)


def dot(a, b, dims=(((1,), (0,)), ((), ()))):
    return lax.dot_general(a, b, dims, preferred_element_type=jnp.float32)


def exchange(blocks, axes):
    return lax.all_to_all(blocks, axes, split_axis=0, concat_axis=0, tiled=True)


def to_all(block, axes):
    copies = jnp.broadcast_to(block[None], (lax.axis_size(axes), *block.shape))
    return exchange(copies, axes)


def moved(block, axis, by):
    n = lax.axis_size(axis)
    return lax.ppermute(block, axis, [(i, (i + by) % n) for i in range(n)])


def swapped(block, axis, bit):
    return lax.ppermute(block, axis, [(i, i ^ bit) for i in range(lax.axis_size(axis))])


def pack_kernel(place, fv, fo, wv, wo, vv, vo, out, vv_in, vo_in, fv_in, fo_in, wv_in, wo_in, sems):
    copies = [
        pltpu.make_async_copy(src, dst, sems.at[i])
        for i, (src, dst) in enumerate(
            ((fv, fv_in), (fo, fo_in), (wv, wv_in), (wo, wo_in), (vv, vv_in), (vo, vo_in))
        )
    ]
    for copy in copies:
        copy.start()
    n = R // 8
    y = place[0]
    j = lax.broadcasted_iota(jnp.int32, (R, R), 0)
    k = lax.broadcasted_iota(jnp.int32, (R, R), 1)
    turn = (j == (k % n) * 8 + k // n).astype(jnp.bfloat16)
    for copy in copies[:4]:
        copy.wait()
    factor = jnp.where(y < 2, fv_in[...].astype(jnp.float32), fo_in[...].astype(jnp.float32))
    factor = dot(factor.astype(jnp.bfloat16), turn)
    tile = jnp.where(y % 2 == 0, factor[:, :LANES], factor[:, LANES:]).astype(jnp.bfloat16)
    tiles = [tile]
    for w in (wv_in, wo_in):
        half = w[...].astype(jnp.bfloat16)
        tiles += [half[:, t : t + LANES] for t in range(0, half.shape[1], LANES)]
    for t, tile in enumerate(tiles):
        out[:, t] = jnp.broadcast_to(tile[None], (out.shape[0], *tile.shape))
    for copy in copies[4:]:
        copy.wait()


def packed(count, place, fv, fo, wv, wo, vv, vo):
    rows, cols = wv.shape
    tiles = 1 + 2 * cols // LANES
    return pl.pallas_call(
        pack_kernel,
        out_shape=(
            jax.ShapeDtypeStruct((count, tiles, rows, LANES), jnp.bfloat16),
            pltpu.VMEM(vv.shape, vv.dtype),
            pltpu.VMEM(vo.shape, vo.dtype),
        ),
        in_specs=[SMEM] + [HBM] * 6,
        out_specs=(VMEM,) * 3,
        scratch_shapes=[
            pltpu.VMEM(fv.shape, fv.dtype),
            pltpu.VMEM(fo.shape, fo.dtype),
            pltpu.VMEM(wv.shape, wv.dtype),
            pltpu.VMEM(wo.shape, wo.dtype),
            pltpu.SemaphoreType.DMA((6,)),
        ],
        name="packed",
        compiler_params=params(4),
        cost_estimate=cost(2 * 8 * R * R, 200_000),
    )(place, *far(fv, fo, wv, wo, vv, vo))


def project_kernel(place, mine, other, xv, vv, xo, vo, out, whole):
    c = place[2]
    nzl, nx = whole.shape[2:4]
    half = R // LANES
    cols = vv.shape[1]
    for f in range(2):
        for src, at in ((mine, c), (other, 1 - c)):
            for x in range(nx):
                for h in range(half):
                    for zl in range(nzl):
                        whole[f, :, zl, x, at, :, h * LANES : (h + 1) * LANES] = src[
                            x * 2 * half + f * half + h, zl
                        ]
    for f, (x, v) in enumerate(((xv, vv), (xo, vo))):
        projected = dot(x[...], whole[f].reshape(D, R)).astype(jnp.bfloat16)
        term = dot(projected, v[...], TN).astype(jnp.bfloat16)
        out[:, :, f * cols : (f + 1) * cols] = term.reshape(out.shape[0], out.shape[1], cols)


def projected_terms(place, mine, other, xv, vv, xo, vo, sizes):
    nzh, nzl, nx, nc = sizes
    shape = (2, nzh, nzl, nx, nc, D // (nzh * nzl * nx * nc), R)
    cols = vv.shape[1]
    tokens = xv.shape[0]
    return pl.pallas_call(
        project_kernel,
        out_shape=(
            jax.ShapeDtypeStruct((nx * nc, nzh * nzl, 2 * cols), jnp.bfloat16),
            pltpu.VMEM(shape, jnp.bfloat16),
        ),
        in_specs=[SMEM] + [VMEM] * 6,
        out_specs=(VMEM, VMEM),
        name="project",
        compiler_params=params(12),
        cost_estimate=cost(4 * tokens * R * (D + cols), 10_000_000),
    )(place, mine, other, *near(xv, vv, xo, vo))


def summed_kernel(t, out, lines):
    total = jnp.sum(t[...].astype(jnp.float32), axis=0)
    nz, tiles, _ = out.shape
    for k in range(tiles):
        lines[pl.ds(k, nz, stride=tiles), :] = total[:, k * LANES : (k + 1) * LANES]
    out[...] = lines[...].reshape(out.shape).astype(jnp.bfloat16)


def summed(t):
    _, nz, width = t.shape
    tiles = width // LANES
    return pl.pallas_call(
        summed_kernel,
        out_shape=jax.ShapeDtypeStruct((nz, tiles, LANES), jnp.bfloat16),
        in_specs=[VMEM],
        out_specs=VMEM,
        scratch_shapes=[pltpu.VMEM((nz * tiles, LANES), jnp.float32)],
        name="summed",
        compiler_params=params(2),
        cost_estimate=cost(t.size, 600_000),
    )(t)


def gram_kernel(factors, grams):
    for f in range(2):
        factor = factors[f].reshape(D, R)
        gram = dot(factor, factor, TN)
        high = gram.astype(jnp.bfloat16)
        grams[f, 0] = high
        grams[f, 1] = (gram - high.astype(jnp.float32)).astype(jnp.bfloat16)


def gram_of(factors):
    shape = (2, 2, R, R)
    return pl.pallas_call(
        gram_kernel,
        out_shape=pltpu.VMEM(shape, jnp.bfloat16),
        in_specs=[VMEM],
        out_specs=VMEM,
        name="gram",
        compiler_params=params(8),
        cost_estimate=cost(4 * D * R * R, 3_000_000),
    )(*near(factors))


def moments_kernel(t, fv, sv, fo, so, out, nfv, nsv, nfo, nso):
    low = jnp.sum(t[...].astype(jnp.float32), axis=0)
    half = low.shape[0] // 2
    directions = []
    for part, first, second, next_first, next_second in (
        (low[:half], fv, sv, nfv, nsv),
        (low[half:], fo, so, nfo, nso),
    ):
        a = 0.9 * first[...] + 0.1 * part
        b = 0.95 * second[...] + 0.05 * part * part
        next_first[...] = a
        next_second[...] = b
        directions.append(a * lax.rsqrt(b))
    d = jnp.concatenate(directions, axis=0).astype(jnp.bfloat16)
    out[...] = jnp.broadcast_to(d[None], out.shape)


def moments(t, *state):
    shape = jax.ShapeDtypeStruct(state[0].shape, jnp.float32)
    return pl.pallas_call(
        moments_kernel,
        out_shape=(jax.ShapeDtypeStruct(t.shape, jnp.bfloat16), shape, shape, shape, shape),
        in_specs=[VMEM] * 5,
        out_specs=(VMEM,) * 5,
        name="moments",
        compiler_params=params(2),
        cost_estimate=cost(100_000, 150_000),
    )(t, *state)


def total_kernel(d, gram, out, whole, lines):
    tiles = d.shape[1]
    half = tiles // 2
    lines[...] = d[...].astype(jnp.float32).reshape(lines.shape)
    parts = [lines[pl.ds(k, R, stride=tiles), :].astype(jnp.bfloat16) for k in range(tiles)]
    rows = out.shape[1] // 2
    for f in range(2):
        part = jnp.concatenate(parts[f * half : (f + 1) * half], axis=1)
        whole[f] = part
        square = part.astype(jnp.float32) * (dot(gram[f, 0], part) + dot(gram[f, 1], part))
        out[:, f * rows : (f + 1) * rows] = jnp.full(
            (out.shape[0], rows, LANES), jnp.sum(square)
        )


def totals_of(count, d, gram):
    _, tiles, _ = d.shape
    cols = tiles // 2 * LANES
    return pl.pallas_call(
        total_kernel,
        out_shape=(
            jax.ShapeDtypeStruct((count, 8, LANES), jnp.float32),
            pltpu.VMEM((2, R, cols), jnp.bfloat16),
        ),
        in_specs=[VMEM, VMEM],
        out_specs=(VMEM, VMEM),
        scratch_shapes=[pltpu.VMEM((R * tiles, LANES), jnp.float32)],
        name="totals",
        compiler_params=params(6),
        cost_estimate=cost(8 * R * R * cols, 2_000_000),
    )(d, *near(gram))


def assemble_kernel(place, *refs):
    parts, out = refs[:-2], refs[-1]
    zl, x = place[1], place[3]
    nx = len(parts)
    for k, part in enumerate(parts):
        px = lax.rem(x + nx - k, nx)
        for s in range(part.shape[0]):
            for t in range(part.shape[2] - 1):
                lanes = slice(t * LANES, (t + 1) * LANES)
                out[:, lax.bitwise_xor(zl, s), px, :, lanes] = part[s, :, 1 + t]


def assembled(place, parts, sizes, after):
    nzh, nzl, nx, _ = sizes
    tiles, rows = parts[0].shape[2:4]
    shape = (nzh, nzl, nx, rows, (tiles - 1) * LANES)
    return pl.pallas_call(
        assemble_kernel,
        out_shape=jax.ShapeDtypeStruct(shape, jnp.bfloat16),
        in_specs=[SMEM] + [VMEM] * len(parts) + [pl.BlockSpec(memory_space=pl.ANY)],
        out_specs=VMEM,
        name="assemble",
        compiler_params=params(8),
        cost_estimate=cost(1_000_000, 4_000_000),
    )(place, *near(*parts), after)


def final_kernel(place, totals, directions, factors, mine, other, ov, oo, *refs):
    copy_v, copy_o, sv, so, nv, no, out_v, out_o, sems = refs
    steps, nzl, nx, nc, rows, _ = factors.shape[1:]
    chunk = D // steps
    cols = directions.shape[2]
    sums = jnp.sum(totals[...], axis=0)
    scale = lax.rsqrt(sums / (D * WIDTH) + 1e-06)
    scales = scale[:1, :1], scale[4:5, :1]
    writes = []
    for k in range(2):
        part = pl.ds(k * steps // 2, steps // 2)
        lanes = pl.ds(k * D // 2, D // 2)
        writes += [
            pltpu.make_async_copy(out_v.at[part], copy_v.at[part], sems.at[2 * k]),
            pltpu.make_async_copy(out_o.at[:, lanes], copy_o.at[:, lanes], sems.at[2 * k + 1]),
        ]

    def copies(pair):
        for i in range(steps):
            for c in range(nc):
                factor = factors[0, i, :, :, c].reshape(chunk // nc, R)
                update = dot(factor, directions[0]) * (0.02 * scales[0])
                w = pair[c][i, :, :, :, :cols].reshape(chunk // nc, cols).astype(jnp.float32)
                out_v[i, :, :, c] = (w - update).astype(jnp.bfloat16).reshape(nzl, nx, rows, cols)
            if (i + 1) * 2 % steps == 0:
                writes[(i + 1) * 4 // steps - 2].start()
            update = dot(factors[1, i].reshape(chunk, R), directions[1]) * (0.02 * scales[1])
            w = jnp.stack([p[i, :, :, :, cols:] for p in pair], axis=2).reshape(chunk, cols)
            half = (w.astype(jnp.float32) - update).astype(jnp.bfloat16)
            out_o[:, i * chunk : (i + 1) * chunk] = half.T
            if (i + 1) * 2 % steps == 0:
                writes[(i + 1) * 4 // steps - 1].start()

    first = place[2] == 0

    @pl.when(first)
    def _():
        copies((mine, other))

    @pl.when(jnp.logical_not(first))
    def _():
        copies((other, mine))

    for f, (w, step, after) in enumerate(((ov, sv, nv), (oo, so, no))):
        own = factors[f, place[5], place[1], place[3], place[2]]
        step[...] = dot(own, directions[f]) * scales[f]
        after[...] = w[...] - 0.02 * step[...]
    for copy in writes:
        copy.wait()


def final(place, totals, directions, factors, mine, other, ov, oo):
    cols = directions.shape[2]
    own = jax.ShapeDtypeStruct(ov.shape, jnp.float32)
    shape = (*factors.shape[1:-1], cols)
    copy_value, *rest = pl.pallas_call(
        final_kernel,
        out_shape=(
            pltpu.HBM(shape, jnp.bfloat16),
            pltpu.HBM((cols, D), jnp.bfloat16),
            own,
            own,
            own,
            own,
        ),
        in_specs=[SMEM] + [VMEM] * 7,
        out_specs=(HBM, HBM, VMEM, VMEM, VMEM, VMEM),
        scratch_shapes=[
            pltpu.VMEM(shape, jnp.bfloat16),
            pltpu.VMEM((cols, D), jnp.bfloat16),
            pltpu.SemaphoreType.DMA((4,)),
        ],
        name="final",
        compiler_params=params(12),
        cost_estimate=cost(4 * D * cols * R, 10_000_000),
    )(place, totals, *near(directions, factors, mine, other), ov, oo)
    return copy_value.reshape(D, cols), *rest


def step(
    normed_input,
    value_cotangent,
    gated_output,
    layer_cotangent,
    factor_value,
    factor_output,
    weight_value,
    weight_output,
    first_value,
    second_value,
    first_output,
    second_output,
):
    sizes = tuple(lax.axis_size(a) for a in FS)
    nzh, _, _, _ = sizes
    ny = lax.axis_size("tp")
    _, cols = weight_value.shape

    at = [lax.axis_index(a) for a in ("tp", "zl", "c", "x", FS, "zh")]
    place = jnp.stack(at).astype(jnp.int32)
    turned_weight = weight_output.T
    w, value_near, output_near = packed(
        nzh,
        place,
        factor_value,
        factor_output,
        weight_value,
        turned_weight,
        value_cotangent,
        gated_output,
    )
    w = exchange(w, "zh")
    f = to_all(w[:, 0], "zl")
    f = to_all(f, ("x", "tp"))
    other = moved(f, "c", 1)

    get = swapped(w, "zl", 1)
    w = jnp.stack([w, get])
    get = swapped(w, "zl", 2)
    w0 = jnp.concatenate([w, get])

    terms, factors = projected_terms(
        place, f, other, normed_input, value_near, layer_cotangent, output_near, sizes
    )
    t = exchange(terms, ("x", "c"))
    t = summed(t)
    t = exchange(t, Z)
    gram = gram_of(factors)

    w1 = moved(w0, "x", 1)
    w3 = moved(w0, "x", 3)

    narrow = (2 * cols // (8 * LANES) * 4, LANES)
    d, *state = moments(
        t, *(s.reshape(narrow) for s in (first_value, second_value, first_output, second_output))
    )
    next_first_value, next_second_value, next_first_output, next_second_output = (
        s.reshape(1, cols) for s in state
    )
    d = exchange(d, Z)

    w2 = moved(w1, "x", 1)
    d = to_all(d, ("x", "c"))
    mine = assembled(place, (w0, w1, w2, w3), sizes, d)
    flip = moved(mine, "c", 1)

    totals, directions = totals_of(ny, d.reshape(R, *d.shape[2:]), gram)
    totals = exchange(totals, "tp")

    copy_value, copy_output, step_value, step_output, next_value, next_output = final(
        place,
        totals,
        directions,
        factors,
        mine,
        flip,
        weight_value,
        turned_weight,
    )
    return (
        step_value,
        step_output.T,
        next_value,
        next_output.T,
        next_first_value,
        next_second_value,
        next_first_output,
        next_second_output,
        copy_value,
        copy_output,
    )


def solution(mesh):
    torus = Mesh(
        mesh.devices.reshape(8, 4, 4, 2, mesh.shape["tp"]), ("zh", "zl", "x", "c", "tp")
    )
    placed = (
        P(FS, None),
        P(FS, "tp"),
        P(FS, "tp"),
        P(FS, None),
        P(FS, None),
        P(FS, None),
        P(FS, "tp"),
        P("tp", FS),
        P(FS, "tp"),
        P(FS, "tp"),
        P(FS, "tp"),
        P(FS, "tp"),
    )
    return jax.shard_map(
        step,
        mesh=torus,
        in_specs=placed,
        out_specs=(
            P(FS, "tp"),
            P("tp", FS),
            P(FS, "tp"),
            P("tp", FS),
            P(FS, "tp"),
            P(FS, "tp"),
            P(FS, "tp"),
            P(FS, "tp"),
            P(None, "tp"),
            P("tp", None),
        ),
        check_vma=False,
    )
```

time: 226 us -> 215 us (0.951)
  Pallas kernels: 30.7 us -> 15.3 us
  blocking collectives: 87.9 us -> 94.6 us
  starting transfers between devices: 53.2 us -> 47.4 us
  waiting for transfers between devices: 48.8 us -> 53.4 us
    pallas_call x4, Pallas kernels: 19.5 us -> 8.18 us  [the longest x1 3.9 us: final(): pl.pallas_call(final_kernel, out_shape=(pltpu.HBM(shape, jnp.bfloat16), p...]
    ppermute x2, waiting for transfers between devices: 7.92 us -> 15.6 us  [swapped(): lax.ppermute(block, axis, [(i, i ^ bit) for i in range(lax.axis_size(axis...]
    all_to_all x3 -> x4, blocking collectives: 87.9 us -> 94.6 us  [exchange(): return lax.all_to_all(blocks, axes, split_axis=0, concat_axis=0, tiled=True)]
    ppermute x8 -> x5, starting transfers between devices: 23.2 us -> 17.3 us  [moved(): return lax.ppermute(block, axis, [(i, (i + by) % n) for i in range(n)])]
    all_to_all x5 -> x4, waiting for transfers between devices: 36.8 us -> 35.5 us  [exchange(): return lax.all_to_all(blocks, axes, split_axis=0, concat_axis=0, tiled=True)]
    all_to_all x5 -> x4, starting transfers between devices: 24.9 us -> 25 us  [exchange(): return lax.all_to_all(blocks, axes, split_axis=0, concat_axis=0, tiled=True)]
  transfers between devices with their start and end apart: 15 -> 11, of which waited for: 7 -> 6; matrix products, arithmetic and copies ran while one was open for 0% -> 1% of each run, Pallas kernels for 9% -> 1%
where the time goes in v3:
time: 215 us; the launch traced here: 214 us
  blocking collectives  94.6 us (44%)
  waiting for transfers between devices  53.4 us (25%)
  starting transfers between devices  47.4 us (22%)
  Pallas kernels  15.3 us (7%)
    all_to_all x4, blocking collectives, exchange(): return lax.all_to_all(blocks, axes, split_axis=0, concat_axis=0, tiled=True)  94.6 us
    all_to_all x4, waiting for transfers between devices, exchange(): return lax.all_to_all(blocks, axes, split_axis=0, concat_axis=0, tiled=True)  35.5 us
    all_to_all x4, starting transfers between devices, exchange(): return lax.all_to_all(blocks, axes, split_axis=0, concat_axis=0, tiled=True)  25 us
    ppermute x5, starting transfers between devices, moved(): return lax.ppermute(block, axis, [(i, (i + by) % n) for i in range(n)])  17.3 us
    ppermute x2, waiting for transfers between devices, swapped(): lax.ppermute(block, axis, [(i, i ^ bit) for i in range(lax.axis_size(axis...  15.6 us
    ppermute x2, starting transfers between devices, swapped(): lax.ppermute(block, axis, [(i, i ^ bit) for i in range(lax.axis_size(axis...  5.19 us
    pallas_call x1, Pallas kernels, projected_terms(): pl.pallas_call(project_kernel, out_shape=(jax.ShapeDtypeStruct((nx * nc,...  4.92 us
  transfers between devices with their start and end apart: 11, of which 6 were waited for; matrix products, arithmetic and copies ran while one was open for 1% of the time, Pallas kernels for 1%

profile of v3, /device:TPU:1, one launch (start us, length us, event | category | flops | bytes accessed | tf_op | source)
XLA Modules:
  0.0 213.9 jit_solution(15134612093465594328)
XLA Ops:
  0.7 1.9 packed.1
  2.7 55.3 %all_to_all.40 = bf16[8,9,8,128]{3,2,1,0:T(8,128)(2,1)S(1)} all-to-all(bf16[8,9,8,128]{3,2,1,0:T(8,128)(2,1)S(1)} %get-tuple-element.28), channel_id=1, replica_groups=mesh['zh'=8,'zl'=4,'x'=4,'c'=2,'tp'=4] {'zh'}, dimensions={0} | all-to-all | bytes 294912 | tf_op jit(solution)/shard_map/all_to_all | solution.py:44
  58.0 11.5 %all_to_all.41 = bf16[4,8,8,128]{3,2,1,0:T(8,128)(2,1)S(1)} all-to-all(bf16[4,8,8,128]{3,2,1,0:T(8,128)(2,1)S(1)} %broadcast_in_dim.9), channel_id=1, replica_groups=mesh['zh'=8,'zl'=4,'x'=4,'c'=2,'tp'=4] {'zl'}, dimensions={0} | all-to-all | bytes 131072 | tf_op jit(solution)/shard_map/all_to_all | solution.py:44
  69.5 0.2 broadcast_in_dim.10
  69.7 21.3 %all_to_all.42.mine = bf16[16,4,8,8,128]{4,3,2,1,0:T(8,128)(2,1)S(1)} all-to-all(bf16[16,4,8,8,128]{4,3,2,1,0:T(8,128)(2,1)S(1)} %broadcast_in_dim.10), channel_id=1, replica_groups=mesh['zh'=8,'zl'=4,'x'=4,'c'=2,'tp'=4] {'x','tp'}, dimensions={0} | all-to-all | bytes 2097152 | tf_op jit(solution)/shard_map/all_to_all | solution.py:44
  91.0 5.2 %collective-permute-start = (bf16[16,4,8,8,128]{4,3,2,1,0:T(8,128)(2,1)S(1)}, bf16[16,4,8,8,128]{4,3,2,1,0:T(8,128)(2,1)S(1)}, u32[]{:S(2)}, u32[]{:S(2)}) collective-permute-start(bf16[16,4,8,8,128]{4,3,2,1,0:T(8,128)(2,1)S(1)} %all_to_all.42.mine), channel_id=1, source_target_pairs={{0,4},{4,0},{1,5},{5,1},{2,6},{6,2},{3,7},{7,3},{8,12},{12,8},{9,1... | collective-permute-start | bytes 3145736 | tf_op jit(solution)/shard_map/ppermute | solution.py:54
  96.2 2.3 %collective-permute-done.other = bf16[16,4,8,8,128]{4,3,2,1,0:T(8,128)(2,1)S(1)} collective-permute-done((bf16[16,4,8,8,128]{4,3,2,1,0:T(8,128)(2,1)S(1)}, bf16[16,4,8,8,128]{4,3,2,1,0:T(8,128)(2,1)S(1)}, u32[]{:S(2)}, u32[]{:S(2)}) %collective-permute-start) | collective-permute-done | bytes 1048608 | tf_op jit(solution)/shard_map/ppermute | solution.py:54
  98.5 4.9 %project.1 = (bf16[8,32,1024]{2,1,0:T(8,128)(2,1)}, bf16[2,8,4,4,2,8,256]{6,5,4,3,2,1,0:T(8,128)(2,1)S(1)}) custom-call(s32[6]{0:T(128)S(1)} %stack.36.place, bf16[16,4,8,8,128]{4,3,2,1,0:T(8,128)(2,1)S(1)} %all_to_all.42.mine, bf16[16,4,8,8,128]{4,3,2,1,0:T(8,128)(2,1)S(1)} %collective-permute-done.other, bf16[512,2048]{1,0:T(8,128)(2,1)S(1)} %copy-done, ...), custom_call_target="tpu_custom_call" | custom-call | flops 1342177280 | bytes 10000000 | tf_op jit(solution)/shard_map/project/pallas_call | solution.py:139
  103.4 3.9 %all-to-all-start.3 = ((bf16[8,32,1024]{2,1,0:T(8,128)(2,1)}), bf16[8,32,1024]{2,1,0:T(8,128)(2,1)S(1)}, u32[]{:S(2)}, u32[]{:S(2)}) async-start(bf16[8,32,1024]{2,1,0:T(8,128)(2,1)} %get-tuple-element.31), calls=%async_computation.3 | async-start | bytes 1048576 | tf_op jit(solution)/shard_map/all_to_all | solution.py:44
  107.3 2.5 %collective-permute-start.1 = (bf16[8,9,8,128]{3,2,1,0:T(8,128)(2,1)S(1)}, bf16[8,9,8,128]{3,2,1,0:T(8,128)(2,1)S(1)}, u32[]{:S(2)}, u32[]{:S(2)}) collective-permute-start(bf16[8,9,8,128]{3,2,1,0:T(8,128)(2,1)S(1)} %all_to_all.40), channel_id=1, source_target_pairs={{0,32},{32,0},{64,96},{96,64},{1,33},{33,1},{65,97},{97,65},{2,34}... | collective-permute-start | bytes 442376 | tf_op jit(solution)/shard_map/ppermute | solution.py:58
  109.9 4.6 %collective-permute-done.1 = bf16[8,9,8,128]{3,2,1,0:T(8,128)(2,1)S(1)} collective-permute-done((bf16[8,9,8,128]{3,2,1,0:T(8,128)(2,1)S(1)}, bf16[8,9,8,128]{3,2,1,0:T(8,128)(2,1)S(1)}, u32[]{:S(2)}, u32[]{:S(2)}) %collective-permute-start.1) | collective-permute-done | bytes 147488 | tf_op jit(solution)/shard_map/ppermute | solution.py:58
  114.5 2.7 %collective-permute-start.2 = (bf16[2,8,9,8,128]{4,3,2,1,0:T(8,128)(2,1)S(1)}, bf16[2,8,9,8,128]{4,3,2,1,0:T(8,128)(2,1)}, u32[]{:S(2)}, u32[]{:S(2)}) collective-permute-start(bf16[2,8,9,8,128]{4,3,2,1,0:T(8,128)(2,1)S(1)} %pad_maximum_fusion.1), channel_id=1, source_target_pairs={{0,64},{32,96},{64,0},{96,32},{1,65},{33,97},{65,1},{97,33},{2,66}... | collective-permute-start | bytes 884744 | tf_op jit(solution)/shard_map/ppermute | solution.py:58
  117.2 0.7 summed.1
  118.0 5.1 %all-to-all-start.4 = ((bf16[32,8,128]{2,1,0:T(8,128)(2,1)}), bf16[32,8,128]{2,1,0:T(8,128)(2,1)S(1)}, u32[]{:S(2)}, u32[]{:S(2)}) async-start(bf16[32,8,128]{2,1,0:T(8,128)(2,1)} %summed.1), calls=%async_computation.4 | async-start | bytes 131072 | tf_op jit(solution)/shard_map/all_to_all | solution.py:44
  123.1 11.0 %collective-permute-done.2 = bf16[2,8,9,8,128]{4,3,2,1,0:T(8,128)(2,1)} collective-permute-done((bf16[2,8,9,8,128]{4,3,2,1,0:T(8,128)(2,1)S(1)}, bf16[2,8,9,8,128]{4,3,2,1,0:T(8,128)(2,1)}, u32[]{:S(2)}, u32[]{:S(2)}) %collective-permute-start.2) | collective-permute-done | bytes 294944 | tf_op jit(solution)/shard_map/ppermute | solution.py:58
  134.1 1.0 pad_maximum_fusion.refs_0_
  135.1 3.0 %collective-permute-start.3 = (bf16[4,8,9,8,128]{4,3,2,1,0:T(8,128)(2,1)S(1)}, bf16[4,8,9,8,128]{4,3,2,1,0:T(8,128)(2,1)}, u32[]{:S(2)}, u32[]{:S(2)}) collective-permute-start(bf16[4,8,9,8,128]{4,3,2,1,0:T(8,128)(2,1)S(1)} %pad_maximum_fusion.refs_0_), channel_id=1, source_target_pairs={{0,8},{8,16},{16,24},{24,0},{1,9},{9,17},{17,25},{25,1},{2,10},{10... | collective-permute-start | bytes 1769480 | tf_op jit(solution)/shard_map/ppermute | solution.py:54
  138.1 9.0 %all-to-all-done.4.t = bf16[32,8,128]{2,1,0:T(8,128)(2,1)S(1)} async-done(((bf16[32,8,128]{2,1,0:T(8,128)(2,1)}), bf16[32,8,128]{2,1,0:T(8,128)(2,1)S(1)}, u32[]{:S(2)}, u32[]{:S(2)}) %all-to-all-start.4) | async-done | bytes 65568 | tf_op jit(solution)/shard_map/all_to_all | solution.py:44
  147.2 0.7 moments.1
  147.8 6.7 %all-to-all-start.5 = ((bf16[32,8,128]{2,1,0:T(8,128)(2,1)}), bf16[32,8,128]{2,1,0:T(8,128)(2,1)S(1)}, u32[]{:S(2)}, u32[]{:S(2)}) async-start(bf16[32,8,128]{2,1,0:T(8,128)(2,1)} %get-tuple-element.32), calls=%async_computation.5 | async-start | bytes 131072 | tf_op jit(solution)/shard_map/all_to_all | solution.py:44
  154.6 4.2 %collective-permute-start.5 = (bf16[4,8,9,8,128]{4,3,2,1,0:T(8,128)(2,1)S(1)}, bf16[4,8,9,8,128]{4,3,2,1,0:T(8,128)(2,1)}, u32[]{:S(2)}, u32[]{:S(2)}) collective-permute-start(bf16[4,8,9,8,128]{4,3,2,1,0:T(8,128)(2,1)S(1)} %pad_maximum_fusion.refs_0_), channel_id=1, source_target_pairs={{0,24},{8,0},{16,8},{24,16},{1,25},{9,1},{17,9},{25,17},{2,26},{10... | collective-permute-start | bytes 1769480 | tf_op jit(solution)/shard_map/ppermute | solution.py:54
  158.8 1.9 collective-permute-start.4
  160.7 17.2 %all-to-all-done.5 = bf16[32,8,128]{2,1,0:T(8,128)(2,1)S(1)} async-done(((bf16[32,8,128]{2,1,0:T(8,128)(2,1)}), bf16[32,8,128]{2,1,0:T(8,128)(2,1)S(1)}, u32[]{:S(2)}, u32[]{:S(2)}) %all-to-all-start.5) | async-done | bytes 65568 | tf_op jit(solution)/shard_map/all_to_all | solution.py:44
  177.9 0.9 broadcast_in_dim.22
  178.8 9.2 %all-to-all-start.6 = ((bf16[8,32,8,128]{3,2,1,0:T(8,128)(2,1)}), bf16[8,32,8,128]{3,2,1,0:T(8,128)(2,1)S(1)}, u32[]{:S(2)}, u32[]{:S(2)}) async-start(bf16[8,32,8,128]{3,2,1,0:T(8,128)(2,1)} %broadcast_in_dim.22), calls=%async_computation.6 | async-start | bytes 1048576 | tf_op jit(solution)/shard_map/all_to_all | solution.py:44
  188.0 9.3 %all-to-all-done.6.refs_4_ = bf16[8,32,8,128]{3,2,1,0:T(8,128)(2,1)S(1)} async-done(((bf16[8,32,8,128]{3,2,1,0:T(8,128)(2,1)}), bf16[8,32,8,128]{3,2,1,0:T(8,128)(2,1)S(1)}, u32[]{:S(2)}, u32[]{:S(2)}) %all-to-all-start.6) | async-done | bytes 524320 | tf_op jit(solution)/shard_map/all_to_all | solution.py:44
  197.4 1.6 assemble.1.mine
  199.0 2.9 %collective-permute-start.6 = (bf16[8,4,4,8,1024]{4,3,2,1,0:T(8,128)(2,1)S(1)}, bf16[8,4,4,8,1024]{4,3,2,1,0:T(8,128)(2,1)S(1)}, u32[]{:S(2)}, u32[]{:S(2)}) collective-permute-start(bf16[8,4,4,8,1024]{4,3,2,1,0:T(8,128)(2,1)S(1)} %assemble.1.mine), channel_id=1, source_target_pairs={{0,4},{4,0},{1,5},{5,1},{2,6},{6,2},{3,7},{7,3},{8,12},{12,8},{9,1... | collective-permute-start | bytes 6291464 | tf_op jit(solution)/shard_map/ppermute | solution.py:54
  201.8 0.8 gram.1
  202.6 0.8 totals.1
  203.4 6.6 %all_to_all.43.totals = f32[4,8,128]{2,1,0:T(8,128)S(1)} all-to-all(f32[4,8,128]{2,1,0:T(8,128)S(1)} %get-tuple-element.34), channel_id=1, replica_groups=mesh['zh'=8,'zl'=4,'x'=4,'c'=2,'tp'=4] {'tp'}, dimensions={0} | all-to-all | bytes 32768 | tf_op jit(solution)/shard_map/all_to_all | solution.py:44
  210.0 3.9 %final.1 = (bf16[8,4,4,2,8,512]{5,4,3,2,1,0:T(8,128)(2,1)}, bf16[512,2048]{1,0:T(8,128)(2,1)}, f32[8,512]{1,0:T(8,128)}, f32[8,512]{1,0:T(8,128)}, f32[8,512]{1,0:T(8,128)}, /*index=5*/f32[8,512]{1,0:T(8,128)}) custom-call(s32[6]{0:T(128)S(1)} %stack.36.place, f32[4,8,128]{2,1,0:T(8,128)S(1)} %all_to_all.43.totals, ...), custom_call_target="tpu_custom_call" | custom-call | flops 1073741824 | bytes 10000000 | tf_op jit(solution)/shard_map/final/pallas_call | solution.py:343
  (25 shorter events, 0.2 us)
Async XLA Ops:
  0.7 97.8 %copy-start.1 = (bf16[512,2048]{1,0:T(8,128)(2,1)S(1)}, bf16[512,2048]{1,0:T(8,128)(2,1)}, u32[]{:S(2)}) copy-start(bf16[512,2048]{1,0:T(8,128)(2,1)} %xo.1) | copy-start | bytes 6291460
  2.7 95.8 %copy-start = (bf16[512,2048]{1,0:T(8,128)(2,1)S(1)}, bf16[512,2048]{1,0:T(8,128)(2,1)}, u32[]{:S(2)}) copy-start(bf16[512,2048]{1,0:T(8,128)(2,1)} %xv.1) | copy-start | bytes 6291460
  91.0 7.5 %collective-permute-start = (bf16[16,4,8,8,128]{4,3,2,1,0:T(8,128)(2,1)S(1)}, bf16[16,4,8,8,128]{4,3,2,1,0:T(8,128)(2,1)S(1)}, u32[]{:S(2)}, u32[]{:S(2)}) collective-permute-start(bf16[16,4,8,8,128]{4,3,2,1,0:T(8,128)(2,1)S(1)} %all_to_all.42.mine), channel_id=1, source_target_pairs={{0,4},{4,0},{1,5},{5,1},{2,6},{6,2},{3,7},{7,3},{8,12},{12,8},{9,1... | collective-permute-start | bytes 3145736 | tf_op jit(solution)/shard_map/ppermute | solution.py:54
  103.4 43.7 %copy-start.4 = (f32[1,512]{1,0:T(1,128)S(1)}, f32[1,512]{1,0:T(1,128)}, u32[]{:S(2)}) copy-start(f32[1,512]{1,0:T(1,128)} %param.20) | copy-start | bytes 6148
  103.4 43.7 %copy-start.5 = (f32[1,512]{1,0:T(1,128)S(1)}, f32[1,512]{1,0:T(1,128)}, u32[]{:S(2)}) copy-start(f32[1,512]{1,0:T(1,128)} %param.21) | copy-start | bytes 6148
  103.4 43.7 %copy-start.6 = (f32[1,512]{1,0:T(1,128)S(1)}, f32[1,512]{1,0:T(1,128)}, u32[]{:S(2)}) copy-start(f32[1,512]{1,0:T(1,128)} %param.22) | copy-start | bytes 6148
  103.4 43.7 %copy-start.7 = (f32[1,512]{1,0:T(1,128)S(1)}, f32[1,512]{1,0:T(1,128)}, u32[]{:S(2)}) copy-start(f32[1,512]{1,0:T(1,128)} %param.23) | copy-start | bytes 6148
  103.4 13.8 %all-to-all-start.3 = ((bf16[8,32,1024]{2,1,0:T(8,128)(2,1)}), bf16[8,32,1024]{2,1,0:T(8,128)(2,1)S(1)}, u32[]{:S(2)}, u32[]{:S(2)}) async-start(bf16[8,32,1024]{2,1,0:T(8,128)(2,1)} %get-tuple-element.31), calls=%async_computation.3 | async-start | bytes 1048576 | tf_op jit(solution)/shard_map/all_to_all | solution.py:44
  107.3 7.2 %collective-permute-start.1 = (bf16[8,9,8,128]{3,2,1,0:T(8,128)(2,1)S(1)}, bf16[8,9,8,128]{3,2,1,0:T(8,128)(2,1)S(1)}, u32[]{:S(2)}, u32[]{:S(2)}) collective-permute-start(bf16[8,9,8,128]{3,2,1,0:T(8,128)(2,1)S(1)} %all_to_all.40), channel_id=1, source_target_pairs={{0,32},{32,0},{64,96},{96,64},{1,33},{33,1},{65,97},{97,65},{2,34}... | collective-permute-start | bytes 442376 | tf_op jit(solution)/shard_map/ppermute | solution.py:58
  114.5 19.5 %collective-permute-start.2 = (bf16[2,8,9,8,128]{4,3,2,1,0:T(8,128)(2,1)S(1)}, bf16[2,8,9,8,128]{4,3,2,1,0:T(8,128)(2,1)}, u32[]{:S(2)}, u32[]{:S(2)}) collective-permute-start(bf16[2,8,9,8,128]{4,3,2,1,0:T(8,128)(2,1)S(1)} %pad_maximum_fusion.1), channel_id=1, source_target_pairs={{0,64},{32,96},{64,0},{96,32},{1,65},{33,97},{65,1},{97,33},{2,66}... | collective-permute-start | bytes 884744 | tf_op jit(solution)/shard_map/ppermute | solution.py:58
  118.0 29.2 %all-to-all-start.4 = ((bf16[32,8,128]{2,1,0:T(8,128)(2,1)}), bf16[32,8,128]{2,1,0:T(8,128)(2,1)S(1)}, u32[]{:S(2)}, u32[]{:S(2)}) async-start(bf16[32,8,128]{2,1,0:T(8,128)(2,1)} %summed.1), calls=%async_computation.4 | async-start | bytes 131072 | tf_op jit(solution)/shard_map/all_to_all | solution.py:44
  135.1 23.7 %collective-permute-start.3 = (bf16[4,8,9,8,128]{4,3,2,1,0:T(8,128)(2,1)S(1)}, bf16[4,8,9,8,128]{4,3,2,1,0:T(8,128)(2,1)}, u32[]{:S(2)}, u32[]{:S(2)}) collective-permute-start(bf16[4,8,9,8,128]{4,3,2,1,0:T(8,128)(2,1)S(1)} %pad_maximum_fusion.refs_0_), channel_id=1, source_target_pairs={{0,8},{8,16},{16,24},{24,0},{1,9},{9,17},{17,25},{25,1},{2,10},{10... | collective-permute-start | bytes 1769480 | tf_op jit(solution)/shard_map/ppermute | solution.py:54
  147.8 30.1 %all-to-all-start.5 = ((bf16[32,8,128]{2,1,0:T(8,128)(2,1)}), bf16[32,8,128]{2,1,0:T(8,128)(2,1)S(1)}, u32[]{:S(2)}, u32[]{:S(2)}) async-start(bf16[32,8,128]{2,1,0:T(8,128)(2,1)} %get-tuple-element.32), calls=%async_computation.5 | async-start | bytes 131072 | tf_op jit(solution)/shard_map/all_to_all | solution.py:44
  154.6 33.5 %collective-permute-start.5 = (bf16[4,8,9,8,128]{4,3,2,1,0:T(8,128)(2,1)S(1)}, bf16[4,8,9,8,128]{4,3,2,1,0:T(8,128)(2,1)}, u32[]{:S(2)}, u32[]{:S(2)}) collective-permute-start(bf16[4,8,9,8,128]{4,3,2,1,0:T(8,128)(2,1)S(1)} %pad_maximum_fusion.refs_0_), channel_id=1, source_target_pairs={{0,24},{8,0},{16,8},{24,16},{1,25},{9,1},{17,9},{25,17},{2,26},{10... | collective-permute-start | bytes 1769480 | tf_op jit(solution)/shard_map/ppermute | solution.py:54
  158.8 29.2 %collective-permute-start.4 = (bf16[4,8,9,8,128]{4,3,2,1,0:T(8,128)(2,1)}, bf16[4,8,9,8,128]{4,3,2,1,0:T(8,128)(2,1)}, u32[]{:S(2)}, u32[]{:S(2)}) collective-permute-start(bf16[4,8,9,8,128]{4,3,2,1,0:T(8,128)(2,1)} %collective-permute-done.3.refs_1_), channel_id=1, source_target_pairs={{0,8},{8,16},{16,24},{24,0},{1,9},{9,17},{17,25},{25,1},{2,10},{10... | collective-permute-start | bytes 1769480 | tf_op jit(solution)/shard_map/ppermute | solution.py:54
  178.8 18.6 %all-to-all-start.6 = ((bf16[8,32,8,128]{3,2,1,0:T(8,128)(2,1)}), bf16[8,32,8,128]{3,2,1,0:T(8,128)(2,1)S(1)}, u32[]{:S(2)}, u32[]{:S(2)}) async-start(bf16[8,32,8,128]{3,2,1,0:T(8,128)(2,1)} %broadcast_in_dim.22), calls=%async_computation.6 | async-start | bytes 1048576 | tf_op jit(solution)/shard_map/all_to_all | solution.py:44
  198.9 11.0 %copy-start.2 = (f32[8,512]{1,0:T(8,128)S(1)}, f32[8,512]{1,0:T(8,128)}, u32[]{:S(2)}) copy-start(f32[8,512]{1,0:T(8,128)} %ov.1) | copy-start | bytes 49156
  198.9 11.0 %copy-start.3 = (f32[512,8]{0,1:T(8,128)S(1)}, f32[512,8]{0,1:T(8,128)}, u32[]{:S(2)}) copy-start(f32[512,8]{0,1:T(8,128)} %param.19) | copy-start | bytes 49156
  199.0 11.0 %collective-permute-start.6 = (bf16[8,4,4,8,1024]{4,3,2,1,0:T(8,128)(2,1)S(1)}, bf16[8,4,4,8,1024]{4,3,2,1,0:T(8,128)(2,1)S(1)}, u32[]{:S(2)}, u32[]{:S(2)}) collective-permute-start(bf16[8,4,4,8,1024]{4,3,2,1,0:T(8,128)(2,1)S(1)} %assemble.1.mine), channel_id=1, source_target_pairs={{0,4},{4,0},{1,5},{5,1},{2,6},{6,2},{3,7},{7,3},{8,12},{12,8},{9,1... | collective-permute-start | bytes 6291464 | tf_op jit(solution)/shard_map/ppermute | solution.py:54

commit v4 on v3

--- a/solution.py
+++ b/solution.py
@@ -9,8 +9,8 @@
 D = 2048
 WIDTH = 2048
 R = 256
-FS = ("zh", "zl", "x", "c")
-Z = ("zh", "zl")
+FS = ("z", "x", "c")
+NZL = 4
 LANES = 128
 TN = (((0,), (0,)), ((), ()))
 
@@ -40,13 +40,29 @@
     return lax.dot_general(a, b, dims, preferred_element_type=jnp.float32)
 
 
-def exchange(blocks, axes):
-    return lax.all_to_all(blocks, axes, split_axis=0, concat_axis=0, tiled=True)
-
-
-def to_all(block, axes):
-    copies = jnp.broadcast_to(block[None], (lax.axis_size(axes), *block.shape))
-    return exchange(copies, axes)
+def turned(n, by):
+    return [(i + by) % n for i in range(n)]
+
+
+def near_z(nz):
+    return [[i + k for k in (1, 0, 2, 3)] for i in range(0, nz, NZL)]
+
+
+def far_z(nz):
+    n = nz // NZL
+    return [[i + NZL * k for k in turned(n, n // 2)] for i in range(NZL)]
+
+
+def exchange(blocks, axes, groups=None):
+    return lax.all_to_all(
+        blocks, axes, split_axis=0, concat_axis=0, axis_index_groups=groups, tiled=True
+    )
+
+
+def to_all(block, axes, groups=None):
+    count = len(groups[0]) if groups else lax.axis_size(axes)
+    copies = jnp.broadcast_to(block[None], (count, *block.shape))
+    return exchange(copies, axes, groups)
 
 
 def moved(block, axis, by):
@@ -71,7 +87,7 @@
     y = place[0]
     j = lax.broadcasted_iota(jnp.int32, (R, R), 0)
     k = lax.broadcasted_iota(jnp.int32, (R, R), 1)
-    turn = (j == (k % n) * 8 + k // n).astype(jnp.bfloat16)
+    turn = (j == (k % n + n // 2) % n * 8 + k // n).astype(jnp.bfloat16)
     for copy in copies[:4]:
         copy.wait()
     factor = jnp.where(y < 2, fv_in[...].astype(jnp.float32), fo_in[...].astype(jnp.float32))
@@ -114,17 +130,19 @@
 
 def project_kernel(place, mine, other, xv, vv, xo, vo, out, whole):
     c = place[2]
-    nzl, nx = whole.shape[2:4]
+    nzh, nzl, nx = whole.shape[1:4]
+    first = nzh // 2
     half = R // LANES
     cols = vv.shape[1]
     for f in range(2):
         for src, at in ((mine, c), (other, 1 - c)):
             for x in range(nx):
                 for h in range(half):
-                    for zl in range(nzl):
-                        whole[f, :, zl, x, at, :, h * LANES : (h + 1) * LANES] = src[
-                            x * 2 * half + f * half + h, zl
-                        ]
+                    for k, zl in enumerate(near_z(nzl)[0]):
+                        lanes = slice(h * LANES, (h + 1) * LANES)
+                        block = src.at[x * 2 * half + f * half + h, k]
+                        whole[f, first:, zl, x, at, :, lanes] = block[: nzh - first]
+                        whole[f, :first, zl, x, at, :, lanes] = block[nzh - first :]
     for f, (x, v) in enumerate(((xv, vv), (xo, vo))):
         projected = dot(x[...], whole[f].reshape(D, R)).astype(jnp.bfloat16)
         term = dot(projected, v[...], TN).astype(jnp.bfloat16)
@@ -259,15 +277,18 @@
 
 
 def assemble_kernel(place, *refs):
-    parts, out = refs[:-2], refs[-1]
+    (*whole, _, out) = refs
     zl, x = place[1], place[3]
-    nx = len(parts)
-    for k, part in enumerate(parts):
+    nzh, nzl, nx = out.shape[:3]
+    first = nzh // 2
+    parts = [(k, s, part.at[s]) for k, part in enumerate(whole) for s in range(nzl)]
+    for k, s, part in parts:
         px = lax.rem(x + nx - k, nx)
-        for s in range(part.shape[0]):
-            for t in range(part.shape[2] - 1):
-                lanes = slice(t * LANES, (t + 1) * LANES)
-                out[:, lax.bitwise_xor(zl, s), px, :, lanes] = part[s, :, 1 + t]
+        at = lax.bitwise_xor(zl, s)
+        for t in range(part.shape[1] - 1):
+            lanes = slice(t * LANES, (t + 1) * LANES)
+            out[first:, at, px, :, lanes] = part[: nzh - first, 1 + t]
+            out[:first, at, px, :, lanes] = part[nzh - first :, 1 + t]
 
 
 def assembled(place, parts, sizes, after):
@@ -286,7 +307,7 @@
 
 
 def final_kernel(place, totals, directions, factors, mine, other, ov, oo, *refs):
-    copy_v, copy_o, sv, so, nv, no, out_v, out_o, sems = refs
+    copy_v, copy_o, sv, so, nv, no, out_v, out_o, own, sems = refs
     steps, nzl, nx, nc, rows, _ = factors.shape[1:]
     chunk = D // steps
     cols = directions.shape[2]
@@ -301,6 +322,19 @@
             pltpu.make_async_copy(out_v.at[part], copy_v.at[part], sems.at[2 * k]),
             pltpu.make_async_copy(out_o.at[:, lanes], copy_o.at[:, lanes], sems.at[2 * k + 1]),
         ]
+
+    small = []
+    for f, (w, targets) in enumerate(((ov, (sv, nv)), (oo, (so, no)))):
+        mine_f = factors[f, place[4], place[1], place[3], place[2]]
+        step = dot(mine_f, directions[f]) * scales[f]
+        own[2 * f] = step
+        own[2 * f + 1] = w[...] - 0.02 * step
+        small += [
+            pltpu.make_async_copy(own.at[2 * f + k], target, sems.at[4 + 2 * f + k])
+            for k, target in enumerate(targets)
+        ]
+    for copy in small:
+        copy.start()
 
     def copies(pair):
         for i in range(steps):
@@ -328,17 +362,13 @@
     def _():
         copies((other, mine))
 
-    for f, (w, step, after) in enumerate(((ov, sv, nv), (oo, so, no))):
-        own = factors[f, place[5], place[1], place[3], place[2]]
-        step[...] = dot(own, directions[f]) * scales[f]
-        after[...] = w[...] - 0.02 * step[...]
-    for copy in writes:
+    for copy in small + writes:
         copy.wait()
 
 
 def final(place, totals, directions, factors, mine, other, ov, oo):
     cols = directions.shape[2]
-    own = jax.ShapeDtypeStruct(ov.shape, jnp.float32)
+    own = pltpu.HBM(ov.shape, jnp.float32)
     shape = (*factors.shape[1:-1], cols)
     copy_value, *rest = pl.pallas_call(
         final_kernel,
@@ -351,11 +381,12 @@
             own,
         ),
         in_specs=[SMEM] + [VMEM] * 7,
-        out_specs=(HBM, HBM, VMEM, VMEM, VMEM, VMEM),
+        out_specs=(HBM,) * 6,
         scratch_shapes=[
             pltpu.VMEM(shape, jnp.bfloat16),
             pltpu.VMEM((cols, D), jnp.bfloat16),
-            pltpu.SemaphoreType.DMA((4,)),
+            pltpu.VMEM((4, *ov.shape), jnp.float32),
+            pltpu.SemaphoreType.DMA((8,)),
         ],
         name="final",
         compiler_params=params(12),
@@ -378,12 +409,15 @@
     first_output,
     second_output,
 ):
-    sizes = tuple(lax.axis_size(a) for a in FS)
-    nzh, _, _, _ = sizes
+    nz, nx, nc = (lax.axis_size(a) for a in FS)
+    nzh, nzl = nz // NZL, NZL
+    sizes = nzh, nzl, nx, nc
     ny = lax.axis_size("tp")
+    around = [turned(nz, nz // 2)]
     _, cols = weight_value.shape
 
-    at = [lax.axis_index(a) for a in ("tp", "zl", "c", "x", FS, "zh")]
+    z = lax.axis_index("z")
+    at = [lax.axis_index("tp"), z % nzl, lax.axis_index("c"), lax.axis_index("x"), z // nzl]
     place = jnp.stack(at).astype(jnp.int32)
     turned_weight = weight_output.T
     w, value_near, output_near = packed(
@@ -396,14 +430,14 @@
         value_cotangent,
         gated_output,
     )
-    w = exchange(w, "zh")
-    f = to_all(w[:, 0], "zl")
+    w = exchange(w, "z", far_z(nz))
+    f = to_all(w[:, 0], "z", near_z(nz))
     f = to_all(f, ("x", "tp"))
     other = moved(f, "c", 1)
 
-    get = swapped(w, "zl", 1)
+    get = swapped(w, "z", 1)
     w = jnp.stack([w, get])
-    get = swapped(w, "zl", 2)
+    get = swapped(w, "z", 2)
     w0 = jnp.concatenate([w, get])
 
     terms, factors = projected_terms(
@@ -411,20 +445,21 @@
     )
     t = exchange(terms, ("x", "c"))
     t = summed(t)
-    t = exchange(t, Z)
+    t = exchange(t, "z", around)
     gram = gram_of(factors)
 
     w1 = moved(w0, "x", 1)
-    w3 = moved(w0, "x", 3)
-
-    narrow = (2 * cols // (8 * LANES) * 4, LANES)
+    w3 = moved(w0, "x", nx - 1)
+
+    narrow = (cols // LANES, LANES)
     d, *state = moments(
-        t, *(s.reshape(narrow) for s in (first_value, second_value, first_output, second_output))
+        t,
+        *(s.reshape(narrow) for s in (first_value, second_value, first_output, second_output)),
     )
     next_first_value, next_second_value, next_first_output, next_second_output = (
         s.reshape(1, cols) for s in state
     )
-    d = exchange(d, Z)
+    d = exchange(d, "z", around)
 
     w2 = moved(w1, "x", 1)
     d = to_all(d, ("x", "c"))
@@ -459,9 +494,7 @@
 
 
 def solution(mesh):
-    torus = Mesh(
-        mesh.devices.reshape(8, 4, 4, 2, mesh.shape["tp"]), ("zh", "zl", "x", "c", "tp")
-    )
+    torus = Mesh(mesh.devices.reshape(32, 4, 2, mesh.shape["tp"]), ("z", "x", "c", "tp"))
     placed = (
         P(FS, None),
         P(FS, "tp"),

time: 215 us -> 207 us (0.963)
  starting transfers between devices: 47.4 us -> 74.4 us
  waiting for transfers between devices: 53.4 us -> 29.7 us
  blocking collectives: 94.6 us -> 83.8 us
    all_to_all x4, starting transfers between devices: 25 us -> 53.1 us  [exchange(): lax.all_to_all(blocks, axes, split_axis=0, concat_axis=0, axis_index_grou...]
    all_to_all x4, waiting for transfers between devices: 35.5 us -> 14.2 us  [exchange(): lax.all_to_all(blocks, axes, split_axis=0, concat_axis=0, axis_index_grou...]
    all_to_all x4, blocking collectives: 94.6 us -> 83.8 us  [exchange(): lax.all_to_all(blocks, axes, split_axis=0, concat_axis=0, axis_index_grou...]
    ppermute x2, waiting for transfers between devices: 15.6 us -> 5.26 us  [swapped(): lax.ppermute(block, axis, [(i, i ^ bit) for i in range(lax.axis_size(axis...]
    ppermute x5, waiting for transfers between devices: 2.28 us -> 10.2 us  [moved(): return lax.ppermute(block, axis, [(i, (i + by) % n) for i in range(n)])]
  transfers between devices with their start and end apart: 11 -> 11, of which waited for: 6 -> 7; matrix products, arithmetic and copies ran while one was open for 1% -> 1% of each run, Pallas kernels for 1% -> 1%
where the time goes in v4:
time: 207 us; the launch traced here: 206 us
  blocking collectives  83.8 us (40%)
  starting transfers between devices  74.4 us (36%)
  waiting for transfers between devices  29.7 us (14%)
  Pallas kernels  15 us (7%)
    all_to_all x4, blocking collectives, exchange(): lax.all_to_all(blocks, axes, split_axis=0, concat_axis=0, axis_index_grou...  83.8 us
    all_to_all x4, starting transfers between devices, exchange(): lax.all_to_all(blocks, axes, split_axis=0, concat_axis=0, axis_index_grou...  53.1 us
    ppermute x5, starting transfers between devices, moved(): return lax.ppermute(block, axis, [(i, (i + by) % n) for i in range(n)])  17.2 us
    all_to_all x4, waiting for transfers between devices, exchange(): lax.all_to_all(blocks, axes, split_axis=0, concat_axis=0, axis_index_grou...  14.2 us
    ppermute x5, waiting for transfers between devices, moved(): return lax.ppermute(block, axis, [(i, (i + by) % n) for i in range(n)])  10.2 us
    ppermute x2, waiting for transfers between devices, swapped(): lax.ppermute(block, axis, [(i, i ^ bit) for i in range(lax.axis_size(axis...  5.26 us
    pallas_call x1, Pallas kernels, projected_terms(): pl.pallas_call(project_kernel, out_shape=(jax.ShapeDtypeStruct((nx * nc,...  4.94 us
  transfers between devices with their start and end apart: 11, of which 7 were waited for; matrix products, arithmetic and copies ran while one was open for 1% of the time, Pallas kernels for 1%

profile of v4, /device:TPU:1, one launch (start us, length us, event | category | flops | bytes accessed | tf_op | source)
XLA Modules:
  0.0 206.1 jit_solution(15297979545415385346)
XLA Ops:
  0.8 1.9 packed.1
  2.7 47.9 %all_to_all.40 = bf16[8,9,8,128]{3,2,1,0:T(8,128)(2,1)S(1)} all-to-all(bf16[8,9,8,128]{3,2,1,0:T(8,128)(2,1)S(1)} %get-tuple-element.28), channel_id=1, replica_groups={{512,640,768,896,0,128,256,384},{544,672,800,928,32,160,288,416},{576,7..., dimensions={0} | all-to-all | bytes 294912 | tf_op jit(solution)/shard_map/all_to_all | solution.py:57
  50.6 7.8 %all_to_all.41 = bf16[4,8,8,128]{3,2,1,0:T(8,128)(2,1)S(1)} all-to-all(bf16[4,8,8,128]{3,2,1,0:T(8,128)(2,1)S(1)} %broadcast_in_dim.9), channel_id=1, replica_groups={{32,0,64,96},{160,128,192,224},{288,256,320,352},{416,384,448,480},{544..., dimensions={0} | all-to-all | bytes 131072 | tf_op jit(solution)/shard_map/all_to_all | solution.py:57
  58.4 0.2 broadcast_in_dim.10
  58.7 21.6 %all_to_all.42.mine = bf16[16,4,8,8,128]{4,3,2,1,0:T(8,128)(2,1)S(1)} all-to-all(bf16[16,4,8,8,128]{4,3,2,1,0:T(8,128)(2,1)S(1)} %broadcast_in_dim.10), channel_id=1, replica_groups=mesh['z'=32,'x'=4,'c'=2,'tp'=4] {'x','tp'}, dimensions={0} | all-to-all | bytes 2097152 | tf_op jit(solution)/shard_map/all_to_all | solution.py:57
  80.3 4.9 %collective-permute-start = (bf16[16,4,8,8,128]{4,3,2,1,0:T(8,128)(2,1)S(1)}, bf16[16,4,8,8,128]{4,3,2,1,0:T(8,128)(2,1)S(1)}, u32[]{:S(2)}, u32[]{:S(2)}) collective-permute-start(bf16[16,4,8,8,128]{4,3,2,1,0:T(8,128)(2,1)S(1)} %all_to_all.42.mine), channel_id=1, source_target_pairs={{0,4},{4,0},{1,5},{5,1},{2,6},{6,2},{3,7},{7,3},{8,12},{12,8},{9,1... | collective-permute-start | bytes 3145736 | tf_op jit(solution)/shard_map/ppermute | solution.py:70
  85.2 2.3 %collective-permute-done.other = bf16[16,4,8,8,128]{4,3,2,1,0:T(8,128)(2,1)S(1)} collective-permute-done((bf16[16,4,8,8,128]{4,3,2,1,0:T(8,128)(2,1)S(1)}, bf16[16,4,8,8,128]{4,3,2,1,0:T(8,128)(2,1)S(1)}, u32[]{:S(2)}, u32[]{:S(2)}) %collective-permute-start) | collective-permute-done | bytes 1048608 | tf_op jit(solution)/shard_map/ppermute | solution.py:70
  87.5 4.9 %project.1 = (bf16[8,32,1024]{2,1,0:T(8,128)(2,1)}, bf16[2,8,4,4,2,8,256]{6,5,4,3,2,1,0:T(8,128)(2,1)S(1)}) custom-call(s32[5]{0:T(128)S(1)} %stack.32.place, bf16[16,4,8,8,128]{4,3,2,1,0:T(8,128)(2,1)S(1)} %all_to_all.42.mine, bf16[16,4,8,8,128]{4,3,2,1,0:T(8,128)(2,1)S(1)} %collective-permute-done.other, bf16[512,2048]{1,0:T(8,128)(2,1)S(1)} %copy-done, ...), custom_call_target="tpu_custom_call" | custom-call | flops 1342177280 | bytes 10000000 | tf_op jit(solution)/shard_map/project/pallas_call | solution.py:157
  92.4 3.9 %all-to-all-start.3 = ((bf16[8,32,1024]{2,1,0:T(8,128)(2,1)}), bf16[8,32,1024]{2,1,0:T(8,128)(2,1)S(1)}, u32[]{:S(2)}, u32[]{:S(2)}) async-start(bf16[8,32,1024]{2,1,0:T(8,128)(2,1)} %get-tuple-element.31), calls=%async_computation.3 | async-start | bytes 1048576 | tf_op jit(solution)/shard_map/all_to_all | solution.py:57
  96.3 1.9 collective-permute-start.1
  98.2 5.3 %collective-permute-done.1 = bf16[8,9,8,128]{3,2,1,0:T(8,128)(2,1)S(1)} collective-permute-done((bf16[8,9,8,128]{3,2,1,0:T(8,128)(2,1)S(1)}, bf16[8,9,8,128]{3,2,1,0:T(8,128)(2,1)S(1)}, u32[]{:S(2)}, u32[]{:S(2)}) %collective-permute-start.1) | collective-permute-done | bytes 147488 | tf_op jit(solution)/shard_map/ppermute | solution.py:74
  103.5 2.2 %collective-permute-start.2 = (bf16[2,8,9,8,128]{4,3,2,1,0:T(8,128)(2,1)S(1)}, bf16[2,8,9,8,128]{4,3,2,1,0:T(8,128)(2,1)}, u32[]{:S(2)}, u32[]{:S(2)}) collective-permute-start(bf16[2,8,9,8,128]{4,3,2,1,0:T(8,128)(2,1)S(1)} %pad_maximum_fusion.1), channel_id=1, source_target_pairs={{0,64},{32,96},{64,0},{96,32},{128,192},{160,224},{192,128},{224,1... | collective-permute-start | bytes 884744 | tf_op jit(solution)/shard_map/ppermute | solution.py:74
  105.7 0.7 summed.1
  106.4 21.3 %all-to-all-start.4 = ((bf16[32,8,128]{2,1,0:T(8,128)(2,1)}), bf16[32,8,128]{2,1,0:T(8,128)(2,1)S(1)}, u32[]{:S(2)}, u32[]{:S(2)}) async-start(bf16[32,8,128]{2,1,0:T(8,128)(2,1)} %summed.1), calls=%async_computation.4 | async-start | bytes 131072 | tf_op jit(solution)/shard_map/all_to_all | solution.py:57
  127.8 1.0 pad_maximum_fusion.refs_0_
  128.8 3.0 %collective-permute-start.3 = (bf16[4,8,9,8,128]{4,3,2,1,0:T(8,128)(2,1)S(1)}, bf16[4,8,9,8,128]{4,3,2,1,0:T(8,128)(2,1)}, u32[]{:S(2)}, u32[]{:S(2)}) collective-permute-start(bf16[4,8,9,8,128]{4,3,2,1,0:T(8,128)(2,1)S(1)} %pad_maximum_fusion.refs_0_), channel_id=1, source_target_pairs={{0,8},{8,16},{16,24},{24,0},{1,9},{9,17},{17,25},{25,1},{2,10},{10... | collective-permute-start | bytes 1769480 | tf_op jit(solution)/shard_map/ppermute | solution.py:70
  131.8 7.7 %all-to-all-done.4.t = bf16[32,8,128]{2,1,0:T(8,128)(2,1)S(1)} async-done(((bf16[32,8,128]{2,1,0:T(8,128)(2,1)}), bf16[32,8,128]{2,1,0:T(8,128)(2,1)S(1)}, u32[]{:S(2)}, u32[]{:S(2)}) %all-to-all-start.4) | async-done | bytes 65568 | tf_op jit(solution)/shard_map/all_to_all | solution.py:57
  139.6 0.7 moments.1
  140.3 21.7 %all-to-all-start.5 = ((bf16[32,8,128]{2,1,0:T(8,128)(2,1)}), bf16[32,8,128]{2,1,0:T(8,128)(2,1)S(1)}, u32[]{:S(2)}, u32[]{:S(2)}) async-start(bf16[32,8,128]{2,1,0:T(8,128)(2,1)} %get-tuple-element.32), calls=%async_computation.5 | async-start | bytes 131072 | tf_op jit(solution)/shard_map/all_to_all | solution.py:57
  162.0 4.2 %collective-permute-start.5 = (bf16[4,8,9,8,128]{4,3,2,1,0:T(8,128)(2,1)S(1)}, bf16[4,8,9,8,128]{4,3,2,1,0:T(8,128)(2,1)}, u32[]{:S(2)}, u32[]{:S(2)}) collective-permute-start(bf16[4,8,9,8,128]{4,3,2,1,0:T(8,128)(2,1)S(1)} %pad_maximum_fusion.refs_0_), channel_id=1, source_target_pairs={{0,24},{8,0},{16,8},{24,16},{1,25},{9,1},{17,9},{25,17},{2,26},{10... | collective-permute-start | bytes 1769480 | tf_op jit(solution)/shard_map/ppermute | solution.py:70
  166.2 1.9 collective-permute-start.4
  168.3 0.9 broadcast_in_dim.22
  169.1 6.2 %all-to-all-start.6 = ((bf16[8,32,8,128]{3,2,1,0:T(8,128)(2,1)}), bf16[8,32,8,128]{3,2,1,0:T(8,128)(2,1)S(1)}, u32[]{:S(2)}, u32[]{:S(2)}) async-start(bf16[8,32,8,128]{3,2,1,0:T(8,128)(2,1)} %broadcast_in_dim.22), calls=%async_computation.6 | async-start | bytes 1048576 | tf_op jit(solution)/shard_map/all_to_all | solution.py:57
  175.3 2.0 collective-permute-done.5.refs_3_
  177.3 6.0 %collective-permute-done.4.refs_2_ = bf16[4,8,9,8,128]{4,3,2,1,0:T(8,128)(2,1)} collective-permute-done((bf16[4,8,9,8,128]{4,3,2,1,0:T(8,128)(2,1)}, bf16[4,8,9,8,128]{4,3,2,1,0:T(8,128)(2,1)}, u32[]{:S(2)}, u32[]{:S(2)}) %collective-permute-start.4) | collective-permute-done | bytes 589856 | tf_op jit(solution)/shard_map/ppermute | solution.py:70
  183.3 6.3 %all-to-all-done.6.refs_4_ = bf16[8,32,8,128]{3,2,1,0:T(8,128)(2,1)S(1)} async-done(((bf16[8,32,8,128]{3,2,1,0:T(8,128)(2,1)}), bf16[8,32,8,128]{3,2,1,0:T(8,128)(2,1)S(1)}, u32[]{:S(2)}, u32[]{:S(2)}) %all-to-all-start.6) | async-done | bytes 524320 | tf_op jit(solution)/shard_map/all_to_all | solution.py:57
  189.6 1.6 assemble.1.mine
  191.2 3.2 %collective-permute-start.6 = (bf16[8,4,4,8,1024]{4,3,2,1,0:T(8,128)(2,1)S(1)}, bf16[8,4,4,8,1024]{4,3,2,1,0:T(8,128)(2,1)S(1)}, u32[]{:S(2)}, u32[]{:S(2)}) collective-permute-start(bf16[8,4,4,8,1024]{4,3,2,1,0:T(8,128)(2,1)S(1)} %assemble.1.mine), channel_id=1, source_target_pairs={{0,4},{4,0},{1,5},{5,1},{2,6},{6,2},{3,7},{7,3},{8,12},{12,8},{9,1... | collective-permute-start | bytes 6291464 | tf_op jit(solution)/shard_map/ppermute | solution.py:70
  194.4 0.8 gram.1
  195.1 0.8 totals.1
  195.9 6.6 %all_to_all.43.totals = f32[4,8,128]{2,1,0:T(8,128)S(1)} all-to-all(f32[4,8,128]{2,1,0:T(8,128)S(1)} %get-tuple-element.34), channel_id=1, replica_groups=mesh['z'=32,'x'=4,'c'=2,'tp'=4] {'tp'}, dimensions={0} | all-to-all | bytes 32768 | tf_op jit(solution)/shard_map/all_to_all | solution.py:57
  202.5 3.6 %final.1 = (bf16[8,4,4,2,8,512]{5,4,3,2,1,0:T(8,128)(2,1)}, bf16[512,2048]{1,0:T(8,128)(2,1)}, f32[8,512]{1,0:T(8,128)}, f32[8,512]{1,0:T(8,128)}, f32[8,512]{1,0:T(8,128)}, /*index=5*/f32[8,512]{1,0:T(8,128)}) custom-call(s32[5]{0:T(128)S(1)} %stack.32.place, f32[4,8,128]{2,1,0:T(8,128)S(1)} %all_to_all.43.totals, ...), custom_call_target="tpu_custom_call" | custom-call | flops 1073741824 | bytes 10000000 | tf_op jit(solution)/shard_map/final/pallas_call | solution.py:373
  (25 shorter events, 0.4 us)
Async XLA Ops:
  0.8 86.7 %copy-start.1 = (bf16[512,2048]{1,0:T(8,128)(2,1)S(1)}, bf16[512,2048]{1,0:T(8,128)(2,1)}, u32[]{:S(2)}) copy-start(bf16[512,2048]{1,0:T(8,128)(2,1)} %xo.1) | copy-start | bytes 6291460
  2.7 84.8 %copy-start = (bf16[512,2048]{1,0:T(8,128)(2,1)S(1)}, bf16[512,2048]{1,0:T(8,128)(2,1)}, u32[]{:S(2)}) copy-start(bf16[512,2048]{1,0:T(8,128)(2,1)} %xv.1) | copy-start | bytes 6291460
  80.3 7.2 %collective-permute-start = (bf16[16,4,8,8,128]{4,3,2,1,0:T(8,128)(2,1)S(1)}, bf16[16,4,8,8,128]{4,3,2,1,0:T(8,128)(2,1)S(1)}, u32[]{:S(2)}, u32[]{:S(2)}) collective-permute-start(bf16[16,4,8,8,128]{4,3,2,1,0:T(8,128)(2,1)S(1)} %all_to_all.42.mine), channel_id=1, source_target_pairs={{0,4},{4,0},{1,5},{5,1},{2,6},{6,2},{3,7},{7,3},{8,12},{12,8},{9,1... | collective-permute-start | bytes 3145736 | tf_op jit(solution)/shard_map/ppermute | solution.py:70
  92.4 47.2 %copy-start.4 = (f32[1,512]{1,0:T(1,128)S(1)}, f32[1,512]{1,0:T(1,128)}, u32[]{:S(2)}) copy-start(f32[1,512]{1,0:T(1,128)} %param.20) | copy-start | bytes 6148
  92.4 47.2 %copy-start.5 = (f32[1,512]{1,0:T(1,128)S(1)}, f32[1,512]{1,0:T(1,128)}, u32[]{:S(2)}) copy-start(f32[1,512]{1,0:T(1,128)} %param.21) | copy-start | bytes 6148
  92.4 47.2 %copy-start.6 = (f32[1,512]{1,0:T(1,128)S(1)}, f32[1,512]{1,0:T(1,128)}, u32[]{:S(2)}) copy-start(f32[1,512]{1,0:T(1,128)} %param.22) | copy-start | bytes 6148
  92.4 47.2 %copy-start.7 = (f32[1,512]{1,0:T(1,128)S(1)}, f32[1,512]{1,0:T(1,128)}, u32[]{:S(2)}) copy-start(f32[1,512]{1,0:T(1,128)} %param.23) | copy-start | bytes 6148
  92.4 13.3 %all-to-all-start.3 = ((bf16[8,32,1024]{2,1,0:T(8,128)(2,1)}), bf16[8,32,1024]{2,1,0:T(8,128)(2,1)S(1)}, u32[]{:S(2)}, u32[]{:S(2)}) async-start(bf16[8,32,1024]{2,1,0:T(8,128)(2,1)} %get-tuple-element.31), calls=%async_computation.3 | async-start | bytes 1048576 | tf_op jit(solution)/shard_map/all_to_all | solution.py:57
  96.3 7.2 %collective-permute-start.1 = (bf16[8,9,8,128]{3,2,1,0:T(8,128)(2,1)S(1)}, bf16[8,9,8,128]{3,2,1,0:T(8,128)(2,1)S(1)}, u32[]{:S(2)}, u32[]{:S(2)}) collective-permute-start(bf16[8,9,8,128]{3,2,1,0:T(8,128)(2,1)S(1)} %all_to_all.40), channel_id=1, source_target_pairs={{0,32},{32,0},{64,96},{96,64},{128,160},{160,128},{192,224},{224,1... | collective-permute-start | bytes 442376 | tf_op jit(solution)/shard_map/ppermute | solution.py:74
  103.5 24.3 %collective-permute-start.2 = (bf16[2,8,9,8,128]{4,3,2,1,0:T(8,128)(2,1)S(1)}, bf16[2,8,9,8,128]{4,3,2,1,0:T(8,128)(2,1)}, u32[]{:S(2)}, u32[]{:S(2)}) collective-permute-start(bf16[2,8,9,8,128]{4,3,2,1,0:T(8,128)(2,1)S(1)} %pad_maximum_fusion.1), channel_id=1, source_target_pairs={{0,64},{32,96},{64,0},{96,32},{128,192},{160,224},{192,128},{224,1... | collective-permute-start | bytes 884744 | tf_op jit(solution)/shard_map/ppermute | solution.py:74
  106.4 33.1 %all-to-all-start.4 = ((bf16[32,8,128]{2,1,0:T(8,128)(2,1)}), bf16[32,8,128]{2,1,0:T(8,128)(2,1)S(1)}, u32[]{:S(2)}, u32[]{:S(2)}) async-start(bf16[32,8,128]{2,1,0:T(8,128)(2,1)} %summed.1), calls=%async_computation.4 | async-start | bytes 131072 | tf_op jit(solution)/shard_map/all_to_all | solution.py:57
  128.8 37.3 %collective-permute-start.3 = (bf16[4,8,9,8,128]{4,3,2,1,0:T(8,128)(2,1)S(1)}, bf16[4,8,9,8,128]{4,3,2,1,0:T(8,128)(2,1)}, u32[]{:S(2)}, u32[]{:S(2)}) collective-permute-start(bf16[4,8,9,8,128]{4,3,2,1,0:T(8,128)(2,1)S(1)} %pad_maximum_fusion.refs_0_), channel_id=1, source_target_pairs={{0,8},{8,16},{16,24},{24,0},{1,9},{9,17},{17,25},{25,1},{2,10},{10... | collective-permute-start | bytes 1769480 | tf_op jit(solution)/shard_map/ppermute | solution.py:70
  140.3 28.0 %all-to-all-start.5 = ((bf16[32,8,128]{2,1,0:T(8,128)(2,1)}), bf16[32,8,128]{2,1,0:T(8,128)(2,1)S(1)}, u32[]{:S(2)}, u32[]{:S(2)}) async-start(bf16[32,8,128]{2,1,0:T(8,128)(2,1)} %get-tuple-element.32), calls=%async_computation.5 | async-start | bytes 131072 | tf_op jit(solution)/shard_map/all_to_all | solution.py:57
  162.0 15.4 %collective-permute-start.5 = (bf16[4,8,9,8,128]{4,3,2,1,0:T(8,128)(2,1)S(1)}, bf16[4,8,9,8,128]{4,3,2,1,0:T(8,128)(2,1)}, u32[]{:S(2)}, u32[]{:S(2)}) collective-permute-start(bf16[4,8,9,8,128]{4,3,2,1,0:T(8,128)(2,1)S(1)} %pad_maximum_fusion.refs_0_), channel_id=1, source_target_pairs={{0,24},{8,0},{16,8},{24,16},{1,25},{9,1},{17,9},{25,17},{2,26},{10... | collective-permute-start | bytes 1769480 | tf_op jit(solution)/shard_map/ppermute | solution.py:70
  166.2 17.1 %collective-permute-start.4 = (bf16[4,8,9,8,128]{4,3,2,1,0:T(8,128)(2,1)}, bf16[4,8,9,8,128]{4,3,2,1,0:T(8,128)(2,1)}, u32[]{:S(2)}, u32[]{:S(2)}) collective-permute-start(bf16[4,8,9,8,128]{4,3,2,1,0:T(8,128)(2,1)} %collective-permute-done.3.refs_1_), channel_id=1, source_target_pairs={{0,8},{8,16},{16,24},{24,0},{1,9},{9,17},{17,25},{25,1},{2,10},{10... | collective-permute-start | bytes 1769480 | tf_op jit(solution)/shard_map/ppermute | solution.py:70
  169.1 20.4 %all-to-all-start.6 = ((bf16[8,32,8,128]{3,2,1,0:T(8,128)(2,1)}), bf16[8,32,8,128]{3,2,1,0:T(8,128)(2,1)S(1)}, u32[]{:S(2)}, u32[]{:S(2)}) async-start(bf16[8,32,8,128]{3,2,1,0:T(8,128)(2,1)} %broadcast_in_dim.22), calls=%async_computation.6 | async-start | bytes 1048576 | tf_op jit(solution)/shard_map/all_to_all | solution.py:57
  191.1 11.3 %copy-start.2 = (f32[8,512]{1,0:T(8,128)S(1)}, f32[8,512]{1,0:T(8,128)}, u32[]{:S(2)}) copy-start(f32[8,512]{1,0:T(8,128)} %ov.1) | copy-start | bytes 49156
  191.2 11.3 %copy-start.3 = (f32[512,8]{0,1:T(8,128)S(1)}, f32[512,8]{0,1:T(8,128)}, u32[]{:S(2)}) copy-start(f32[512,8]{0,1:T(8,128)} %param.19) | copy-start | bytes 49156
  191.2 11.3 %collective-permute-start.6 = (bf16[8,4,4,8,1024]{4,3,2,1,0:T(8,128)(2,1)S(1)}, bf16[8,4,4,8,1024]{4,3,2,1,0:T(8,128)(2,1)S(1)}, u32[]{:S(2)}, u32[]{:S(2)}) collective-permute-start(bf16[8,4,4,8,1024]{4,3,2,1,0:T(8,128)(2,1)S(1)} %assemble.1.mine), channel_id=1, source_target_pairs={{0,4},{4,0},{1,5},{5,1},{2,6},{6,2},{3,7},{7,3},{8,12},{12,8},{9,1... | collective-permute-start | bytes 6291464 | tf_op jit(solution)/shard_map/ppermute | solution.py:70

commit v5 on v4

--- a/solution.py
+++ b/solution.py
@@ -11,12 +11,12 @@
 R = 256
 FS = ("z", "x", "c")
 NZL = 4
+FIRST = 5
 LANES = 128
 TN = (((0,), (0,)), ((), ()))
 
 
 VMEM = pl.BlockSpec(memory_space=pltpu.VMEM)
-SMEM = pl.BlockSpec(memory_space=pltpu.SMEM)
 HBM = pl.BlockSpec(memory_space=pltpu.HBM)
 
 
@@ -50,7 +50,7 @@
 
 def far_z(nz):
     n = nz // NZL
-    return [[i + NZL * k for k in turned(n, n // 2)] for i in range(NZL)]
+    return [[i + NZL * k for k in turned(n, FIRST)] for i in range(NZL)]
 
 
 def exchange(blocks, axes, groups=None):
@@ -74,21 +74,19 @@
     return lax.ppermute(block, axis, [(i, i ^ bit) for i in range(lax.axis_size(axis))])
 
 
-def pack_kernel(place, fv, fo, wv, wo, vv, vo, out, vv_in, vo_in, fv_in, fo_in, wv_in, wo_in, sems):
+def pack_kernel(fv, fo, wv, wo, out, fv_in, fo_in, wv_in, wo_in, sems):
     copies = [
         pltpu.make_async_copy(src, dst, sems.at[i])
-        for i, (src, dst) in enumerate(
-            ((fv, fv_in), (fo, fo_in), (wv, wv_in), (wo, wo_in), (vv, vv_in), (vo, vo_in))
-        )
+        for i, (src, dst) in enumerate(((fv, fv_in), (fo, fo_in), (wv, wv_in), (wo, wo_in)))
     ]
     for copy in copies:
         copy.start()
     n = R // 8
-    y = place[0]
+    y = lax.axis_index("tp")
     j = lax.broadcasted_iota(jnp.int32, (R, R), 0)
     k = lax.broadcasted_iota(jnp.int32, (R, R), 1)
-    turn = (j == (k % n + n // 2) % n * 8 + k // n).astype(jnp.bfloat16)
-    for copy in copies[:4]:
+    turn = (j == (k % n + FIRST * NZL) % n * 8 + k // n).astype(jnp.bfloat16)
+    for copy in copies:
         copy.wait()
     factor = jnp.where(y < 2, fv_in[...].astype(jnp.float32), fo_in[...].astype(jnp.float32))
     factor = dot(factor.astype(jnp.bfloat16), turn)
@@ -99,39 +97,35 @@
         tiles += [half[:, t : t + LANES] for t in range(0, half.shape[1], LANES)]
     for t, tile in enumerate(tiles):
         out[:, t] = jnp.broadcast_to(tile[None], (out.shape[0], *tile.shape))
-    for copy in copies[4:]:
-        copy.wait()
-
-
-def packed(count, place, fv, fo, wv, wo, vv, vo):
+
+
+def packed(count, fv, fo, wv, wo):
     rows, cols = wv.shape
     tiles = 1 + 2 * cols // LANES
     return pl.pallas_call(
         pack_kernel,
-        out_shape=(
-            jax.ShapeDtypeStruct((count, tiles, rows, LANES), jnp.bfloat16),
-            pltpu.VMEM(vv.shape, vv.dtype),
-            pltpu.VMEM(vo.shape, vo.dtype),
-        ),
-        in_specs=[SMEM] + [HBM] * 6,
-        out_specs=(VMEM,) * 3,
+        out_shape=jax.ShapeDtypeStruct((count, tiles, rows, LANES), jnp.bfloat16),
+        in_specs=[HBM] * 4,
+        out_specs=VMEM,
         scratch_shapes=[
             pltpu.VMEM(fv.shape, fv.dtype),
             pltpu.VMEM(fo.shape, fo.dtype),
             pltpu.VMEM(wv.shape, wv.dtype),
             pltpu.VMEM(wo.shape, wo.dtype),
-            pltpu.SemaphoreType.DMA((6,)),
+            pltpu.SemaphoreType.DMA((4,)),
         ],
         name="packed",
         compiler_params=params(4),
         cost_estimate=cost(2 * 8 * R * R, 200_000),
-    )(place, *far(fv, fo, wv, wo, vv, vo))
-
-
-def project_kernel(place, mine, other, xv, vv, xo, vo, out, whole):
-    c = place[2]
+    )(*far(fv, fo, wv, wo))
+
+
+def project_kernel(mine, other, xv, vv, xo, vo, out, whole, late, sems):
+    c = lax.axis_index("c")
+    read = pltpu.make_async_copy(xo, late, sems.at[0])
+    read.start()
     nzh, nzl, nx = whole.shape[1:4]
-    first = nzh // 2
+    first = FIRST
     half = R // LANES
     cols = vv.shape[1]
     for f in range(2):
@@ -143,13 +137,15 @@
                         block = src.at[x * 2 * half + f * half + h, k]
                         whole[f, first:, zl, x, at, :, lanes] = block[: nzh - first]
                         whole[f, :first, zl, x, at, :, lanes] = block[nzh - first :]
-    for f, (x, v) in enumerate(((xv, vv), (xo, vo))):
+    for f, (x, v) in enumerate(((xv, vv), (late, vo))):
+        if f == 1:
+            read.wait()
         projected = dot(x[...], whole[f].reshape(D, R)).astype(jnp.bfloat16)
         term = dot(projected, v[...], TN).astype(jnp.bfloat16)
         out[:, :, f * cols : (f + 1) * cols] = term.reshape(out.shape[0], out.shape[1], cols)
 
 
-def projected_terms(place, mine, other, xv, vv, xo, vo, sizes):
+def projected_terms(mine, other, xv, vv, xo, vo, sizes):
     nzh, nzl, nx, nc = sizes
     shape = (2, nzh, nzl, nx, nc, D // (nzh * nzl * nx * nc), R)
     cols = vv.shape[1]
@@ -160,12 +156,13 @@
             jax.ShapeDtypeStruct((nx * nc, nzh * nzl, 2 * cols), jnp.bfloat16),
             pltpu.VMEM(shape, jnp.bfloat16),
         ),
-        in_specs=[SMEM] + [VMEM] * 6,
+        in_specs=[VMEM] * 4 + [HBM, VMEM],
         out_specs=(VMEM, VMEM),
+        scratch_shapes=[pltpu.VMEM(xo.shape, xo.dtype), pltpu.SemaphoreType.DMA((1,))],
         name="project",
         compiler_params=params(12),
         cost_estimate=cost(4 * tokens * R * (D + cols), 10_000_000),
-    )(place, mine, other, *near(xv, vv, xo, vo))
+    )(mine, other, *near(xv, vv), *far(xo), *near(vo))
 
 
 def summed_kernel(t, out, lines):
@@ -276,11 +273,11 @@
     )(d, *near(gram))
 
 
-def assemble_kernel(place, *refs):
+def assemble_kernel(*refs):
     (*whole, _, out) = refs
-    zl, x = place[1], place[3]
+    zl, x = lax.axis_index("z") % NZL, lax.axis_index("x")
     nzh, nzl, nx = out.shape[:3]
-    first = nzh // 2
+    first = FIRST
     parts = [(k, s, part.at[s]) for k, part in enumerate(whole) for s in range(nzl)]
     for k, s, part in parts:
         px = lax.rem(x + nx - k, nx)
@@ -291,22 +288,22 @@
             out[:first, at, px, :, lanes] = part[nzh - first :, 1 + t]
 
 
-def assembled(place, parts, sizes, after):
+def assembled(parts, sizes, after):
     nzh, nzl, nx, _ = sizes
     tiles, rows = parts[0].shape[2:4]
     shape = (nzh, nzl, nx, rows, (tiles - 1) * LANES)
     return pl.pallas_call(
         assemble_kernel,
         out_shape=jax.ShapeDtypeStruct(shape, jnp.bfloat16),
-        in_specs=[SMEM] + [VMEM] * len(parts) + [pl.BlockSpec(memory_space=pl.ANY)],
+        in_specs=[VMEM] * len(parts) + [pl.BlockSpec(memory_space=pl.ANY)],
         out_specs=VMEM,
         name="assemble",
         compiler_params=params(8),
         cost_estimate=cost(1_000_000, 4_000_000),
-    )(place, *near(*parts), after)
-
-
-def final_kernel(place, totals, directions, factors, mine, other, ov, oo, *refs):
+    )(*near(*parts), after)
+
+
+def final_kernel(totals, directions, factors, mine, other, ov, oo, *refs):
     copy_v, copy_o, sv, so, nv, no, out_v, out_o, own, sems = refs
     steps, nzl, nx, nc, rows, _ = factors.shape[1:]
     chunk = D // steps
@@ -323,10 +320,11 @@
             pltpu.make_async_copy(out_o.at[:, lanes], copy_o.at[:, lanes], sems.at[2 * k + 1]),
         ]
 
+    z, x, c = (lax.axis_index(a) for a in FS)
     small = []
     for f, (w, targets) in enumerate(((ov, (sv, nv)), (oo, (so, no)))):
-        mine_f = factors[f, place[4], place[1], place[3], place[2]]
-        step = dot(mine_f, directions[f]) * scales[f]
+        factor = factors[f, z // NZL, z % NZL, x, c]
+        step = dot(factor, directions[f]) * scales[f]
         own[2 * f] = step
         own[2 * f + 1] = w[...] - 0.02 * step
         small += [
@@ -338,11 +336,11 @@
 
     def copies(pair):
         for i in range(steps):
-            for c in range(nc):
-                factor = factors[0, i, :, :, c].reshape(chunk // nc, R)
+            for k in range(nc):
+                factor = factors[0, i, :, :, k].reshape(chunk // nc, R)
                 update = dot(factor, directions[0]) * (0.02 * scales[0])
-                w = pair[c][i, :, :, :, :cols].reshape(chunk // nc, cols).astype(jnp.float32)
-                out_v[i, :, :, c] = (w - update).astype(jnp.bfloat16).reshape(nzl, nx, rows, cols)
+                w = pair[k][i, :, :, :, :cols].reshape(chunk // nc, cols).astype(jnp.float32)
+                out_v[i, :, :, k] = (w - update).astype(jnp.bfloat16).reshape(nzl, nx, rows, cols)
             if (i + 1) * 2 % steps == 0:
                 writes[(i + 1) * 4 // steps - 2].start()
             update = dot(factors[1, i].reshape(chunk, R), directions[1]) * (0.02 * scales[1])
@@ -352,7 +350,7 @@
             if (i + 1) * 2 % steps == 0:
                 writes[(i + 1) * 4 // steps - 1].start()
 
-    first = place[2] == 0
+    first = c == 0
 
     @pl.when(first)
     def _():
@@ -366,7 +364,7 @@
         copy.wait()
 
 
-def final(place, totals, directions, factors, mine, other, ov, oo):
+def final(totals, directions, factors, mine, other, ov, oo):
     cols = directions.shape[2]
     own = pltpu.HBM(ov.shape, jnp.float32)
     shape = (*factors.shape[1:-1], cols)
@@ -380,7 +378,7 @@
             own,
             own,
         ),
-        in_specs=[SMEM] + [VMEM] * 7,
+        in_specs=[VMEM] * 7,
         out_specs=(HBM,) * 6,
         scratch_shapes=[
             pltpu.VMEM(shape, jnp.bfloat16),
@@ -391,7 +389,7 @@
         name="final",
         compiler_params=params(12),
         cost_estimate=cost(4 * D * cols * R, 10_000_000),
-    )(place, totals, *near(directions, factors, mine, other), ov, oo)
+    )(totals, *near(directions, factors, mine, other), ov, oo)
     return copy_value.reshape(D, cols), *rest
 
 
@@ -413,23 +411,11 @@
     nzh, nzl = nz // NZL, NZL
     sizes = nzh, nzl, nx, nc
     ny = lax.axis_size("tp")
-    around = [turned(nz, nz // 2)]
+    around = [turned(nz, FIRST * NZL)]
     _, cols = weight_value.shape
 
-    z = lax.axis_index("z")
-    at = [lax.axis_index("tp"), z % nzl, lax.axis_index("c"), lax.axis_index("x"), z // nzl]
-    place = jnp.stack(at).astype(jnp.int32)
     turned_weight = weight_output.T
-    w, value_near, output_near = packed(
-        nzh,
-        place,
-        factor_value,
-        factor_output,
-        weight_value,
-        turned_weight,
-        value_cotangent,
-        gated_output,
-    )
+    w = packed(nzh, factor_value, factor_output, weight_value, turned_weight)
     w = exchange(w, "z", far_z(nz))
     f = to_all(w[:, 0], "z", near_z(nz))
     f = to_all(f, ("x", "tp"))
@@ -441,7 +427,7 @@
     w0 = jnp.concatenate([w, get])
 
     terms, factors = projected_terms(
-        place, f, other, normed_input, value_near, layer_cotangent, output_near, sizes
+        f, other, normed_input, value_cotangent, layer_cotangent, gated_output, sizes
     )
     t = exchange(terms, ("x", "c"))
     t = summed(t)
@@ -463,14 +449,13 @@
 
     w2 = moved(w1, "x", 1)
     d = to_all(d, ("x", "c"))
-    mine = assembled(place, (w0, w1, w2, w3), sizes, d)
+    mine = assembled((w0, w1, w2, w3), sizes, d)
     flip = moved(mine, "c", 1)
 
     totals, directions = totals_of(ny, d.reshape(R, *d.shape[2:]), gram)
     totals = exchange(totals, "tp")
 
     copy_value, copy_output, step_value, step_output, next_value, next_output = final(
-        place,
         totals,
         directions,
         factors,

time: 207 us -> 201 us (0.971)
  blocking collectives: 83.8 us -> 80.4 us
    all_to_all x4, waiting for transfers between devices: 14.2 us -> 19.1 us  [exchange(): lax.all_to_all(blocks, axes, split_axis=0, concat_axis=0, axis_index_grou...]
    ppermute x5, waiting for transfers between devices: 10.2 us -> 5.86 us  [moved(): return lax.ppermute(block, axis, [(i, (i + by) % n) for i in range(n)])]
    all_to_all x4, blocking collectives: 83.8 us -> 80.4 us  [exchange(): lax.all_to_all(blocks, axes, split_axis=0, concat_axis=0, axis_index_grou...]
    all_to_all x4, starting transfers between devices: 53.1 us -> 49.7 us  [exchange(): lax.all_to_all(blocks, axes, split_axis=0, concat_axis=0, axis_index_grou...]
where the time goes in v5:
time: 201 us; the launch traced here: 200 us
  blocking collectives  80.4 us (40%)
  starting transfers between devices  72.5 us (36%)
  waiting for transfers between devices  30.3 us (15%)
  Pallas kernels  14.2 us (7%)
    all_to_all x4, blocking collectives, exchange(): lax.all_to_all(blocks, axes, split_axis=0, concat_axis=0, axis_index_grou...  80.4 us
    all_to_all x4, starting transfers between devices, exchange(): lax.all_to_all(blocks, axes, split_axis=0, concat_axis=0, axis_index_grou...  49.7 us
    all_to_all x4, waiting for transfers between devices, exchange(): lax.all_to_all(blocks, axes, split_axis=0, concat_axis=0, axis_index_grou...  19.1 us
    ppermute x5, starting transfers between devices, moved(): return lax.ppermute(block, axis, [(i, (i + by) % n) for i in range(n)])  18.9 us
    ppermute x5, waiting for transfers between devices, moved(): return lax.ppermute(block, axis, [(i, (i + by) % n) for i in range(n)])  5.86 us
    pallas_call x1, Pallas kernels, projected_terms(): pl.pallas_call(project_kernel, out_shape=(jax.ShapeDtypeStruct((nx * nc,...  5.6 us
    ppermute x2, waiting for transfers between devices, swapped(): lax.ppermute(block, axis, [(i, i ^ bit) for i in range(lax.axis_size(axis...  5.26 us
  transfers between devices with their start and end apart: 11, of which 7 were waited for; matrix products, arithmetic and copies ran while one was open for 1% of the time, Pallas kernels for 1%

profile of v5, /device:TPU:1, one launch (start us, length us, event | category | flops | bytes accessed | tf_op | source)
XLA Modules:
  0.0 200.4 jit_solution(14447421283355818935)
XLA Ops:
  0.7 1.1 packed.1
  1.8 45.6 %all_to_all.40 = bf16[8,9,8,128]{3,2,1,0:T(8,128)(2,1)S(1)} all-to-all(bf16[8,9,8,128]{3,2,1,0:T(8,128)(2,1)S(1)} %packed.1), channel_id=1, replica_groups={{640,768,896,0,128,256,384,512},{672,800,928,32,160,288,416,544},{704,8..., dimensions={0} | all-to-all | bytes 294912 | tf_op jit(solution)/shard_map/all_to_all | solution.py:57
  47.4 8.2 %all_to_all.41 = bf16[4,8,8,128]{3,2,1,0:T(8,128)(2,1)S(1)} all-to-all(bf16[4,8,8,128]{3,2,1,0:T(8,128)(2,1)S(1)} %broadcast_in_dim.9), channel_id=1, replica_groups={{32,0,64,96},{160,128,192,224},{288,256,320,352},{416,384,448,480},{544..., dimensions={0} | all-to-all | bytes 131072 | tf_op jit(solution)/shard_map/all_to_all | solution.py:57
  55.6 0.2 broadcast_in_dim.10
  55.9 20.0 %all_to_all.42.mine = bf16[16,4,8,8,128]{4,3,2,1,0:T(8,128)(2,1)S(1)} all-to-all(bf16[16,4,8,8,128]{4,3,2,1,0:T(8,128)(2,1)S(1)} %broadcast_in_dim.10), channel_id=1, replica_groups=mesh['z'=32,'x'=4,'c'=2,'tp'=4] {'x','tp'}, dimensions={0} | all-to-all | bytes 2097152 | tf_op jit(solution)/shard_map/all_to_all | solution.py:57
  75.9 6.5 %collective-permute-start = (bf16[16,4,8,8,128]{4,3,2,1,0:T(8,128)(2,1)S(1)}, bf16[16,4,8,8,128]{4,3,2,1,0:T(8,128)(2,1)S(1)}, u32[]{:S(2)}, u32[]{:S(2)}) collective-permute-start(bf16[16,4,8,8,128]{4,3,2,1,0:T(8,128)(2,1)S(1)} %all_to_all.42.mine), channel_id=1, source_target_pairs={{0,4},{4,0},{1,5},{5,1},{2,6},{6,2},{3,7},{7,3},{8,12},{12,8},{9,1... | collective-permute-start | bytes 3145736 | tf_op jit(solution)/shard_map/ppermute | solution.py:70
  82.4 2.3 %collective-permute-done.other = bf16[16,4,8,8,128]{4,3,2,1,0:T(8,128)(2,1)S(1)} collective-permute-done((bf16[16,4,8,8,128]{4,3,2,1,0:T(8,128)(2,1)S(1)}, bf16[16,4,8,8,128]{4,3,2,1,0:T(8,128)(2,1)S(1)}, u32[]{:S(2)}, u32[]{:S(2)}) %collective-permute-start) | collective-permute-done | bytes 1048608 | tf_op jit(solution)/shard_map/ppermute | solution.py:70
  84.7 5.6 %project.1 = (bf16[8,32,1024]{2,1,0:T(8,128)(2,1)}, bf16[2,8,4,4,2,8,256]{6,5,4,3,2,1,0:T(8,128)(2,1)S(1)}) custom-call(bf16[16,4,8,8,128]{4,3,2,1,0:T(8,128)(2,1)S(1)} %all_to_all.42.mine, bf16[16,4,8,8,128]{4,3,2,1,0:T(8,128)(2,1)S(1)} %collective-permute-done.other, bf16[512,2048]{1,0:T(8,128)(2,1)S(1)} %copy-done, bf16[512,512]{1,0:T(8,128)(2,1)S(1)} %copy-done.1, ...), custom_call_target="tpu_custom_call" | custom-call | flops 1342177280 | bytes 10000000 | tf_op jit(solution)/shard_map/project/pallas_call | solution.py:153
  90.3 3.9 %all-to-all-start.3 = ((bf16[8,32,1024]{2,1,0:T(8,128)(2,1)}), bf16[8,32,1024]{2,1,0:T(8,128)(2,1)S(1)}, u32[]{:S(2)}, u32[]{:S(2)}) async-start(bf16[8,32,1024]{2,1,0:T(8,128)(2,1)} %get-tuple-element.25), calls=%async_computation.3 | async-start | bytes 1048576 | tf_op jit(solution)/shard_map/all_to_all | solution.py:57
  94.3 1.9 collective-permute-start.1
  96.2 5.3 %collective-permute-done.1 = bf16[8,9,8,128]{3,2,1,0:T(8,128)(2,1)S(1)} collective-permute-done((bf16[8,9,8,128]{3,2,1,0:T(8,128)(2,1)S(1)}, bf16[8,9,8,128]{3,2,1,0:T(8,128)(2,1)S(1)}, u32[]{:S(2)}, u32[]{:S(2)}) %collective-permute-start.1) | collective-permute-done | bytes 147488 | tf_op jit(solution)/shard_map/ppermute | solution.py:74
  101.5 2.0 %collective-permute-start.2 = (bf16[2,8,9,8,128]{4,3,2,1,0:T(8,128)(2,1)S(1)}, bf16[2,8,9,8,128]{4,3,2,1,0:T(8,128)(2,1)}, u32[]{:S(2)}, u32[]{:S(2)}) collective-permute-start(bf16[2,8,9,8,128]{4,3,2,1,0:T(8,128)(2,1)S(1)} %pad_maximum_fusion.1), channel_id=1, source_target_pairs={{0,64},{32,96},{64,0},{96,32},{128,192},{160,224},{192,128},{224,1... | collective-permute-start | bytes 884744 | tf_op jit(solution)/shard_map/ppermute | solution.py:74
  103.6 0.7 summed.1
  104.4 18.4 %all-to-all-start.4 = ((bf16[32,8,128]{2,1,0:T(8,128)(2,1)}), bf16[32,8,128]{2,1,0:T(8,128)(2,1)S(1)}, u32[]{:S(2)}, u32[]{:S(2)}) async-start(bf16[32,8,128]{2,1,0:T(8,128)(2,1)} %summed.1), calls=%async_computation.4 | async-start | bytes 131072 | tf_op jit(solution)/shard_map/all_to_all | solution.py:57
  122.8 1.0 pad_maximum_fusion.refs_0_
  123.8 3.0 %collective-permute-start.3 = (bf16[4,8,9,8,128]{4,3,2,1,0:T(8,128)(2,1)S(1)}, bf16[4,8,9,8,128]{4,3,2,1,0:T(8,128)(2,1)}, u32[]{:S(2)}, u32[]{:S(2)}) collective-permute-start(bf16[4,8,9,8,128]{4,3,2,1,0:T(8,128)(2,1)S(1)} %pad_maximum_fusion.refs_0_), channel_id=1, source_target_pairs={{0,8},{8,16},{16,24},{24,0},{1,9},{9,17},{17,25},{25,1},{2,10},{10... | collective-permute-start | bytes 1769480 | tf_op jit(solution)/shard_map/ppermute | solution.py:70
  126.8 7.4 %all-to-all-done.4.t = bf16[32,8,128]{2,1,0:T(8,128)(2,1)S(1)} async-done(((bf16[32,8,128]{2,1,0:T(8,128)(2,1)}), bf16[32,8,128]{2,1,0:T(8,128)(2,1)S(1)}, u32[]{:S(2)}, u32[]{:S(2)}) %all-to-all-start.4) | async-done | bytes 65568 | tf_op jit(solution)/shard_map/all_to_all | solution.py:57
  134.3 0.7 moments.1
  134.9 22.0 %all-to-all-start.5 = ((bf16[32,8,128]{2,1,0:T(8,128)(2,1)}), bf16[32,8,128]{2,1,0:T(8,128)(2,1)S(1)}, u32[]{:S(2)}, u32[]{:S(2)}) async-start(bf16[32,8,128]{2,1,0:T(8,128)(2,1)} %get-tuple-element.26), calls=%async_computation.5 | async-start | bytes 131072 | tf_op jit(solution)/shard_map/all_to_all | solution.py:57
  156.9 4.2 %collective-permute-start.5 = (bf16[4,8,9,8,128]{4,3,2,1,0:T(8,128)(2,1)S(1)}, bf16[4,8,9,8,128]{4,3,2,1,0:T(8,128)(2,1)}, u32[]{:S(2)}, u32[]{:S(2)}) collective-permute-start(bf16[4,8,9,8,128]{4,3,2,1,0:T(8,128)(2,1)S(1)} %pad_maximum_fusion.refs_0_), channel_id=1, source_target_pairs={{0,24},{8,0},{16,8},{24,16},{1,25},{9,1},{17,9},{25,17},{2,26},{10... | collective-permute-start | bytes 1769480 | tf_op jit(solution)/shard_map/ppermute | solution.py:70
  161.1 1.9 collective-permute-start.4
  163.1 4.8 %all-to-all-done.5 = bf16[32,8,128]{2,1,0:T(8,128)(2,1)S(1)} async-done(((bf16[32,8,128]{2,1,0:T(8,128)(2,1)}), bf16[32,8,128]{2,1,0:T(8,128)(2,1)S(1)}, u32[]{:S(2)}, u32[]{:S(2)}) %all-to-all-start.5) | async-done | bytes 65568 | tf_op jit(solution)/shard_map/all_to_all | solution.py:57
  167.9 0.9 broadcast_in_dim.22
  168.7 5.4 %all-to-all-start.6 = ((bf16[8,32,8,128]{3,2,1,0:T(8,128)(2,1)}), bf16[8,32,8,128]{3,2,1,0:T(8,128)(2,1)S(1)}, u32[]{:S(2)}, u32[]{:S(2)}) async-start(bf16[8,32,8,128]{3,2,1,0:T(8,128)(2,1)} %broadcast_in_dim.22), calls=%async_computation.6 | async-start | bytes 1048576 | tf_op jit(solution)/shard_map/all_to_all | solution.py:57
  174.2 3.6 %collective-permute-done.4.refs_2_ = bf16[4,8,9,8,128]{4,3,2,1,0:T(8,128)(2,1)} collective-permute-done((bf16[4,8,9,8,128]{4,3,2,1,0:T(8,128)(2,1)}, bf16[4,8,9,8,128]{4,3,2,1,0:T(8,128)(2,1)}, u32[]{:S(2)}, u32[]{:S(2)}) %collective-permute-start.4) | collective-permute-done | bytes 589856 | tf_op jit(solution)/shard_map/ppermute | solution.py:70
  177.8 6.8 %all-to-all-done.6.refs_4_ = bf16[8,32,8,128]{3,2,1,0:T(8,128)(2,1)S(1)} async-done(((bf16[8,32,8,128]{3,2,1,0:T(8,128)(2,1)}), bf16[8,32,8,128]{3,2,1,0:T(8,128)(2,1)S(1)}, u32[]{:S(2)}, u32[]{:S(2)}) %all-to-all-start.6) | async-done | bytes 524320 | tf_op jit(solution)/shard_map/all_to_all | solution.py:57
  184.5 1.6 assemble.1.mine
  186.2 3.2 %collective-permute-start.6 = (bf16[8,4,4,8,1024]{4,3,2,1,0:T(8,128)(2,1)S(1)}, bf16[8,4,4,8,1024]{4,3,2,1,0:T(8,128)(2,1)S(1)}, u32[]{:S(2)}, u32[]{:S(2)}) collective-permute-start(bf16[8,4,4,8,1024]{4,3,2,1,0:T(8,128)(2,1)S(1)} %assemble.1.mine), channel_id=1, source_target_pairs={{0,4},{4,0},{1,5},{5,1},{2,6},{6,2},{3,7},{7,3},{8,12},{12,8},{9,1... | collective-permute-start | bytes 6291464 | tf_op jit(solution)/shard_map/ppermute | solution.py:70
  189.3 0.8 gram.1
  190.1 0.8 totals.1
  190.9 6.6 %all_to_all.43.totals = f32[4,8,128]{2,1,0:T(8,128)S(1)} all-to-all(f32[4,8,128]{2,1,0:T(8,128)S(1)} %get-tuple-element.28), channel_id=1, replica_groups=mesh['z'=32,'x'=4,'c'=2,'tp'=4] {'tp'}, dimensions={0} | all-to-all | bytes 32768 | tf_op jit(solution)/shard_map/all_to_all | solution.py:57
  197.5 3.0 %final.1 = (bf16[8,4,4,2,8,512]{5,4,3,2,1,0:T(8,128)(2,1)}, bf16[512,2048]{1,0:T(8,128)(2,1)}, f32[8,512]{1,0:T(8,128)}, f32[8,512]{1,0:T(8,128)}, f32[8,512]{1,0:T(8,128)}, /*index=5*/f32[8,512]{1,0:T(8,128)}) custom-call(f32[4,8,128]{2,1,0:T(8,128)S(1)} %all_to_all.43.totals, bf16[2,256,512]{2,1,0:T(8,128)(2,1)S(1)} %get-tuple-element.29.directions, ...), custom_call_target="tpu_custom_call" | custom-call | flops 1073741824 | bytes 10000000 | tf_op jit(solution)/shard_map/final/pallas_call | solution.py:371
  (26 shorter events, 0.3 us)
Async XLA Ops:
  0.6 84.0 %copy-start.2 = (bf16[512,512]{1,0:T(8,128)(2,1)S(1)}, bf16[512,512]{1,0:T(8,128)(2,1)}, u32[]{:S(2)}) copy-start(bf16[512,512]{1,0:T(8,128)(2,1)} %vo.1) | copy-start | bytes 1572868
  0.7 84.0 %copy-start.1 = (bf16[512,512]{1,0:T(8,128)(2,1)S(1)}, bf16[512,512]{1,0:T(8,128)(2,1)}, u32[]{:S(2)}) copy-start(bf16[512,512]{1,0:T(8,128)(2,1)} %vv.1) | copy-start | bytes 1572868
  0.7 84.0 %copy-start = (bf16[512,2048]{1,0:T(8,128)(2,1)S(1)}, bf16[512,2048]{1,0:T(8,128)(2,1)}, u32[]{:S(2)}) copy-start(bf16[512,2048]{1,0:T(8,128)(2,1)} %xv.1) | copy-start | bytes 6291460
  75.9 8.8 %collective-permute-start = (bf16[16,4,8,8,128]{4,3,2,1,0:T(8,128)(2,1)S(1)}, bf16[16,4,8,8,128]{4,3,2,1,0:T(8,128)(2,1)S(1)}, u32[]{:S(2)}, u32[]{:S(2)}) collective-permute-start(bf16[16,4,8,8,128]{4,3,2,1,0:T(8,128)(2,1)S(1)} %all_to_all.42.mine), channel_id=1, source_target_pairs={{0,4},{4,0},{1,5},{5,1},{2,6},{6,2},{3,7},{7,3},{8,12},{12,8},{9,1... | collective-permute-start | bytes 3145736 | tf_op jit(solution)/shard_map/ppermute | solution.py:70
  90.3 44.0 %copy-start.5 = (f32[1,512]{1,0:T(1,128)S(1)}, f32[1,512]{1,0:T(1,128)}, u32[]{:S(2)}) copy-start(f32[1,512]{1,0:T(1,128)} %param.20) | copy-start | bytes 6148
  90.3 43.9 %copy-start.6 = (f32[1,512]{1,0:T(1,128)S(1)}, f32[1,512]{1,0:T(1,128)}, u32[]{:S(2)}) copy-start(f32[1,512]{1,0:T(1,128)} %param.21) | copy-start | bytes 6148
  90.3 43.9 %copy-start.7 = (f32[1,512]{1,0:T(1,128)S(1)}, f32[1,512]{1,0:T(1,128)}, u32[]{:S(2)}) copy-start(f32[1,512]{1,0:T(1,128)} %param.22) | copy-start | bytes 6148
  90.3 43.9 %copy-start.8 = (f32[1,512]{1,0:T(1,128)S(1)}, f32[1,512]{1,0:T(1,128)}, u32[]{:S(2)}) copy-start(f32[1,512]{1,0:T(1,128)} %param.23) | copy-start | bytes 6148
  90.3 13.3 %all-to-all-start.3 = ((bf16[8,32,1024]{2,1,0:T(8,128)(2,1)}), bf16[8,32,1024]{2,1,0:T(8,128)(2,1)S(1)}, u32[]{:S(2)}, u32[]{:S(2)}) async-start(bf16[8,32,1024]{2,1,0:T(8,128)(2,1)} %get-tuple-element.25), calls=%async_computation.3 | async-start | bytes 1048576 | tf_op jit(solution)/shard_map/all_to_all | solution.py:57
  94.3 7.2 %collective-permute-start.1 = (bf16[8,9,8,128]{3,2,1,0:T(8,128)(2,1)S(1)}, bf16[8,9,8,128]{3,2,1,0:T(8,128)(2,1)S(1)}, u32[]{:S(2)}, u32[]{:S(2)}) collective-permute-start(bf16[8,9,8,128]{3,2,1,0:T(8,128)(2,1)S(1)} %all_to_all.40), channel_id=1, source_target_pairs={{0,32},{32,0},{64,96},{96,64},{128,160},{160,128},{192,224},{224,1... | collective-permute-start | bytes 442376 | tf_op jit(solution)/shard_map/ppermute | solution.py:74
  101.5 21.3 %collective-permute-start.2 = (bf16[2,8,9,8,128]{4,3,2,1,0:T(8,128)(2,1)S(1)}, bf16[2,8,9,8,128]{4,3,2,1,0:T(8,128)(2,1)}, u32[]{:S(2)}, u32[]{:S(2)}) collective-permute-start(bf16[2,8,9,8,128]{4,3,2,1,0:T(8,128)(2,1)S(1)} %pad_maximum_fusion.1), channel_id=1, source_target_pairs={{0,64},{32,96},{64,0},{96,32},{128,192},{160,224},{192,128},{224,1... | collective-permute-start | bytes 884744 | tf_op jit(solution)/shard_map/ppermute | solution.py:74
  104.4 29.9 %all-to-all-start.4 = ((bf16[32,8,128]{2,1,0:T(8,128)(2,1)}), bf16[32,8,128]{2,1,0:T(8,128)(2,1)S(1)}, u32[]{:S(2)}, u32[]{:S(2)}) async-start(bf16[32,8,128]{2,1,0:T(8,128)(2,1)} %summed.1), calls=%async_computation.4 | async-start | bytes 131072 | tf_op jit(solution)/shard_map/all_to_all | solution.py:57
  123.8 37.3 %collective-permute-start.3 = (bf16[4,8,9,8,128]{4,3,2,1,0:T(8,128)(2,1)S(1)}, bf16[4,8,9,8,128]{4,3,2,1,0:T(8,128)(2,1)}, u32[]{:S(2)}, u32[]{:S(2)}) collective-permute-start(bf16[4,8,9,8,128]{4,3,2,1,0:T(8,128)(2,1)S(1)} %pad_maximum_fusion.refs_0_), channel_id=1, source_target_pairs={{0,8},{8,16},{16,24},{24,0},{1,9},{9,17},{17,25},{25,1},{2,10},{10... | collective-permute-start | bytes 1769480 | tf_op jit(solution)/shard_map/ppermute | solution.py:70
  134.9 32.9 %all-to-all-start.5 = ((bf16[32,8,128]{2,1,0:T(8,128)(2,1)}), bf16[32,8,128]{2,1,0:T(8,128)(2,1)S(1)}, u32[]{:S(2)}, u32[]{:S(2)}) async-start(bf16[32,8,128]{2,1,0:T(8,128)(2,1)} %get-tuple-element.26), calls=%async_computation.5 | async-start | bytes 131072 | tf_op jit(solution)/shard_map/all_to_all | solution.py:57
  156.9 17.2 %collective-permute-start.5 = (bf16[4,8,9,8,128]{4,3,2,1,0:T(8,128)(2,1)S(1)}, bf16[4,8,9,8,128]{4,3,2,1,0:T(8,128)(2,1)}, u32[]{:S(2)}, u32[]{:S(2)}) collective-permute-start(bf16[4,8,9,8,128]{4,3,2,1,0:T(8,128)(2,1)S(1)} %pad_maximum_fusion.refs_0_), channel_id=1, source_target_pairs={{0,24},{8,0},{16,8},{24,16},{1,25},{9,1},{17,9},{25,17},{2,26},{10... | collective-permute-start | bytes 1769480 | tf_op jit(solution)/shard_map/ppermute | solution.py:70
  161.1 16.6 %collective-permute-start.4 = (bf16[4,8,9,8,128]{4,3,2,1,0:T(8,128)(2,1)}, bf16[4,8,9,8,128]{4,3,2,1,0:T(8,128)(2,1)}, u32[]{:S(2)}, u32[]{:S(2)}) collective-permute-start(bf16[4,8,9,8,128]{4,3,2,1,0:T(8,128)(2,1)} %collective-permute-done.3.refs_1_), channel_id=1, source_target_pairs={{0,8},{8,16},{16,24},{24,0},{1,9},{9,17},{17,25},{25,1},{2,10},{10... | collective-permute-start | bytes 1769480 | tf_op jit(solution)/shard_map/ppermute | solution.py:70
  168.7 15.8 %all-to-all-start.6 = ((bf16[8,32,8,128]{3,2,1,0:T(8,128)(2,1)}), bf16[8,32,8,128]{3,2,1,0:T(8,128)(2,1)S(1)}, u32[]{:S(2)}, u32[]{:S(2)}) async-start(bf16[8,32,8,128]{3,2,1,0:T(8,128)(2,1)} %broadcast_in_dim.22), calls=%async_computation.6 | async-start | bytes 1048576 | tf_op jit(solution)/shard_map/all_to_all | solution.py:57
  186.1 11.3 %copy-start.3 = (f32[8,512]{1,0:T(8,128)S(1)}, f32[8,512]{1,0:T(8,128)}, u32[]{:S(2)}) copy-start(f32[8,512]{1,0:T(8,128)} %ov.1) | copy-start | bytes 49156
  186.1 11.3 %copy-start.4 = (f32[512,8]{0,1:T(8,128)S(1)}, f32[512,8]{0,1:T(8,128)}, u32[]{:S(2)}) copy-start(f32[512,8]{0,1:T(8,128)} %param.19) | copy-start | bytes 49156
  186.2 11.3 %collective-permute-start.6 = (bf16[8,4,4,8,1024]{4,3,2,1,0:T(8,128)(2,1)S(1)}, bf16[8,4,4,8,1024]{4,3,2,1,0:T(8,128)(2,1)S(1)}, u32[]{:S(2)}, u32[]{:S(2)}) collective-permute-start(bf16[8,4,4,8,1024]{4,3,2,1,0:T(8,128)(2,1)S(1)} %assemble.1.mine), channel_id=1, source_target_pairs={{0,4},{4,0},{1,5},{5,1},{2,6},{6,2},{3,7},{7,3},{8,12},{12,8},{9,1... | collective-permute-start | bytes 6291464 | tf_op jit(solution)/shard_map/ppermute | solution.py:70

commit v6 on v5

--- a/solution.py
+++ b/solution.py
@@ -10,6 +10,7 @@
 WIDTH = 2048
 R = 256
 FS = ("z", "x", "c")
+PLANE = ("x", "c", "tp")
 NZL = 4
 FIRST = 5
 LANES = 128
@@ -51,6 +52,16 @@
 def far_z(nz):
     n = nz // NZL
     return [[i + NZL * k for k in turned(n, FIRST)] for i in range(NZL)]
+
+
+def plane_groups(nx, nc, ny):
+    xs, ys = turned(nx, nx // 2), turned(ny, ny // 2)
+    at = lambda x, c, y: (x * nc + c) * ny + y
+    return (
+        [[at(x, c, y) for x in xs for y in ys] for c in range(nc)],
+        [[at(x, c, y) for x in xs for c in range(nc)] for y in range(ny)],
+        [[at(x, c, y) for y in ys] for x in range(nx) for c in range(nc)],
+    )
 
 
 def exchange(blocks, axes, groups=None):
@@ -85,7 +96,7 @@
     y = lax.axis_index("tp")
     j = lax.broadcasted_iota(jnp.int32, (R, R), 0)
     k = lax.broadcasted_iota(jnp.int32, (R, R), 1)
-    turn = (j == (k % n + FIRST * NZL) % n * 8 + k // n).astype(jnp.bfloat16)
+    turn = (j == ((k % n + FIRST * NZL) % n * 8 + (k // n + 4) % 8)).astype(jnp.bfloat16)
     for copy in copies:
         copy.wait()
     factor = jnp.where(y < 2, fv_in[...].astype(jnp.float32), fo_in[...].astype(jnp.float32))
@@ -134,7 +145,8 @@
                 for h in range(half):
                     for k, zl in enumerate(near_z(nzl)[0]):
                         lanes = slice(h * LANES, (h + 1) * LANES)
-                        block = src.at[x * 2 * half + f * half + h, k]
+                        y = (f * half + h + half) % (2 * half)
+                        block = src.at[(x + nx // 2) % nx * 2 * half + y, k]
                         whole[f, first:, zl, x, at, :, lanes] = block[: nzh - first]
                         whole[f, :first, zl, x, at, :, lanes] = block[nzh - first :]
     for f, (x, v) in enumerate(((xv, vv), (late, vo))):
@@ -412,13 +424,14 @@
     sizes = nzh, nzl, nx, nc
     ny = lax.axis_size("tp")
     around = [turned(nz, FIRST * NZL)]
+    over_xy, over_xc, over_y = plane_groups(nx, nc, ny)
     _, cols = weight_value.shape
 
     turned_weight = weight_output.T
     w = packed(nzh, factor_value, factor_output, weight_value, turned_weight)
     w = exchange(w, "z", far_z(nz))
     f = to_all(w[:, 0], "z", near_z(nz))
-    f = to_all(f, ("x", "tp"))
+    f = to_all(f, PLANE, over_xy)
     other = moved(f, "c", 1)
 
     get = swapped(w, "z", 1)
@@ -429,7 +442,7 @@
     terms, factors = projected_terms(
         f, other, normed_input, value_cotangent, layer_cotangent, gated_output, sizes
     )
-    t = exchange(terms, ("x", "c"))
+    t = exchange(terms, PLANE, over_xc)
     t = summed(t)
     t = exchange(t, "z", around)
     gram = gram_of(factors)
@@ -448,12 +461,12 @@
     d = exchange(d, "z", around)
 
     w2 = moved(w1, "x", 1)
-    d = to_all(d, ("x", "c"))
+    d = to_all(d, PLANE, over_xc)
     mine = assembled((w0, w1, w2, w3), sizes, d)
     flip = moved(mine, "c", 1)
 
     totals, directions = totals_of(ny, d.reshape(R, *d.shape[2:]), gram)
-    totals = exchange(totals, "tp")
+    totals = exchange(totals, PLANE, over_y)
 
     copy_value, copy_output, step_value, step_output, next_value, next_output = final(
         totals,

time: 201 us -> 198 us (0.985)
  blocking collectives: 80.4 us -> 76.6 us
    all_to_all x4, blocking collectives: 80.4 us -> 76.6 us  [exchange(): lax.all_to_all(blocks, axes, split_axis=0, concat_axis=0, axis_index_grou...]
    all_to_all x4, starting transfers between devices: 49.7 us -> 52.3 us  [exchange(): lax.all_to_all(blocks, axes, split_axis=0, concat_axis=0, axis_index_grou...]
    ppermute x5, waiting for transfers between devices: 5.86 us -> 3.55 us  [moved(): return lax.ppermute(block, axis, [(i, (i + by) % n) for i in range(n)])]
  transfers between devices with their start and end apart: 11 -> 11, of which waited for: 7 -> 6; matrix products, arithmetic and copies ran while one was open for 1% -> 1% of each run, Pallas kernels for 1% -> 1%
where the time goes in v6:
time: 198 us; the launch traced here: 197 us
  blocking collectives  76.6 us (39%)
  starting transfers between devices  73.4 us (37%)
  waiting for transfers between devices  29.4 us (15%)
  Pallas kernels  14.2 us (7%)
    all_to_all x4, blocking collectives, exchange(): lax.all_to_all(blocks, axes, split_axis=0, concat_axis=0, axis_index_grou...  76.6 us
    all_to_all x4, starting transfers between devices, exchange(): lax.all_to_all(blocks, axes, split_axis=0, concat_axis=0, axis_index_grou...  52.3 us
    all_to_all x4, waiting for transfers between devices, exchange(): lax.all_to_all(blocks, axes, split_axis=0, concat_axis=0, axis_index_grou...  20.9 us
    ppermute x5, starting transfers between devices, moved(): return lax.ppermute(block, axis, [(i, (i + by) % n) for i in range(n)])  17.2 us
    pallas_call x1, Pallas kernels, projected_terms(): pl.pallas_call(project_kernel, out_shape=(jax.ShapeDtypeStruct((nx * nc,...  5.6 us
    ppermute x2, waiting for transfers between devices, swapped(): lax.ppermute(block, axis, [(i, i ^ bit) for i in range(lax.axis_size(axis...  4.99 us
  transfers between devices with their start and end apart: 11, of which 6 were waited for; matrix products, arithmetic and copies ran while one was open for 1% of the time, Pallas kernels for 1%

profile of v6, /device:TPU:1, one launch (start us, length us, event | category | flops | bytes accessed | tf_op | source)
XLA Modules:
  0.0 196.8 jit_solution(8668197500006944251)
XLA Ops:
  0.7 1.1 packed.1
  1.8 45.6 %all_to_all.40 = bf16[8,9,8,128]{3,2,1,0:T(8,128)(2,1)S(1)} all-to-all(bf16[8,9,8,128]{3,2,1,0:T(8,128)(2,1)S(1)} %packed.1), channel_id=1, replica_groups={{640,768,896,0,128,256,384,512},{672,800,928,32,160,288,416,544},{704,8..., dimensions={0} | all-to-all | bytes 294912 | tf_op jit(solution)/shard_map/all_to_all | solution.py:68
  47.4 8.2 %all_to_all.41 = bf16[4,8,8,128]{3,2,1,0:T(8,128)(2,1)S(1)} all-to-all(bf16[4,8,8,128]{3,2,1,0:T(8,128)(2,1)S(1)} %broadcast_in_dim.9), channel_id=1, replica_groups={{32,0,64,96},{160,128,192,224},{288,256,320,352},{416,384,448,480},{544..., dimensions={0} | all-to-all | bytes 131072 | tf_op jit(solution)/shard_map/all_to_all | solution.py:68
  55.6 0.2 broadcast_in_dim.10
  55.9 16.9 %all_to_all.42.mine = bf16[16,4,8,8,128]{4,3,2,1,0:T(8,128)(2,1)S(1)} all-to-all(bf16[16,4,8,8,128]{4,3,2,1,0:T(8,128)(2,1)S(1)} %broadcast_in_dim.10), channel_id=1, replica_groups={{18,19,16,17,26,27,24,25,2,3,0,1,10,11,8,9},{22,23,20,21,30,31,28,29,6,..., dimensions={0} | all-to-all | bytes 2097152 | tf_op jit(solution)/shard_map/all_to_all | solution.py:68
  72.8 6.7 %collective-permute-start = (bf16[16,4,8,8,128]{4,3,2,1,0:T(8,128)(2,1)S(1)}, bf16[16,4,8,8,128]{4,3,2,1,0:T(8,128)(2,1)S(1)}, u32[]{:S(2)}, u32[]{:S(2)}) collective-permute-start(bf16[16,4,8,8,128]{4,3,2,1,0:T(8,128)(2,1)S(1)} %all_to_all.42.mine), channel_id=1, source_target_pairs={{0,4},{4,0},{1,5},{5,1},{2,6},{6,2},{3,7},{7,3},{8,12},{12,8},{9,1... | collective-permute-start | bytes 3145736 | tf_op jit(solution)/shard_map/ppermute | solution.py:81
  79.5 2.3 %collective-permute-done.other = bf16[16,4,8,8,128]{4,3,2,1,0:T(8,128)(2,1)S(1)} collective-permute-done((bf16[16,4,8,8,128]{4,3,2,1,0:T(8,128)(2,1)S(1)}, bf16[16,4,8,8,128]{4,3,2,1,0:T(8,128)(2,1)S(1)}, u32[]{:S(2)}, u32[]{:S(2)}) %collective-permute-start) | collective-permute-done | bytes 1048608 | tf_op jit(solution)/shard_map/ppermute | solution.py:81
  81.8 5.6 %project.1 = (bf16[8,32,1024]{2,1,0:T(8,128)(2,1)}, bf16[2,8,4,4,2,8,256]{6,5,4,3,2,1,0:T(8,128)(2,1)S(1)}) custom-call(bf16[16,4,8,8,128]{4,3,2,1,0:T(8,128)(2,1)S(1)} %all_to_all.42.mine, bf16[16,4,8,8,128]{4,3,2,1,0:T(8,128)(2,1)S(1)} %collective-permute-done.other, bf16[512,2048]{1,0:T(8,128)(2,1)S(1)} %copy-done, bf16[512,512]{1,0:T(8,128)(2,1)S(1)} %copy-done.1, ...), custom_call_target="tpu_custom_call" | custom-call | flops 1342177280 | bytes 10000000 | tf_op jit(solution)/shard_map/project/pallas_call | solution.py:165
  87.5 6.2 %all-to-all-start.3 = ((bf16[8,32,1024]{2,1,0:T(8,128)(2,1)}), bf16[8,32,1024]{2,1,0:T(8,128)(2,1)S(1)}, u32[]{:S(2)}, u32[]{:S(2)}) async-start(bf16[8,32,1024]{2,1,0:T(8,128)(2,1)} %get-tuple-element.25), calls=%async_computation.3 | async-start | bytes 1048576 | tf_op jit(solution)/shard_map/all_to_all | solution.py:68
  93.7 1.9 collective-permute-start.1
  95.6 5.0 %collective-permute-done.1 = bf16[8,9,8,128]{3,2,1,0:T(8,128)(2,1)S(1)} collective-permute-done((bf16[8,9,8,128]{3,2,1,0:T(8,128)(2,1)S(1)}, bf16[8,9,8,128]{3,2,1,0:T(8,128)(2,1)S(1)}, u32[]{:S(2)}, u32[]{:S(2)}) %collective-permute-start.1) | collective-permute-done | bytes 147488 | tf_op jit(solution)/shard_map/ppermute | solution.py:85
  100.6 2.0 %collective-permute-start.2 = (bf16[2,8,9,8,128]{4,3,2,1,0:T(8,128)(2,1)S(1)}, bf16[2,8,9,8,128]{4,3,2,1,0:T(8,128)(2,1)}, u32[]{:S(2)}, u32[]{:S(2)}) collective-permute-start(bf16[2,8,9,8,128]{4,3,2,1,0:T(8,128)(2,1)S(1)} %pad_maximum_fusion.1), channel_id=1, source_target_pairs={{0,64},{32,96},{64,0},{96,32},{128,192},{160,224},{192,128},{224,1... | collective-permute-start | bytes 884744 | tf_op jit(solution)/shard_map/ppermute | solution.py:85
  102.7 0.7 summed.1
  103.4 18.5 %all-to-all-start.4 = ((bf16[32,8,128]{2,1,0:T(8,128)(2,1)}), bf16[32,8,128]{2,1,0:T(8,128)(2,1)S(1)}, u32[]{:S(2)}, u32[]{:S(2)}) async-start(bf16[32,8,128]{2,1,0:T(8,128)(2,1)} %summed.1), calls=%async_computation.4 | async-start | bytes 131072 | tf_op jit(solution)/shard_map/all_to_all | solution.py:68
  122.0 1.0 pad_maximum_fusion.refs_0_
  123.0 1.9 collective-permute-start.3
  124.9 8.5 %all-to-all-done.4.t = bf16[32,8,128]{2,1,0:T(8,128)(2,1)S(1)} async-done(((bf16[32,8,128]{2,1,0:T(8,128)(2,1)}), bf16[32,8,128]{2,1,0:T(8,128)(2,1)S(1)}, u32[]{:S(2)}, u32[]{:S(2)}) %all-to-all-start.4) | async-done | bytes 65568 | tf_op jit(solution)/shard_map/all_to_all | solution.py:68
  133.4 0.7 moments.1
  134.1 21.9 %all-to-all-start.5 = ((bf16[32,8,128]{2,1,0:T(8,128)(2,1)}), bf16[32,8,128]{2,1,0:T(8,128)(2,1)S(1)}, u32[]{:S(2)}, u32[]{:S(2)}) async-start(bf16[32,8,128]{2,1,0:T(8,128)(2,1)} %get-tuple-element.26), calls=%async_computation.5 | async-start | bytes 131072 | tf_op jit(solution)/shard_map/all_to_all | solution.py:68
  156.1 2.2 %collective-permute-start.5 = (bf16[4,8,9,8,128]{4,3,2,1,0:T(8,128)(2,1)S(1)}, bf16[4,8,9,8,128]{4,3,2,1,0:T(8,128)(2,1)}, u32[]{:S(2)}, u32[]{:S(2)}) collective-permute-start(bf16[4,8,9,8,128]{4,3,2,1,0:T(8,128)(2,1)S(1)} %pad_maximum_fusion.refs_0_), channel_id=1, source_target_pairs={{0,24},{8,0},{16,8},{24,16},{1,25},{9,1},{17,9},{25,17},{2,26},{10... | collective-permute-start | bytes 1769480 | tf_op jit(solution)/shard_map/ppermute | solution.py:81
  158.2 3.1 %collective-permute-start.4 = (bf16[4,8,9,8,128]{4,3,2,1,0:T(8,128)(2,1)}, bf16[4,8,9,8,128]{4,3,2,1,0:T(8,128)(2,1)}, u32[]{:S(2)}, u32[]{:S(2)}) collective-permute-start(bf16[4,8,9,8,128]{4,3,2,1,0:T(8,128)(2,1)} %collective-permute-done.3.refs_1_), channel_id=1, source_target_pairs={{0,8},{8,16},{16,24},{24,0},{1,9},{9,17},{17,25},{25,1},{2,10},{10... | collective-permute-start | bytes 1769480 | tf_op jit(solution)/shard_map/ppermute | solution.py:81
  161.4 5.7 %all-to-all-done.5 = bf16[32,8,128]{2,1,0:T(8,128)(2,1)S(1)} async-done(((bf16[32,8,128]{2,1,0:T(8,128)(2,1)}), bf16[32,8,128]{2,1,0:T(8,128)(2,1)S(1)}, u32[]{:S(2)}, u32[]{:S(2)}) %all-to-all-start.5) | async-done | bytes 65568 | tf_op jit(solution)/shard_map/all_to_all | solution.py:68
  167.1 0.9 broadcast_in_dim.22
  168.0 5.6 %all-to-all-start.6 = ((bf16[8,32,8,128]{3,2,1,0:T(8,128)(2,1)}), bf16[8,32,8,128]{3,2,1,0:T(8,128)(2,1)S(1)}, u32[]{:S(2)}, u32[]{:S(2)}) async-start(bf16[8,32,8,128]{3,2,1,0:T(8,128)(2,1)} %broadcast_in_dim.22), calls=%async_computation.6 | async-start | bytes 1048576 | tf_op jit(solution)/shard_map/all_to_all | solution.py:68
  173.6 1.3 collective-permute-done.4.refs_2_
  174.9 6.7 %all-to-all-done.6.refs_4_ = bf16[8,32,8,128]{3,2,1,0:T(8,128)(2,1)S(1)} async-done(((bf16[8,32,8,128]{3,2,1,0:T(8,128)(2,1)}), bf16[8,32,8,128]{3,2,1,0:T(8,128)(2,1)S(1)}, u32[]{:S(2)}, u32[]{:S(2)}) %all-to-all-start.6) | async-done | bytes 524320 | tf_op jit(solution)/shard_map/all_to_all | solution.py:68
  181.5 1.6 assemble.1.mine
  183.1 3.3 %collective-permute-start.6 = (bf16[8,4,4,8,1024]{4,3,2,1,0:T(8,128)(2,1)S(1)}, bf16[8,4,4,8,1024]{4,3,2,1,0:T(8,128)(2,1)S(1)}, u32[]{:S(2)}, u32[]{:S(2)}) collective-permute-start(bf16[8,4,4,8,1024]{4,3,2,1,0:T(8,128)(2,1)S(1)} %assemble.1.mine), channel_id=1, source_target_pairs={{0,4},{4,0},{1,5},{5,1},{2,6},{6,2},{3,7},{7,3},{8,12},{12,8},{9,1... | collective-permute-start | bytes 6291464 | tf_op jit(solution)/shard_map/ppermute | solution.py:81
  186.4 0.8 gram.1
  187.2 0.8 totals.1
  188.0 5.8 %all_to_all.43.totals = f32[4,8,128]{2,1,0:T(8,128)S(1)} all-to-all(f32[4,8,128]{2,1,0:T(8,128)S(1)} %get-tuple-element.28), channel_id=1, replica_groups={{2,3,0,1},{6,7,4,5},{10,11,8,9},{14,15,12,13},{18,19,16,17},{22,23,20,2..., dimensions={0} | all-to-all | bytes 32768 | tf_op jit(solution)/shard_map/all_to_all | solution.py:68
  193.8 2.9 %final.1 = (bf16[8,4,4,2,8,512]{5,4,3,2,1,0:T(8,128)(2,1)}, bf16[512,2048]{1,0:T(8,128)(2,1)}, f32[8,512]{1,0:T(8,128)}, f32[8,512]{1,0:T(8,128)}, f32[8,512]{1,0:T(8,128)}, /*index=5*/f32[8,512]{1,0:T(8,128)}) custom-call(f32[4,8,128]{2,1,0:T(8,128)S(1)} %all_to_all.43.totals, bf16[2,256,512]{2,1,0:T(8,128)(2,1)S(1)} %get-tuple-element.29.directions, ...), custom_call_target="tpu_custom_call" | custom-call | flops 1073741824 | bytes 10000000 | tf_op jit(solution)/shard_map/final/pallas_call | solution.py:383
  (26 shorter events, 0.1 us)
Async XLA Ops:
  0.6 81.2 %copy-start.2 = (bf16[512,512]{1,0:T(8,128)(2,1)S(1)}, bf16[512,512]{1,0:T(8,128)(2,1)}, u32[]{:S(2)}) copy-start(bf16[512,512]{1,0:T(8,128)(2,1)} %vo.1) | copy-start | bytes 1572868
  0.7 81.1 %copy-start.1 = (bf16[512,512]{1,0:T(8,128)(2,1)S(1)}, bf16[512,512]{1,0:T(8,128)(2,1)}, u32[]{:S(2)}) copy-start(bf16[512,512]{1,0:T(8,128)(2,1)} %vv.1) | copy-start | bytes 1572868
  0.7 81.1 %copy-start = (bf16[512,2048]{1,0:T(8,128)(2,1)S(1)}, bf16[512,2048]{1,0:T(8,128)(2,1)}, u32[]{:S(2)}) copy-start(bf16[512,2048]{1,0:T(8,128)(2,1)} %xv.1) | copy-start | bytes 6291460
  72.8 9.0 %collective-permute-start = (bf16[16,4,8,8,128]{4,3,2,1,0:T(8,128)(2,1)S(1)}, bf16[16,4,8,8,128]{4,3,2,1,0:T(8,128)(2,1)S(1)}, u32[]{:S(2)}, u32[]{:S(2)}) collective-permute-start(bf16[16,4,8,8,128]{4,3,2,1,0:T(8,128)(2,1)S(1)} %all_to_all.42.mine), channel_id=1, source_target_pairs={{0,4},{4,0},{1,5},{5,1},{2,6},{6,2},{3,7},{7,3},{8,12},{12,8},{9,1... | collective-permute-start | bytes 3145736 | tf_op jit(solution)/shard_map/ppermute | solution.py:81
  87.4 46.0 %copy-start.5 = (f32[1,512]{1,0:T(1,128)S(1)}, f32[1,512]{1,0:T(1,128)}, u32[]{:S(2)}) copy-start(f32[1,512]{1,0:T(1,128)} %param.20) | copy-start | bytes 6148
  87.4 46.0 %copy-start.6 = (f32[1,512]{1,0:T(1,128)S(1)}, f32[1,512]{1,0:T(1,128)}, u32[]{:S(2)}) copy-start(f32[1,512]{1,0:T(1,128)} %param.21) | copy-start | bytes 6148
  87.4 46.0 %copy-start.7 = (f32[1,512]{1,0:T(1,128)S(1)}, f32[1,512]{1,0:T(1,128)}, u32[]{:S(2)}) copy-start(f32[1,512]{1,0:T(1,128)} %param.22) | copy-start | bytes 6148
  87.4 46.0 %copy-start.8 = (f32[1,512]{1,0:T(1,128)S(1)}, f32[1,512]{1,0:T(1,128)}, u32[]{:S(2)}) copy-start(f32[1,512]{1,0:T(1,128)} %param.23) | copy-start | bytes 6148
  87.5 15.2 %all-to-all-start.3 = ((bf16[8,32,1024]{2,1,0:T(8,128)(2,1)}), bf16[8,32,1024]{2,1,0:T(8,128)(2,1)S(1)}, u32[]{:S(2)}, u32[]{:S(2)}) async-start(bf16[8,32,1024]{2,1,0:T(8,128)(2,1)} %get-tuple-element.25), calls=%async_computation.3 | async-start | bytes 1048576 | tf_op jit(solution)/shard_map/all_to_all | solution.py:68
  93.7 6.9 %collective-permute-start.1 = (bf16[8,9,8,128]{3,2,1,0:T(8,128)(2,1)S(1)}, bf16[8,9,8,128]{3,2,1,0:T(8,128)(2,1)S(1)}, u32[]{:S(2)}, u32[]{:S(2)}) collective-permute-start(bf16[8,9,8,128]{3,2,1,0:T(8,128)(2,1)S(1)} %all_to_all.40), channel_id=1, source_target_pairs={{0,32},{32,0},{64,96},{96,64},{128,160},{160,128},{192,224},{224,1... | collective-permute-start | bytes 442376 | tf_op jit(solution)/shard_map/ppermute | solution.py:85
  100.6 21.3 %collective-permute-start.2 = (bf16[2,8,9,8,128]{4,3,2,1,0:T(8,128)(2,1)S(1)}, bf16[2,8,9,8,128]{4,3,2,1,0:T(8,128)(2,1)}, u32[]{:S(2)}, u32[]{:S(2)}) collective-permute-start(bf16[2,8,9,8,128]{4,3,2,1,0:T(8,128)(2,1)S(1)} %pad_maximum_fusion.1), channel_id=1, source_target_pairs={{0,64},{32,96},{64,0},{96,32},{128,192},{160,224},{192,128},{224,1... | collective-permute-start | bytes 884744 | tf_op jit(solution)/shard_map/ppermute | solution.py:85
  103.4 30.0 %all-to-all-start.4 = ((bf16[32,8,128]{2,1,0:T(8,128)(2,1)}), bf16[32,8,128]{2,1,0:T(8,128)(2,1)S(1)}, u32[]{:S(2)}, u32[]{:S(2)}) async-start(bf16[32,8,128]{2,1,0:T(8,128)(2,1)} %summed.1), calls=%async_computation.4 | async-start | bytes 131072 | tf_op jit(solution)/shard_map/all_to_all | solution.py:68
  123.0 35.3 %collective-permute-start.3 = (bf16[4,8,9,8,128]{4,3,2,1,0:T(8,128)(2,1)S(1)}, bf16[4,8,9,8,128]{4,3,2,1,0:T(8,128)(2,1)}, u32[]{:S(2)}, u32[]{:S(2)}) collective-permute-start(bf16[4,8,9,8,128]{4,3,2,1,0:T(8,128)(2,1)S(1)} %pad_maximum_fusion.refs_0_), channel_id=1, source_target_pairs={{0,8},{8,16},{16,24},{24,0},{1,9},{9,17},{17,25},{25,1},{2,10},{10... | collective-permute-start | bytes 1769480 | tf_op jit(solution)/shard_map/ppermute | solution.py:81
  134.1 33.0 %all-to-all-start.5 = ((bf16[32,8,128]{2,1,0:T(8,128)(2,1)}), bf16[32,8,128]{2,1,0:T(8,128)(2,1)S(1)}, u32[]{:S(2)}, u32[]{:S(2)}) async-start(bf16[32,8,128]{2,1,0:T(8,128)(2,1)} %get-tuple-element.26), calls=%async_computation.5 | async-start | bytes 131072 | tf_op jit(solution)/shard_map/all_to_all | solution.py:68
  156.1 17.5 %collective-permute-start.5 = (bf16[4,8,9,8,128]{4,3,2,1,0:T(8,128)(2,1)S(1)}, bf16[4,8,9,8,128]{4,3,2,1,0:T(8,128)(2,1)}, u32[]{:S(2)}, u32[]{:S(2)}) collective-permute-start(bf16[4,8,9,8,128]{4,3,2,1,0:T(8,128)(2,1)S(1)} %pad_maximum_fusion.refs_0_), channel_id=1, source_target_pairs={{0,24},{8,0},{16,8},{24,16},{1,25},{9,1},{17,9},{25,17},{2,26},{10... | collective-permute-start | bytes 1769480 | tf_op jit(solution)/shard_map/ppermute | solution.py:81
  158.2 16.6 %collective-permute-start.4 = (bf16[4,8,9,8,128]{4,3,2,1,0:T(8,128)(2,1)}, bf16[4,8,9,8,128]{4,3,2,1,0:T(8,128)(2,1)}, u32[]{:S(2)}, u32[]{:S(2)}) collective-permute-start(bf16[4,8,9,8,128]{4,3,2,1,0:T(8,128)(2,1)} %collective-permute-done.3.refs_1_), channel_id=1, source_target_pairs={{0,8},{8,16},{16,24},{24,0},{1,9},{9,17},{17,25},{25,1},{2,10},{10... | collective-permute-start | bytes 1769480 | tf_op jit(solution)/shard_map/ppermute | solution.py:81
  168.0 13.6 %all-to-all-start.6 = ((bf16[8,32,8,128]{3,2,1,0:T(8,128)(2,1)}), bf16[8,32,8,128]{3,2,1,0:T(8,128)(2,1)S(1)}, u32[]{:S(2)}, u32[]{:S(2)}) async-start(bf16[8,32,8,128]{3,2,1,0:T(8,128)(2,1)} %broadcast_in_dim.22), calls=%async_computation.6 | async-start | bytes 1048576 | tf_op jit(solution)/shard_map/all_to_all | solution.py:68
  183.1 10.7 %copy-start.3 = (f32[8,512]{1,0:T(8,128)S(1)}, f32[8,512]{1,0:T(8,128)}, u32[]{:S(2)}) copy-start(f32[8,512]{1,0:T(8,128)} %ov.1) | copy-start | bytes 49156
  183.1 10.7 %copy-start.4 = (f32[512,8]{0,1:T(8,128)S(1)}, f32[512,8]{0,1:T(8,128)}, u32[]{:S(2)}) copy-start(f32[512,8]{0,1:T(8,128)} %param.19) | copy-start | bytes 49156
  183.1 10.7 %collective-permute-start.6 = (bf16[8,4,4,8,1024]{4,3,2,1,0:T(8,128)(2,1)S(1)}, bf16[8,4,4,8,1024]{4,3,2,1,0:T(8,128)(2,1)S(1)}, u32[]{:S(2)}, u32[]{:S(2)}) collective-permute-start(bf16[8,4,4,8,1024]{4,3,2,1,0:T(8,128)(2,1)S(1)} %assemble.1.mine), channel_id=1, source_target_pairs={{0,4},{4,0},{1,5},{5,1},{2,6},{6,2},{3,7},{7,3},{8,12},{12,8},{9,1... | collective-permute-start | bytes 6291464 | tf_op jit(solution)/shard_map/ppermute | solution.py:81

commit v7 on v6

--- a/solution.py
+++ b/solution.py
@@ -62,6 +62,13 @@
         [[at(x, c, y) for x in xs for c in range(nc)] for y in range(ny)],
         [[at(x, c, y) for y in ys] for x in range(nx) for c in range(nc)],
     )
+
+
+def column_of(k, nzh):
+    slot = k // nzh % NZL
+    near = jnp.where(slot < 2, 1 - slot, slot)
+    z = (k % nzh + FIRST) % nzh * NZL + near
+    return z * 8 + (k // (nzh * NZL) + 4) % 8
 
 
 def exchange(blocks, axes, groups=None):
@@ -96,7 +103,7 @@
     y = lax.axis_index("tp")
     j = lax.broadcasted_iota(jnp.int32, (R, R), 0)
     k = lax.broadcasted_iota(jnp.int32, (R, R), 1)
-    turn = (j == ((k % n + FIRST * NZL) % n * 8 + (k // n + 4) % 8)).astype(jnp.bfloat16)
+    turn = (j == column_of(k, n // NZL)).astype(jnp.bfloat16)
     for copy in copies:
         copy.wait()
     factor = jnp.where(y < 2, fv_in[...].astype(jnp.float32), fo_in[...].astype(jnp.float32))
@@ -177,27 +184,47 @@
     )(mine, other, *near(xv, vv), *far(xo), *near(vo))
 
 
-def summed_kernel(t, out, lines):
-    total = jnp.sum(t[...].astype(jnp.float32), axis=0)
-    nz, tiles, _ = out.shape
-    for k in range(tiles):
-        lines[pl.ds(k, nz, stride=tiles), :] = total[:, k * LANES : (k + 1) * LANES]
-    out[...] = lines[...].reshape(out.shape).astype(jnp.bfloat16)
-
-
-def summed(t):
+def summed_kernel(t, out):
+    out[...] = jnp.sum(t[...].astype(jnp.float32), axis=0).reshape(out.shape)
+
+
+def summed(t, nzh):
     _, nz, width = t.shape
-    tiles = width // LANES
     return pl.pallas_call(
         summed_kernel,
-        out_shape=jax.ShapeDtypeStruct((nz, tiles, LANES), jnp.bfloat16),
+        out_shape=jax.ShapeDtypeStruct((nz // nzh, nzh, width), jnp.float32),
         in_specs=[VMEM],
         out_specs=VMEM,
-        scratch_shapes=[pltpu.VMEM((nz * tiles, LANES), jnp.float32)],
         name="summed",
         compiler_params=params(2),
         cost_estimate=cost(t.size, 600_000),
     )(t)
+
+
+def shared_kernel(t, fv, sv, fo, so, out):
+    total = jnp.sum(t[...], axis=0)
+    tiles = total.shape[1] // LANES
+    first = 0.9 * jnp.concatenate([fv[...], fo[...]], axis=0)
+    high = first.astype(jnp.bfloat16)
+    low = (first - high.astype(jnp.float32)).astype(jnp.bfloat16)
+    second = (0.95 * jnp.concatenate([sv[...], so[...]], axis=0)).astype(jnp.bfloat16)
+    blocks = [total[:, k * LANES : (k + 1) * LANES].astype(jnp.bfloat16) for k in range(tiles)]
+    for k, block in enumerate([*blocks, high, low, second]):
+        out[:, k] = jnp.broadcast_to(block[None], (out.shape[0], *block.shape))
+
+
+def shared(t, *state):
+    _, nzh, width = t.shape
+    shape = (nzh, width // LANES + 3, nzh, LANES)
+    return pl.pallas_call(
+        shared_kernel,
+        out_shape=jax.ShapeDtypeStruct(shape, jnp.bfloat16),
+        in_specs=[VMEM] * 5,
+        out_specs=VMEM,
+        name="shared",
+        compiler_params=params(2),
+        cost_estimate=cost(t.size, 400_000),
+    )(t, *state)
 
 
 def gram_kernel(factors, grams):
@@ -222,44 +249,58 @@
     )(*near(factors))
 
 
-def moments_kernel(t, fv, sv, fo, so, out, nfv, nsv, nfo, nso):
-    low = jnp.sum(t[...].astype(jnp.float32), axis=0)
-    half = low.shape[0] // 2
-    directions = []
-    for part, first, second, next_first, next_second in (
-        (low[:half], fv, sv, nfv, nsv),
-        (low[half:], fo, so, nfo, nso),
-    ):
-        a = 0.9 * first[...] + 0.1 * part
-        b = 0.95 * second[...] + 0.05 * part * part
-        next_first[...] = a
-        next_second[...] = b
-        directions.append(a * lax.rsqrt(b))
-    d = jnp.concatenate(directions, axis=0).astype(jnp.bfloat16)
-    out[...] = jnp.broadcast_to(d[None], out.shape)
+def moments_kernel(t, fv, sv, fo, so, out, nfv, nsv, nfo, nso, lines):
+    nzh = t.shape[0]
+    tiles = t.shape[1] - 3
+    states = []
+    for k in range(3):
+        lines[k] = t[:, tiles + k].astype(jnp.float32).reshape(nzh * tiles, LANES)
+        states.append([lines[k, pl.ds(s, nzh, stride=tiles), :] for s in range(tiles)])
+    mine = lax.rem(lax.axis_index("z") // NZL + nzh - FIRST, nzh)
+    here = lax.broadcasted_iota(jnp.int32, (nzh, LANES), 0) == mine
+    half = tiles // 2
+    for k in range(tiles):
+        low = jnp.sum(t[:, k].astype(jnp.float32), axis=0)
+        first = states[0][k] + states[1][k] + 0.1 * low
+        second = states[2][k] + 0.05 * low * low
+        d = (first * lax.rsqrt(second)).astype(jnp.bfloat16)
+        out[:, k] = jnp.broadcast_to(d[None], (out.shape[0], *d.shape))
+        own = jnp.sum(jnp.where(here, low, 0.0), axis=0, keepdims=True)
+        at = slice(k % half, k % half + 1)
+        f, s, nf, ns = (fv, sv, nfv, nsv) if k < half else (fo, so, nfo, nso)
+        nf[at] = 0.9 * f[at] + 0.1 * own
+        ns[at] = 0.95 * s[at] + 0.05 * own * own
 
 
 def moments(t, *state):
+    nzh, tiles = t.shape[0], t.shape[1] - 3
     shape = jax.ShapeDtypeStruct(state[0].shape, jnp.float32)
     return pl.pallas_call(
         moments_kernel,
-        out_shape=(jax.ShapeDtypeStruct(t.shape, jnp.bfloat16), shape, shape, shape, shape),
+        out_shape=(
+            jax.ShapeDtypeStruct((NZL, tiles, nzh, LANES), jnp.bfloat16),
+            shape,
+            shape,
+            shape,
+            shape,
+        ),
         in_specs=[VMEM] * 5,
         out_specs=(VMEM,) * 5,
+        scratch_shapes=[pltpu.VMEM((3, nzh * tiles, LANES), jnp.float32)],
         name="moments",
         compiler_params=params(2),
-        cost_estimate=cost(100_000, 150_000),
+        cost_estimate=cost(300_000, 400_000),
     )(t, *state)
 
 
-def total_kernel(d, gram, out, whole, lines):
+def total_kernel(d, gram, out, whole):
     tiles = d.shape[1]
     half = tiles // 2
-    lines[...] = d[...].astype(jnp.float32).reshape(lines.shape)
-    parts = [lines[pl.ds(k, R, stride=tiles), :].astype(jnp.bfloat16) for k in range(tiles)]
     rows = out.shape[1] // 2
     for f in range(2):
-        part = jnp.concatenate(parts[f * half : (f + 1) * half], axis=1)
+        part = jnp.concatenate(
+            [d[:, k].reshape(R, LANES) for k in range(f * half, (f + 1) * half)], axis=1
+        )
         whole[f] = part
         square = part.astype(jnp.float32) * (dot(gram[f, 0], part) + dot(gram[f, 1], part))
         out[:, f * rows : (f + 1) * rows] = jnp.full(
@@ -268,7 +309,7 @@
 
 
 def totals_of(count, d, gram):
-    _, tiles, _ = d.shape
+    tiles = d.shape[1]
     cols = tiles // 2 * LANES
     return pl.pallas_call(
         total_kernel,
@@ -278,7 +319,6 @@
         ),
         in_specs=[VMEM, VMEM],
         out_specs=(VMEM, VMEM),
-        scratch_shapes=[pltpu.VMEM((R * tiles, LANES), jnp.float32)],
         name="totals",
         compiler_params=params(6),
         cost_estimate=cost(8 * R * R * cols, 2_000_000),
@@ -294,16 +334,16 @@
     for k, s, part in parts:
         px = lax.rem(x + nx - k, nx)
         at = lax.bitwise_xor(zl, s)
-        for t in range(part.shape[1] - 1):
+        for t in range(part.shape[1]):
             lanes = slice(t * LANES, (t + 1) * LANES)
-            out[first:, at, px, :, lanes] = part[: nzh - first, 1 + t]
-            out[:first, at, px, :, lanes] = part[nzh - first :, 1 + t]
+            out[first:, at, px, :, lanes] = part[: nzh - first, t]
+            out[:first, at, px, :, lanes] = part[nzh - first :, t]
 
 
 def assembled(parts, sizes, after):
     nzh, nzl, nx, _ = sizes
     tiles, rows = parts[0].shape[2:4]
-    shape = (nzh, nzl, nx, rows, (tiles - 1) * LANES)
+    shape = (nzh, nzl, nx, rows, tiles * LANES)
     return pl.pallas_call(
         assemble_kernel,
         out_shape=jax.ShapeDtypeStruct(shape, jnp.bfloat16),
@@ -423,7 +463,6 @@
     nzh, nzl = nz // NZL, NZL
     sizes = nzh, nzl, nx, nc
     ny = lax.axis_size("tp")
-    around = [turned(nz, FIRST * NZL)]
     over_xy, over_xc, over_y = plane_groups(nx, nc, ny)
     _, cols = weight_value.shape
 
@@ -437,35 +476,33 @@
     get = swapped(w, "z", 1)
     w = jnp.stack([w, get])
     get = swapped(w, "z", 2)
-    w0 = jnp.concatenate([w, get])
+    w0 = jnp.concatenate([w[:, :, 1:], get[:, :, 1:]])
 
     terms, factors = projected_terms(
         f, other, normed_input, value_cotangent, layer_cotangent, gated_output, sizes
     )
     t = exchange(terms, PLANE, over_xc)
-    t = summed(t)
-    t = exchange(t, "z", around)
-    gram = gram_of(factors)
-
+    t = summed(t, nzh)
     w1 = moved(w0, "x", 1)
     w3 = moved(w0, "x", nx - 1)
+    t = exchange(t, "z", near_z(nz))
 
     narrow = (cols // LANES, LANES)
-    d, *state = moments(
-        t,
-        *(s.reshape(narrow) for s in (first_value, second_value, first_output, second_output)),
-    )
+    state = [s.reshape(narrow) for s in (first_value, second_value, first_output, second_output)]
+    t = shared(t, *state)
+    t = exchange(t, "z", far_z(nz))
+    w2 = moved(w1, "x", 1)
+    gram = gram_of(factors)
+    d, *state = moments(t, *state)
     next_first_value, next_second_value, next_first_output, next_second_output = (
         s.reshape(1, cols) for s in state
     )
-    d = exchange(d, "z", around)
-
-    w2 = moved(w1, "x", 1)
+    d = exchange(d, "z", near_z(nz))
     d = to_all(d, PLANE, over_xc)
     mine = assembled((w0, w1, w2, w3), sizes, d)
     flip = moved(mine, "c", 1)
 
-    totals, directions = totals_of(ny, d.reshape(R, *d.shape[2:]), gram)
+    totals, directions = totals_of(ny, d.reshape(-1, *d.shape[2:]), gram)
     totals = exchange(totals, PLANE, over_y)
 
     copy_value, copy_output, step_value, step_output, next_value, next_output = final(

time: 198 us -> 212 us (1.071); the launches traced: 197 us -> 208 us
  blocking collectives: 76.6 us -> 95.9 us
  starting transfers between devices: 73.4 us -> 58.6 us
  waiting for transfers between devices: 29.4 us -> 39.5 us
  Pallas kernels: 14.2 us -> 11.9 us
    ppermute x2, waiting for transfers between devices: 4.99 us -> 26.7 us  [swapped(): lax.ppermute(block, axis, [(i, i ^ bit) for i in range(lax.axis_size(axis...]
    all_to_all x4 -> x6, blocking collectives: 76.6 us -> 95.9 us  [exchange(): lax.all_to_all(blocks, axes, split_axis=0, concat_axis=0, axis_index_grou...]
    all_to_all x4 -> x3, starting transfers between devices: 52.3 us -> 33.8 us  [exchange(): lax.all_to_all(blocks, axes, split_axis=0, concat_axis=0, axis_index_grou...]
    all_to_all x4 -> x3, waiting for transfers between devices: 20.9 us -> 7.98 us  [exchange(): lax.all_to_all(blocks, axes, split_axis=0, concat_axis=0, axis_index_grou...]
    ppermute x2, starting transfers between devices: 3.93 us -> 6.32 us  [swapped(): lax.ppermute(block, axis, [(i, i ^ bit) for i in range(lax.axis_size(axis...]
    pallas_call x1, Pallas kernels: 5.6 us -> 3.44 us  [projected_terms(): pl.pallas_call(project_kernel, out_shape=(jax.ShapeDtypeStruct((nx * nc,...]
  transfers between devices with their start and end apart: 11 -> 10, of which waited for: 6 -> 6; matrix products, arithmetic and copies ran while one was open for 1% -> 0% of each run, Pallas kernels for 1% -> 1%
where the time goes in v7:
time: 212 us; the launch traced here: 208 us
  blocking collectives  95.9 us (45%)
  starting transfers between devices  58.6 us (28%)
  waiting for transfers between devices  39.5 us (19%)
  Pallas kernels  11.9 us (6%)
    all_to_all x6, blocking collectives, exchange(): lax.all_to_all(blocks, axes, split_axis=0, concat_axis=0, axis_index_grou...  95.9 us
    all_to_all x3, starting transfers between devices, exchange(): lax.all_to_all(blocks, axes, split_axis=0, concat_axis=0, axis_index_grou...  33.8 us
    ppermute x2, waiting for transfers between devices, swapped(): lax.ppermute(block, axis, [(i, i ^ bit) for i in range(lax.axis_size(axis...  26.7 us
    ppermute x5, starting transfers between devices, moved(): return lax.ppermute(block, axis, [(i, (i + by) % n) for i in range(n)])  18.5 us
    all_to_all x3, waiting for transfers between devices, exchange(): lax.all_to_all(blocks, axes, split_axis=0, concat_axis=0, axis_index_grou...  7.98 us
    ppermute x2, starting transfers between devices, swapped(): lax.ppermute(block, axis, [(i, i ^ bit) for i in range(lax.axis_size(axis...  6.32 us
    ppermute x5, waiting for transfers between devices, moved(): return lax.ppermute(block, axis, [(i, (i + by) % n) for i in range(n)])  4.82 us
  transfers between devices with their start and end apart: 10, of which 6 were waited for; matrix products, arithmetic and copies ran while one was open for 0% of the time, Pallas kernels for 1%

profile of v7, /device:TPU:1, one launch (start us, length us, event | category | flops | bytes accessed | tf_op | source)
XLA Modules:
  0.0 208.2 jit_solution(12209588361140610715)
XLA Ops:
  0.7 1.1 packed.1
  1.8 45.6 %all_to_all.45 = bf16[8,9,8,128]{3,2,1,0:T(8,128)(2,1)S(1)} all-to-all(bf16[8,9,8,128]{3,2,1,0:T(8,128)(2,1)S(1)} %packed.1), channel_id=1, replica_groups={{640,768,896,0,128,256,384,512},{672,800,928,32,160,288,416,544},{704,8..., dimensions={0} | all-to-all | bytes 294912 | tf_op jit(solution)/shard_map/all_to_all | solution.py:75
  47.4 8.2 %all_to_all.46 = bf16[4,8,8,128]{3,2,1,0:T(8,128)(2,1)S(1)} all-to-all(bf16[4,8,8,128]{3,2,1,0:T(8,128)(2,1)S(1)} %broadcast_in_dim.9), channel_id=1, replica_groups={{32,0,64,96},{160,128,192,224},{288,256,320,352},{416,384,448,480},{544..., dimensions={0} | all-to-all | bytes 131072 | tf_op jit(solution)/shard_map/all_to_all | solution.py:75
  55.6 0.2 broadcast_in_dim.10
  55.9 16.9 %all_to_all.47.mine = bf16[16,4,8,8,128]{4,3,2,1,0:T(8,128)(2,1)S(1)} all-to-all(bf16[16,4,8,8,128]{4,3,2,1,0:T(8,128)(2,1)S(1)} %broadcast_in_dim.10), channel_id=1, replica_groups={{18,19,16,17,26,27,24,25,2,3,0,1,10,11,8,9},{22,23,20,21,30,31,28,29,6,..., dimensions={0} | all-to-all | bytes 2097152 | tf_op jit(solution)/shard_map/all_to_all | solution.py:75
  72.8 6.8 %collective-permute-start = (bf16[16,4,8,8,128]{4,3,2,1,0:T(8,128)(2,1)S(1)}, bf16[16,4,8,8,128]{4,3,2,1,0:T(8,128)(2,1)S(1)}, u32[]{:S(2)}, u32[]{:S(2)}) collective-permute-start(bf16[16,4,8,8,128]{4,3,2,1,0:T(8,128)(2,1)S(1)} %all_to_all.47.mine), channel_id=1, source_target_pairs={{0,4},{4,0},{1,5},{5,1},{2,6},{6,2},{3,7},{7,3},{8,12},{12,8},{9,1... | collective-permute-start | bytes 3145736 | tf_op jit(solution)/shard_map/ppermute | solution.py:88
  79.7 2.3 %collective-permute-done.other = bf16[16,4,8,8,128]{4,3,2,1,0:T(8,128)(2,1)S(1)} collective-permute-done((bf16[16,4,8,8,128]{4,3,2,1,0:T(8,128)(2,1)S(1)}, bf16[16,4,8,8,128]{4,3,2,1,0:T(8,128)(2,1)S(1)}, u32[]{:S(2)}, u32[]{:S(2)}) %collective-permute-start) | collective-permute-done | bytes 1048608 | tf_op jit(solution)/shard_map/ppermute | solution.py:88
  82.0 3.4 %project.1 = (bf16[8,32,1024]{2,1,0:T(8,128)(2,1)S(1)}, bf16[2,8,4,4,2,8,256]{6,5,4,3,2,1,0:T(8,128)(2,1)S(1)}) custom-call(bf16[16,4,8,8,128]{4,3,2,1,0:T(8,128)(2,1)S(1)} %all_to_all.47.mine, bf16[16,4,8,8,128]{4,3,2,1,0:T(8,128)(2,1)S(1)} %collective-permute-done.other, bf16[512,2048]{1,0:T(8,128)(2,1)S(1)} %copy-done, bf16[512,512]{1,0:T(8,128)(2,1)S(1)} %copy-done.1, ...), custom_call_target="tpu_custom_call" | custom-call | flops 1342177280 | bytes 10000000 | tf_op jit(solution)/shard_map/project/pallas_call | solution.py:172
  85.4 12.1 %all_to_all.48.t = bf16[8,32,1024]{2,1,0:T(8,128)(2,1)S(1)} all-to-all(bf16[8,32,1024]{2,1,0:T(8,128)(2,1)S(1)} %get-tuple-element.25), channel_id=1, replica_groups={{16,20,24,28,0,4,8,12},{17,21,25,29,1,5,9,13},{18,22,26,30,2,6,10,14},{..., dimensions={0} | all-to-all | bytes 1048576 | tf_op jit(solution)/shard_map/all_to_all | solution.py:75
  97.5 6.9 %all_to_all.49.t = f32[4,8,1024]{2,1,0:T(8,128)S(1)} all-to-all(f32[4,8,1024]{2,1,0:T(8,128)S(1)} %summed.1), channel_id=1, replica_groups={{32,0,64,96},{160,128,192,224},{288,256,320,352},{416,384,448,480},{544..., dimensions={0} | all-to-all | bytes 262144 | tf_op jit(solution)/shard_map/all_to_all | solution.py:75
  104.5 0.7 shared.1
  105.2 18.2 %all-to-all-start.5 = ((bf16[8,11,8,128]{3,2,1,0:T(8,128)(2,1)}), bf16[8,11,8,128]{3,2,1,0:T(8,128)(2,1)S(1)}, u32[]{:S(2)}, u32[]{:S(2)}) async-start(bf16[8,11,8,128]{3,2,1,0:T(8,128)(2,1)} %shared.1), calls=%async_computation.5 | async-start | bytes 360448 | tf_op jit(solution)/shard_map/all_to_all | solution.py:75
  123.4 1.9 collective-permute-start.1
  125.3 14.9 %collective-permute-done.1 = bf16[8,9,8,128]{3,2,1,0:T(8,128)(2,1)S(1)} collective-permute-done((bf16[8,9,8,128]{3,2,1,0:T(8,128)(2,1)S(1)}, bf16[8,9,8,128]{3,2,1,0:T(8,128)(2,1)S(1)}, u32[]{:S(2)}, u32[]{:S(2)}) %collective-permute-start.1) | collective-permute-done | bytes 147488 | tf_op jit(solution)/shard_map/ppermute | solution.py:92
  140.3 4.4 %collective-permute-start.2 = (bf16[2,8,9,8,128]{4,3,2,1,0:T(8,128)(2,1)S(1)}, bf16[2,8,9,8,128]{4,3,2,1,0:T(8,128)(2,1)S(1)}, u32[]{:S(2)}, u32[]{:S(2)}) collective-permute-start(bf16[2,8,9,8,128]{4,3,2,1,0:T(8,128)(2,1)S(1)} %pad_maximum_fusion.1), channel_id=1, source_target_pairs={{0,64},{32,96},{64,0},{96,32},{128,192},{160,224},{192,128},{224,1... | collective-permute-start | bytes 884744 | tf_op jit(solution)/shard_map/ppermute | solution.py:92
  144.7 11.8 %collective-permute-done.2 = bf16[2,8,9,8,128]{4,3,2,1,0:T(8,128)(2,1)S(1)} collective-permute-done((bf16[2,8,9,8,128]{4,3,2,1,0:T(8,128)(2,1)S(1)}, bf16[2,8,9,8,128]{4,3,2,1,0:T(8,128)(2,1)S(1)}, u32[]{:S(2)}, u32[]{:S(2)}) %collective-permute-start.2) | collective-permute-done | bytes 294944 | tf_op jit(solution)/shard_map/ppermute | solution.py:92
  156.6 2.0 collective-permute-start.3
  158.6 0.7 moments.1
  159.3 6.7 %all-to-all-start.6 = ((bf16[4,8,8,128]{3,2,1,0:T(8,128)(2,1)}), bf16[4,8,8,128]{3,2,1,0:T(8,128)(2,1)S(1)}, u32[]{:S(2)}, u32[]{:S(2)}) async-start(bf16[4,8,8,128]{3,2,1,0:T(8,128)(2,1)} %get-tuple-element.26), calls=%async_computation.6 | async-start | bytes 131072 | tf_op jit(solution)/shard_map/all_to_all | solution.py:75
  166.0 4.5 %collective-permute-start.5 = (bf16[4,8,8,8,128]{4,3,2,1,0:T(8,128)(2,1)S(1)}, bf16[4,8,8,8,128]{4,3,2,1,0:T(8,128)(2,1)}, u32[]{:S(2)}, u32[]{:S(2)}) collective-permute-start(bf16[4,8,8,8,128]{4,3,2,1,0:T(8,128)(2,1)S(1)} %pad_maximum_fusion.refs_0_), channel_id=1, source_target_pairs={{0,24},{8,0},{16,8},{24,16},{1,25},{9,1},{17,9},{25,17},{2,26},{10... | collective-permute-start | bytes 1572872 | tf_op jit(solution)/shard_map/ppermute | solution.py:88
  170.5 0.3 collective-permute-done.3.refs_1_
  170.9 1.9 collective-permute-start.4
  172.8 0.9 broadcast_in_dim.22
  173.7 8.8 %all-to-all-start.7 = ((bf16[8,4,8,8,128]{4,3,2,1,0:T(8,128)(2,1)}), bf16[8,4,8,8,128]{4,3,2,1,0:T(8,128)(2,1)S(1)}, u32[]{:S(2)}, u32[]{:S(2)}) async-start(bf16[8,4,8,8,128]{4,3,2,1,0:T(8,128)(2,1)} %broadcast_in_dim.22), calls=%async_computation.7 | async-start | bytes 1048576 | tf_op jit(solution)/shard_map/all_to_all | solution.py:75
  182.6 2.2 %collective-permute-done.4.refs_2_ = bf16[4,8,8,8,128]{4,3,2,1,0:T(8,128)(2,1)} collective-permute-done((bf16[4,8,8,8,128]{4,3,2,1,0:T(8,128)(2,1)}, bf16[4,8,8,8,128]{4,3,2,1,0:T(8,128)(2,1)}, u32[]{:S(2)}, u32[]{:S(2)}) %collective-permute-start.4) | collective-permute-done | bytes 524320 | tf_op jit(solution)/shard_map/ppermute | solution.py:88
  184.8 8.0 %all-to-all-done.7.refs_4_ = bf16[8,4,8,8,128]{4,3,2,1,0:T(8,128)(2,1)S(1)} async-done(((bf16[8,4,8,8,128]{4,3,2,1,0:T(8,128)(2,1)}), bf16[8,4,8,8,128]{4,3,2,1,0:T(8,128)(2,1)S(1)}, u32[]{:S(2)}, u32[]{:S(2)}) %all-to-all-start.7) | async-done | bytes 524320 | tf_op jit(solution)/shard_map/all_to_all | solution.py:75
  192.8 1.5 assemble.1.mine
  194.3 3.3 %collective-permute-start.6 = (bf16[8,4,4,8,1024]{4,3,2,1,0:T(8,128)(2,1)S(1)}, bf16[8,4,4,8,1024]{4,3,2,1,0:T(8,128)(2,1)S(1)}, u32[]{:S(2)}, u32[]{:S(2)}) collective-permute-start(bf16[8,4,4,8,1024]{4,3,2,1,0:T(8,128)(2,1)S(1)} %assemble.1.mine), channel_id=1, source_target_pairs={{0,4},{4,0},{1,5},{5,1},{2,6},{6,2},{3,7},{7,3},{8,12},{12,8},{9,1... | collective-permute-start | bytes 6291464 | tf_op jit(solution)/shard_map/ppermute | solution.py:88
  197.6 0.8 gram.1
  198.4 0.6 totals.1
  199.0 6.2 %all_to_all.50.totals = f32[4,8,128]{2,1,0:T(8,128)S(1)} all-to-all(f32[4,8,128]{2,1,0:T(8,128)S(1)} %get-tuple-element.28), channel_id=1, replica_groups={{2,3,0,1},{6,7,4,5},{10,11,8,9},{14,15,12,13},{18,19,16,17},{22,23,20,2..., dimensions={0} | all-to-all | bytes 32768 | tf_op jit(solution)/shard_map/all_to_all | solution.py:75
  205.2 2.9 %final.1 = (bf16[8,4,4,2,8,512]{5,4,3,2,1,0:T(8,128)(2,1)}, bf16[512,2048]{1,0:T(8,128)(2,1)}, f32[8,512]{1,0:T(8,128)}, f32[8,512]{1,0:T(8,128)}, f32[8,512]{1,0:T(8,128)}, /*index=5*/f32[8,512]{1,0:T(8,128)}) custom-call(f32[4,8,128]{2,1,0:T(8,128)S(1)} %all_to_all.50.totals, bf16[2,256,512]{2,1,0:T(8,128)(2,1)S(1)} %get-tuple-element.29.directions, ...), custom_call_target="tpu_custom_call" | custom-call | flops 1073741824 | bytes 10000000 | tf_op jit(solution)/shard_map/final/pallas_call | solution.py:423
  (29 shorter events, 0.3 us)
Async XLA Ops:
  0.6 81.3 %copy-start.2 = (bf16[512,512]{1,0:T(8,128)(2,1)S(1)}, bf16[512,512]{1,0:T(8,128)(2,1)}, u32[]{:S(2)}) copy-start(bf16[512,512]{1,0:T(8,128)(2,1)} %vo.1) | copy-start | bytes 1572868
  0.7 81.3 %copy-start.1 = (bf16[512,512]{1,0:T(8,128)(2,1)S(1)}, bf16[512,512]{1,0:T(8,128)(2,1)}, u32[]{:S(2)}) copy-start(bf16[512,512]{1,0:T(8,128)(2,1)} %vv.1) | copy-start | bytes 1572868
  0.7 81.3 %copy-start = (bf16[512,2048]{1,0:T(8,128)(2,1)S(1)}, bf16[512,2048]{1,0:T(8,128)(2,1)}, u32[]{:S(2)}) copy-start(bf16[512,2048]{1,0:T(8,128)(2,1)} %xv.1) | copy-start | bytes 6291460
  72.8 31.6 %copy-start.5 = (f32[1,512]{1,0:T(1,128)S(1)}, f32[1,512]{1,0:T(1,128)}, u32[]{:S(2)}) copy-start(f32[1,512]{1,0:T(1,128)} %param.20) | copy-start | bytes 6148
  72.8 31.6 %copy-start.6 = (f32[1,512]{1,0:T(1,128)S(1)}, f32[1,512]{1,0:T(1,128)}, u32[]{:S(2)}) copy-start(f32[1,512]{1,0:T(1,128)} %param.21) | copy-start | bytes 6148
  72.8 31.6 %copy-start.7 = (f32[1,512]{1,0:T(1,128)S(1)}, f32[1,512]{1,0:T(1,128)}, u32[]{:S(2)}) copy-start(f32[1,512]{1,0:T(1,128)} %param.22) | copy-start | bytes 6148
  72.8 31.6 %copy-start.8 = (f32[1,512]{1,0:T(1,128)S(1)}, f32[1,512]{1,0:T(1,128)}, u32[]{:S(2)}) copy-start(f32[1,512]{1,0:T(1,128)} %param.23) | copy-start | bytes 6148
  72.8 9.1 %collective-permute-start = (bf16[16,4,8,8,128]{4,3,2,1,0:T(8,128)(2,1)S(1)}, bf16[16,4,8,8,128]{4,3,2,1,0:T(8,128)(2,1)S(1)}, u32[]{:S(2)}, u32[]{:S(2)}) collective-permute-start(bf16[16,4,8,8,128]{4,3,2,1,0:T(8,128)(2,1)S(1)} %all_to_all.47.mine), channel_id=1, source_target_pairs={{0,4},{4,0},{1,5},{5,1},{2,6},{6,2},{3,7},{7,3},{8,12},{12,8},{9,1... | collective-permute-start | bytes 3145736 | tf_op jit(solution)/shard_map/ppermute | solution.py:88
  105.2 53.4 %all-to-all-start.5 = ((bf16[8,11,8,128]{3,2,1,0:T(8,128)(2,1)}), bf16[8,11,8,128]{3,2,1,0:T(8,128)(2,1)S(1)}, u32[]{:S(2)}, u32[]{:S(2)}) async-start(bf16[8,11,8,128]{3,2,1,0:T(8,128)(2,1)} %shared.1), calls=%async_computation.5 | async-start | bytes 360448 | tf_op jit(solution)/shard_map/all_to_all | solution.py:75
  123.4 16.8 %collective-permute-start.1 = (bf16[8,9,8,128]{3,2,1,0:T(8,128)(2,1)S(1)}, bf16[8,9,8,128]{3,2,1,0:T(8,128)(2,1)S(1)}, u32[]{:S(2)}, u32[]{:S(2)}) collective-permute-start(bf16[8,9,8,128]{3,2,1,0:T(8,128)(2,1)S(1)} %all_to_all.45), channel_id=1, source_target_pairs={{0,32},{32,0},{64,96},{96,64},{128,160},{160,128},{192,224},{224,1... | collective-permute-start | bytes 442376 | tf_op jit(solution)/shard_map/ppermute | solution.py:92
  140.3 16.3 %collective-permute-start.2 = (bf16[2,8,9,8,128]{4,3,2,1,0:T(8,128)(2,1)S(1)}, bf16[2,8,9,8,128]{4,3,2,1,0:T(8,128)(2,1)S(1)}, u32[]{:S(2)}, u32[]{:S(2)}) collective-permute-start(bf16[2,8,9,8,128]{4,3,2,1,0:T(8,128)(2,1)S(1)} %pad_maximum_fusion.1), channel_id=1, source_target_pairs={{0,64},{32,96},{64,0},{96,32},{128,192},{160,224},{192,128},{224,1... | collective-permute-start | bytes 884744 | tf_op jit(solution)/shard_map/ppermute | solution.py:92
  156.6 14.3 %collective-permute-start.3 = (bf16[4,8,8,8,128]{4,3,2,1,0:T(8,128)(2,1)S(1)}, bf16[4,8,8,8,128]{4,3,2,1,0:T(8,128)(2,1)}, u32[]{:S(2)}, u32[]{:S(2)}) collective-permute-start(bf16[4,8,8,8,128]{4,3,2,1,0:T(8,128)(2,1)S(1)} %pad_maximum_fusion.refs_0_), channel_id=1, source_target_pairs={{0,8},{8,16},{16,24},{24,0},{1,9},{9,17},{17,25},{25,1},{2,10},{10... | collective-permute-start | bytes 1572872 | tf_op jit(solution)/shard_map/ppermute | solution.py:88
  159.3 13.5 %all-to-all-start.6 = ((bf16[4,8,8,128]{3,2,1,0:T(8,128)(2,1)}), bf16[4,8,8,128]{3,2,1,0:T(8,128)(2,1)S(1)}, u32[]{:S(2)}, u32[]{:S(2)}) async-start(bf16[4,8,8,128]{3,2,1,0:T(8,128)(2,1)} %get-tuple-element.26), calls=%async_computation.6 | async-start | bytes 131072 | tf_op jit(solution)/shard_map/all_to_all | solution.py:75
  166.0 16.5 %collective-permute-start.5 = (bf16[4,8,8,8,128]{4,3,2,1,0:T(8,128)(2,1)S(1)}, bf16[4,8,8,8,128]{4,3,2,1,0:T(8,128)(2,1)}, u32[]{:S(2)}, u32[]{:S(2)}) collective-permute-start(bf16[4,8,8,8,128]{4,3,2,1,0:T(8,128)(2,1)S(1)} %pad_maximum_fusion.refs_0_), channel_id=1, source_target_pairs={{0,24},{8,0},{16,8},{24,16},{1,25},{9,1},{17,9},{25,17},{2,26},{10... | collective-permute-start | bytes 1572872 | tf_op jit(solution)/shard_map/ppermute | solution.py:88
  170.9 13.9 %collective-permute-start.4 = (bf16[4,8,8,8,128]{4,3,2,1,0:T(8,128)(2,1)}, bf16[4,8,8,8,128]{4,3,2,1,0:T(8,128)(2,1)}, u32[]{:S(2)}, u32[]{:S(2)}) collective-permute-start(bf16[4,8,8,8,128]{4,3,2,1,0:T(8,128)(2,1)} %collective-permute-done.3.refs_1_), channel_id=1, source_target_pairs={{0,8},{8,16},{16,24},{24,0},{1,9},{9,17},{17,25},{25,1},{2,10},{10... | collective-permute-start | bytes 1572872 | tf_op jit(solution)/shard_map/ppermute | solution.py:88
  173.7 19.0 %all-to-all-start.7 = ((bf16[8,4,8,8,128]{4,3,2,1,0:T(8,128)(2,1)}), bf16[8,4,8,8,128]{4,3,2,1,0:T(8,128)(2,1)S(1)}, u32[]{:S(2)}, u32[]{:S(2)}) async-start(bf16[8,4,8,8,128]{4,3,2,1,0:T(8,128)(2,1)} %broadcast_in_dim.22), calls=%async_computation.7 | async-start | bytes 1048576 | tf_op jit(solution)/shard_map/all_to_all | solution.py:75
  194.3 10.9 %copy-start.3 = (f32[8,512]{1,0:T(8,128)S(1)}, f32[8,512]{1,0:T(8,128)}, u32[]{:S(2)}) copy-start(f32[8,512]{1,0:T(8,128)} %ov.1) | copy-start | bytes 49156
  194.3 10.9 %copy-start.4 = (f32[512,8]{0,1:T(8,128)S(1)}, f32[512,8]{0,1:T(8,128)}, u32[]{:S(2)}) copy-start(f32[512,8]{0,1:T(8,128)} %param.19) | copy-start | bytes 49156
  194.3 10.9 %collective-permute-start.6 = (bf16[8,4,4,8,1024]{4,3,2,1,0:T(8,128)(2,1)S(1)}, bf16[8,4,4,8,1024]{4,3,2,1,0:T(8,128)(2,1)S(1)}, u32[]{:S(2)}, u32[]{:S(2)}) collective-permute-start(bf16[8,4,4,8,1024]{4,3,2,1,0:T(8,128)(2,1)S(1)} %assemble.1.mine), channel_id=1, source_target_pairs={{0,4},{4,0},{1,5},{5,1},{2,6},{6,2},{3,7},{7,3},{8,12},{12,8},{9,1... | collective-permute-start | bytes 6291464 | tf_op jit(solution)/shard_map/ppermute | solution.py:88

commit v8 on v7

--- a/solution.py
+++ b/solution.py
@@ -11,6 +11,7 @@
 R = 256
 FS = ("z", "x", "c")
 PLANE = ("x", "c", "tp")
+ALL = ("z", *PLANE)
 NZL = 4
 FIRST = 5
 LANES = 128
@@ -59,16 +60,26 @@
     at = lambda x, c, y: (x * nc + c) * ny + y
     return (
         [[at(x, c, y) for x in xs for y in ys] for c in range(nc)],
-        [[at(x, c, y) for x in xs for c in range(nc)] for y in range(ny)],
+        [[at(x, c, y) for c in range(nc) for x in xs] for y in range(ny)],
         [[at(x, c, y) for y in ys] for x in range(nx) for c in range(nc)],
     )
+
+
+def block_groups(nz, nx, nc, ny):
+    return [
+        [((z * nx + x) * nc + c) * ny + y for x in turned(nx, nx // 2) for z in near]
+        for near in near_z(nz)
+        for c in range(nc)
+        for y in range(ny)
+    ]
 
 
 def column_of(k, nzh):
     slot = k // nzh % NZL
     near = jnp.where(slot < 2, 1 - slot, slot)
     z = (k % nzh + FIRST) % nzh * NZL + near
-    return z * 8 + (k // (nzh * NZL) + 4) % 8
+    place = k // (nzh * NZL)
+    return z * 8 + (place + 2) % 4 * 2 + place // 4
 
 
 def exchange(blocks, axes, groups=None):
@@ -272,13 +283,13 @@
         ns[at] = 0.95 * s[at] + 0.05 * own * own
 
 
-def moments(t, *state):
+def moments(count, t, *state):
     nzh, tiles = t.shape[0], t.shape[1] - 3
     shape = jax.ShapeDtypeStruct(state[0].shape, jnp.float32)
     return pl.pallas_call(
         moments_kernel,
         out_shape=(
-            jax.ShapeDtypeStruct((NZL, tiles, nzh, LANES), jnp.bfloat16),
+            jax.ShapeDtypeStruct((count, tiles, nzh, LANES), jnp.bfloat16),
             shape,
             shape,
             shape,
@@ -464,6 +475,7 @@
     sizes = nzh, nzl, nx, nc
     ny = lax.axis_size("tp")
     over_xy, over_xc, over_y = plane_groups(nx, nc, ny)
+    over_block = block_groups(nz, nx, nc, ny)
     _, cols = weight_value.shape
 
     turned_weight = weight_output.T
@@ -493,16 +505,16 @@
     t = exchange(t, "z", far_z(nz))
     w2 = moved(w1, "x", 1)
     gram = gram_of(factors)
-    d, *state = moments(t, *state)
+    d, *state = moments(nzl * nx, t, *state)
     next_first_value, next_second_value, next_first_output, next_second_output = (
         s.reshape(1, cols) for s in state
     )
-    d = exchange(d, "z", near_z(nz))
-    d = to_all(d, PLANE, over_xc)
+    d = exchange(d, ALL, over_block)
+    d = lax.all_gather(d, "c", axis=0, tiled=True)
     mine = assembled((w0, w1, w2, w3), sizes, d)
     flip = moved(mine, "c", 1)
 
-    totals, directions = totals_of(ny, d.reshape(-1, *d.shape[2:]), gram)
+    totals, directions = totals_of(ny, d, gram)
     totals = exchange(totals, PLANE, over_y)
 
     copy_value, copy_output, step_value, step_output, next_value, next_output = final(

time: 212 us -> 225 us (1.061); the launches traced: 208 us -> 224 us
  blocking collectives: 95.9 us -> 138 us
  starting transfers between devices: 58.6 us -> 29.5 us
  waiting for transfers between devices: 39.5 us -> 44.1 us
    all_to_all x6 -> x7, blocking collectives: 95.9 us -> 135 us  [exchange(): lax.all_to_all(blocks, axes, split_axis=0, concat_axis=0, axis_index_grou...]
    all_to_all x3 -> x1, starting transfers between devices: 33.8 us -> 5.72 us  [exchange(): lax.all_to_all(blocks, axes, split_axis=0, concat_axis=0, axis_index_grou...]
    ppermute x5, waiting for transfers between devices: 4.82 us -> 22.1 us  [moved(): return lax.ppermute(block, axis, [(i, (i + by) % n) for i in range(n)])]
    all_to_all x3 -> x1, waiting for transfers between devices: 7.98 us -> 0.01 us  [exchange(): lax.all_to_all(blocks, axes, split_axis=0, concat_axis=0, axis_index_grou...]
    ppermute x2, waiting for transfers between devices: 26.7 us -> 22 us  [swapped(): lax.ppermute(block, axis, [(i, i ^ bit) for i in range(lax.axis_size(axis...]
    all_gather x0 -> x1, blocking collectives: none -> 3.16 us  [step(): d = lax.all_gather(d, 'c', axis=0, tiled=True)]
  transfers between devices with their start and end apart: 10 -> 8, of which waited for: 6 -> 5; matrix products, arithmetic and copies ran while one was open for 0% -> 0% of each run, Pallas kernels for 1% -> 1%
where the time goes in v8:
time: 225 us; the launch traced here: 224 us
  blocking collectives  138 us (61%)
  waiting for transfers between devices  44.1 us (20%)
  starting transfers between devices  29.5 us (13%)
  Pallas kernels  11.2 us (5%)
    all_to_all x7, blocking collectives, exchange(): lax.all_to_all(blocks, axes, split_axis=0, concat_axis=0, axis_index_grou...  135 us
    ppermute x5, waiting for transfers between devices, moved(): return lax.ppermute(block, axis, [(i, (i + by) % n) for i in range(n)])  22.1 us
    ppermute x2, waiting for transfers between devices, swapped(): lax.ppermute(block, axis, [(i, i ^ bit) for i in range(lax.axis_size(axis...  22 us
    ppermute x5, starting transfers between devices, moved(): return lax.ppermute(block, axis, [(i, (i + by) % n) for i in range(n)])  19.4 us
    all_to_all x1, starting transfers between devices, exchange(): lax.all_to_all(blocks, axes, split_axis=0, concat_axis=0, axis_index_grou...  5.72 us
  transfers between devices with their start and end apart: 8, of which 5 were waited for; matrix products, arithmetic and copies ran while one was open for 0% of the time, Pallas kernels for 1%

profile of v8, /device:TPU:1, one launch (start us, length us, event | category | flops | bytes accessed | tf_op | source)
XLA Modules:
  0.0 223.9 jit_solution(14352201087684662296)
XLA Ops:
  0.7 1.1 packed.1
  1.8 45.6 %all_to_all.40 = bf16[8,9,8,128]{3,2,1,0:T(8,128)(2,1)S(1)} all-to-all(bf16[8,9,8,128]{3,2,1,0:T(8,128)(2,1)S(1)} %packed.1), channel_id=1, replica_groups={{640,768,896,0,128,256,384,512},{672,800,928,32,160,288,416,544},{704,8..., dimensions={0} | all-to-all | bytes 294912 | tf_op jit(solution)/shard_map/all_to_all | solution.py:86
  47.4 8.2 %all_to_all.41 = bf16[4,8,8,128]{3,2,1,0:T(8,128)(2,1)S(1)} all-to-all(bf16[4,8,8,128]{3,2,1,0:T(8,128)(2,1)S(1)} %broadcast_in_dim.14), channel_id=1, replica_groups={{32,0,64,96},{160,128,192,224},{288,256,320,352},{416,384,448,480},{544..., dimensions={0} | all-to-all | bytes 131072 | tf_op jit(solution)/shard_map/all_to_all | solution.py:86
  55.6 0.2 broadcast_in_dim.15
  55.9 16.9 %all_to_all.42.mine = bf16[16,4,8,8,128]{4,3,2,1,0:T(8,128)(2,1)S(1)} all-to-all(bf16[16,4,8,8,128]{4,3,2,1,0:T(8,128)(2,1)S(1)} %broadcast_in_dim.15), channel_id=1, replica_groups={{18,19,16,17,26,27,24,25,2,3,0,1,10,11,8,9},{22,23,20,21,30,31,28,29,6,..., dimensions={0} | all-to-all | bytes 2097152 | tf_op jit(solution)/shard_map/all_to_all | solution.py:86
  72.8 6.8 %collective-permute-start = (bf16[16,4,8,8,128]{4,3,2,1,0:T(8,128)(2,1)S(1)}, bf16[16,4,8,8,128]{4,3,2,1,0:T(8,128)(2,1)S(1)}, u32[]{:S(2)}, u32[]{:S(2)}) collective-permute-start(bf16[16,4,8,8,128]{4,3,2,1,0:T(8,128)(2,1)S(1)} %all_to_all.42.mine), channel_id=1, source_target_pairs={{0,4},{4,0},{1,5},{5,1},{2,6},{6,2},{3,7},{7,3},{8,12},{12,8},{9,1... | collective-permute-start | bytes 3145736 | tf_op jit(solution)/shard_map/ppermute | solution.py:99
  79.7 2.3 %collective-permute-done.other = bf16[16,4,8,8,128]{4,3,2,1,0:T(8,128)(2,1)S(1)} collective-permute-done((bf16[16,4,8,8,128]{4,3,2,1,0:T(8,128)(2,1)S(1)}, bf16[16,4,8,8,128]{4,3,2,1,0:T(8,128)(2,1)S(1)}, u32[]{:S(2)}, u32[]{:S(2)}) %collective-permute-start) | collective-permute-done | bytes 1048608 | tf_op jit(solution)/shard_map/ppermute | solution.py:99
  82.0 3.4 %project.1 = (bf16[8,32,1024]{2,1,0:T(8,128)(2,1)S(1)}, bf16[2,8,4,4,2,8,256]{6,5,4,3,2,1,0:T(8,128)(2,1)S(1)}) custom-call(bf16[16,4,8,8,128]{4,3,2,1,0:T(8,128)(2,1)S(1)} %all_to_all.42.mine, bf16[16,4,8,8,128]{4,3,2,1,0:T(8,128)(2,1)S(1)} %collective-permute-done.other, bf16[512,2048]{1,0:T(8,128)(2,1)S(1)} %copy-done, bf16[512,512]{1,0:T(8,128)(2,1)S(1)} %copy-done.1, ...), custom_call_target="tpu_custom_call" | custom-call | flops 1342177280 | bytes 10000000 | tf_op jit(solution)/shard_map/project/pallas_call | solution.py:183
  85.4 12.2 %all_to_all.43.t = bf16[8,32,1024]{2,1,0:T(8,128)(2,1)S(1)} all-to-all(bf16[8,32,1024]{2,1,0:T(8,128)(2,1)S(1)} %get-tuple-element.25), channel_id=1, replica_groups={{16,24,0,8,20,28,4,12},{17,25,1,9,21,29,5,13},{18,26,2,10,22,30,6,14},{..., dimensions={0} | all-to-all | bytes 1048576 | tf_op jit(solution)/shard_map/all_to_all | solution.py:86
  97.6 0.1 summed.1
  97.7 6.8 %all_to_all.44.t = f32[4,8,1024]{2,1,0:T(8,128)S(1)} all-to-all(f32[4,8,1024]{2,1,0:T(8,128)S(1)} %summed.1), channel_id=1, replica_groups={{32,0,64,96},{160,128,192,224},{288,256,320,352},{416,384,448,480},{544..., dimensions={0} | all-to-all | bytes 262144 | tf_op jit(solution)/shard_map/all_to_all | solution.py:86
  104.6 38.8 %all_to_all.45.t = bf16[8,11,8,128]{3,2,1,0:T(8,128)(2,1)S(1)} all-to-all(bf16[8,11,8,128]{3,2,1,0:T(8,128)(2,1)S(1)} %shared.1), channel_id=1, replica_groups={{640,768,896,0,128,256,384,512},{672,800,928,32,160,288,416,544},{704,8..., dimensions={0} | all-to-all | bytes 360448 | tf_op jit(solution)/shard_map/all_to_all | solution.py:86
  143.4 0.8 moments.1
  144.2 5.7 %all-to-all-start.6 = ((bf16[16,8,8,128]{3,2,1,0:T(8,128)(2,1)}), bf16[16,8,8,128]{3,2,1,0:T(8,128)(2,1)S(1)}, u32[]{:S(2)}, u32[]{:S(2)}) async-start(bf16[16,8,8,128]{3,2,1,0:T(8,128)(2,1)} %get-tuple-element.26), calls=%async_computation.6 | async-start | bytes 524288 | tf_op jit(solution)/shard_map/all_to_all | solution.py:86
  149.9 2.2 collective-permute-start.1
  152.1 6.8 %collective-permute-done.1 = bf16[8,9,8,128]{3,2,1,0:T(8,128)(2,1)S(1)} collective-permute-done((bf16[8,9,8,128]{3,2,1,0:T(8,128)(2,1)S(1)}, bf16[8,9,8,128]{3,2,1,0:T(8,128)(2,1)S(1)}, u32[]{:S(2)}, u32[]{:S(2)}) %collective-permute-start.1) | collective-permute-done | bytes 147488 | tf_op jit(solution)/shard_map/ppermute | solution.py:103
  159.0 2.2 collective-permute-start.2
  161.2 15.2 %collective-permute-done.2 = bf16[2,8,9,8,128]{4,3,2,1,0:T(8,128)(2,1)S(1)} collective-permute-done((bf16[2,8,9,8,128]{4,3,2,1,0:T(8,128)(2,1)S(1)}, bf16[2,8,9,8,128]{4,3,2,1,0:T(8,128)(2,1)S(1)}, u32[]{:S(2)}, u32[]{:S(2)}) %collective-permute-start.2) | collective-permute-done | bytes 294944 | tf_op jit(solution)/shard_map/ppermute | solution.py:103
  176.5 1.9 collective-permute-start.3
  178.4 4.6 %collective-permute-start.5 = (bf16[4,8,8,8,128]{4,3,2,1,0:T(8,128)(2,1)S(1)}, bf16[4,8,8,8,128]{4,3,2,1,0:T(8,128)(2,1)}, u32[]{:S(2)}, u32[]{:S(2)}) collective-permute-start(bf16[4,8,8,8,128]{4,3,2,1,0:T(8,128)(2,1)S(1)} %pad_maximum_fusion.refs_0_), channel_id=1, source_target_pairs={{0,24},{8,0},{16,8},{24,16},{1,25},{9,1},{17,9},{25,17},{2,26},{10... | collective-permute-start | bytes 1572872 | tf_op jit(solution)/shard_map/ppermute | solution.py:99
  183.0 9.6 %collective-permute-done.3.refs_1_ = bf16[4,8,8,8,128]{4,3,2,1,0:T(8,128)(2,1)S(1)} collective-permute-done((bf16[4,8,8,8,128]{4,3,2,1,0:T(8,128)(2,1)S(1)}, bf16[4,8,8,8,128]{4,3,2,1,0:T(8,128)(2,1)S(1)}, u32[]{:S(2)}, u32[]{:S(2)}) %collective-permute-start.3) | collective-permute-done | bytes 524320 | tf_op jit(solution)/shard_map/ppermute | solution.py:99
  192.6 1.9 collective-permute-start.4
  194.5 3.2 %all_gather.3.d.refs_4_ = bf16[32,8,8,128]{3,2,1,0:T(8,128)(2,1)S(1)} all-gather(bf16[16,8,8,128]{3,2,1,0:T(8,128)(2,1)S(1)} %all-to-all-done.6), channel_id=1, replica_groups=mesh['z'=32,'x'=4,'c'=2,'tp'=4] {'c'}, dimensions={0}, use_global_device_ids=true | all-gather | bytes 786432 | tf_op jit(solution)/shard_map/all_gather | solution.py:513
  197.7 10.2 %collective-permute-done.4.refs_2_ = bf16[4,8,8,8,128]{4,3,2,1,0:T(8,128)(2,1)} collective-permute-done((bf16[4,8,8,8,128]{4,3,2,1,0:T(8,128)(2,1)S(1)}, bf16[4,8,8,8,128]{4,3,2,1,0:T(8,128)(2,1)}, u32[]{:S(2)}, u32[]{:S(2)}) %collective-permute-start.4) | collective-permute-done | bytes 524320 | tf_op jit(solution)/shard_map/ppermute | solution.py:99
  207.9 1.4 assemble.1.mine
  209.3 0.0 copy-start.3
  209.3 0.0 copy-start.4
  209.3 4.1 %collective-permute-start.6 = (bf16[8,4,4,8,1024]{4,3,2,1,0:T(8,128)(2,1)S(1)}, bf16[8,4,4,8,1024]{4,3,2,1,0:T(8,128)(2,1)S(1)}, u32[]{:S(2)}, u32[]{:S(2)}) collective-permute-start(bf16[8,4,4,8,1024]{4,3,2,1,0:T(8,128)(2,1)S(1)} %assemble.1.mine), channel_id=1, source_target_pairs={{0,4},{4,0},{1,5},{5,1},{2,6},{6,2},{3,7},{7,3},{8,12},{12,8},{9,1... | collective-permute-start | bytes 6291464 | tf_op jit(solution)/shard_map/ppermute | solution.py:99
  213.5 0.8 gram.1
  214.2 0.6 totals.1
  214.9 6.1 %all_to_all.46.totals = f32[4,8,128]{2,1,0:T(8,128)S(1)} all-to-all(f32[4,8,128]{2,1,0:T(8,128)S(1)} %get-tuple-element.28), channel_id=1, replica_groups={{2,3,0,1},{6,7,4,5},{10,11,8,9},{14,15,12,13},{18,19,16,17},{22,23,20,2..., dimensions={0} | all-to-all | bytes 32768 | tf_op jit(solution)/shard_map/all_to_all | solution.py:86
  221.0 2.9 %final.1 = (bf16[8,4,4,2,8,512]{5,4,3,2,1,0:T(8,128)(2,1)}, bf16[512,2048]{1,0:T(8,128)(2,1)}, f32[8,512]{1,0:T(8,128)}, f32[8,512]{1,0:T(8,128)}, f32[8,512]{1,0:T(8,128)}, /*index=5*/f32[8,512]{1,0:T(8,128)}) custom-call(f32[4,8,128]{2,1,0:T(8,128)S(1)} %all_to_all.46.totals, bf16[2,256,512]{2,1,0:T(8,128)(2,1)S(1)} %get-tuple-element.29.directions, ...), custom_call_target="tpu_custom_call" | custom-call | flops 1073741824 | bytes 10000000 | tf_op jit(solution)/shard_map/final/pallas_call | solution.py:434
  (26 shorter events, 0.2 us)
Async XLA Ops:
  0.6 81.3 %copy-start.2 = (bf16[512,512]{1,0:T(8,128)(2,1)S(1)}, bf16[512,512]{1,0:T(8,128)(2,1)}, u32[]{:S(2)}) copy-start(bf16[512,512]{1,0:T(8,128)(2,1)} %vo.1) | copy-start | bytes 1572868
  0.7 81.3 %copy-start.1 = (bf16[512,512]{1,0:T(8,128)(2,1)S(1)}, bf16[512,512]{1,0:T(8,128)(2,1)}, u32[]{:S(2)}) copy-start(bf16[512,512]{1,0:T(8,128)(2,1)} %vv.1) | copy-start | bytes 1572868
  0.7 81.3 %copy-start = (bf16[512,2048]{1,0:T(8,128)(2,1)S(1)}, bf16[512,2048]{1,0:T(8,128)(2,1)}, u32[]{:S(2)}) copy-start(bf16[512,2048]{1,0:T(8,128)(2,1)} %xv.1) | copy-start | bytes 6291460
  72.8 31.7 %copy-start.5 = (f32[1,512]{1,0:T(1,128)S(1)}, f32[1,512]{1,0:T(1,128)}, u32[]{:S(2)}) copy-start(f32[1,512]{1,0:T(1,128)} %param.20) | copy-start | bytes 6148
  72.8 31.7 %copy-start.6 = (f32[1,512]{1,0:T(1,128)S(1)}, f32[1,512]{1,0:T(1,128)}, u32[]{:S(2)}) copy-start(f32[1,512]{1,0:T(1,128)} %param.21) | copy-start | bytes 6148
  72.8 31.7 %copy-start.7 = (f32[1,512]{1,0:T(1,128)S(1)}, f32[1,512]{1,0:T(1,128)}, u32[]{:S(2)}) copy-start(f32[1,512]{1,0:T(1,128)} %param.22) | copy-start | bytes 6148
  72.8 31.7 %copy-start.8 = (f32[1,512]{1,0:T(1,128)S(1)}, f32[1,512]{1,0:T(1,128)}, u32[]{:S(2)}) copy-start(f32[1,512]{1,0:T(1,128)} %param.23) | copy-start | bytes 6148
  72.8 9.1 %collective-permute-start = (bf16[16,4,8,8,128]{4,3,2,1,0:T(8,128)(2,1)S(1)}, bf16[16,4,8,8,128]{4,3,2,1,0:T(8,128)(2,1)S(1)}, u32[]{:S(2)}, u32[]{:S(2)}) collective-permute-start(bf16[16,4,8,8,128]{4,3,2,1,0:T(8,128)(2,1)S(1)} %all_to_all.42.mine), channel_id=1, source_target_pairs={{0,4},{4,0},{1,5},{5,1},{2,6},{6,2},{3,7},{7,3},{8,12},{12,8},{9,1... | collective-permute-start | bytes 3145736 | tf_op jit(solution)/shard_map/ppermute | solution.py:99
  144.2 50.3 %all-to-all-start.6 = ((bf16[16,8,8,128]{3,2,1,0:T(8,128)(2,1)}), bf16[16,8,8,128]{3,2,1,0:T(8,128)(2,1)S(1)}, u32[]{:S(2)}, u32[]{:S(2)}) async-start(bf16[16,8,8,128]{3,2,1,0:T(8,128)(2,1)} %get-tuple-element.26), calls=%async_computation.6 | async-start | bytes 524288 | tf_op jit(solution)/shard_map/all_to_all | solution.py:86
  149.9 9.0 %collective-permute-start.1 = (bf16[8,9,8,128]{3,2,1,0:T(8,128)(2,1)S(1)}, bf16[8,9,8,128]{3,2,1,0:T(8,128)(2,1)S(1)}, u32[]{:S(2)}, u32[]{:S(2)}) collective-permute-start(bf16[8,9,8,128]{3,2,1,0:T(8,128)(2,1)S(1)} %all_to_all.40), channel_id=1, source_target_pairs={{0,32},{32,0},{64,96},{96,64},{128,160},{160,128},{192,224},{224,1... | collective-permute-start | bytes 442376 | tf_op jit(solution)/shard_map/ppermute | solution.py:103
  159.0 17.5 %collective-permute-start.2 = (bf16[2,8,9,8,128]{4,3,2,1,0:T(8,128)(2,1)S(1)}, bf16[2,8,9,8,128]{4,3,2,1,0:T(8,128)(2,1)S(1)}, u32[]{:S(2)}, u32[]{:S(2)}) collective-permute-start(bf16[2,8,9,8,128]{4,3,2,1,0:T(8,128)(2,1)S(1)} %pad_maximum_fusion.1), channel_id=1, source_target_pairs={{0,64},{32,96},{64,0},{96,32},{128,192},{160,224},{192,128},{224,1... | collective-permute-start | bytes 884744 | tf_op jit(solution)/shard_map/ppermute | solution.py:103
  176.5 16.1 %collective-permute-start.3 = (bf16[4,8,8,8,128]{4,3,2,1,0:T(8,128)(2,1)S(1)}, bf16[4,8,8,8,128]{4,3,2,1,0:T(8,128)(2,1)S(1)}, u32[]{:S(2)}, u32[]{:S(2)}) collective-permute-start(bf16[4,8,8,8,128]{4,3,2,1,0:T(8,128)(2,1)S(1)} %pad_maximum_fusion.refs_0_), channel_id=1, source_target_pairs={{0,8},{8,16},{16,24},{24,0},{1,9},{9,17},{17,25},{25,1},{2,10},{10... | collective-permute-start | bytes 1572872 | tf_op jit(solution)/shard_map/ppermute | solution.py:99
  178.4 19.3 %collective-permute-start.5 = (bf16[4,8,8,8,128]{4,3,2,1,0:T(8,128)(2,1)S(1)}, bf16[4,8,8,8,128]{4,3,2,1,0:T(8,128)(2,1)}, u32[]{:S(2)}, u32[]{:S(2)}) collective-permute-start(bf16[4,8,8,8,128]{4,3,2,1,0:T(8,128)(2,1)S(1)} %pad_maximum_fusion.refs_0_), channel_id=1, source_target_pairs={{0,24},{8,0},{16,8},{24,16},{1,25},{9,1},{17,9},{25,17},{2,26},{10... | collective-permute-start | bytes 1572872 | tf_op jit(solution)/shard_map/ppermute | solution.py:99
  192.6 15.3 %collective-permute-start.4 = (bf16[4,8,8,8,128]{4,3,2,1,0:T(8,128)(2,1)S(1)}, bf16[4,8,8,8,128]{4,3,2,1,0:T(8,128)(2,1)}, u32[]{:S(2)}, u32[]{:S(2)}) collective-permute-start(bf16[4,8,8,8,128]{4,3,2,1,0:T(8,128)(2,1)S(1)} %collective-permute-done.3.refs_1_), channel_id=1, source_target_pairs={{0,8},{8,16},{16,24},{24,0},{1,9},{9,17},{17,25},{25,1},{2,10},{10... | collective-permute-start | bytes 1572872 | tf_op jit(solution)/shard_map/ppermute | solution.py:99
  209.3 11.7 %copy-start.3 = (f32[8,512]{1,0:T(8,128)S(1)}, f32[8,512]{1,0:T(8,128)}, u32[]{:S(2)}) copy-start(f32[8,512]{1,0:T(8,128)} %ov.1) | copy-start | bytes 49156
  209.3 11.7 %copy-start.4 = (f32[512,8]{0,1:T(8,128)S(1)}, f32[512,8]{0,1:T(8,128)}, u32[]{:S(2)}) copy-start(f32[512,8]{0,1:T(8,128)} %param.19) | copy-start | bytes 49156
  209.3 11.6 %collective-permute-start.6 = (bf16[8,4,4,8,1024]{4,3,2,1,0:T(8,128)(2,1)S(1)}, bf16[8,4,4,8,1024]{4,3,2,1,0:T(8,128)(2,1)S(1)}, u32[]{:S(2)}, u32[]{:S(2)}) collective-permute-start(bf16[8,4,4,8,1024]{4,3,2,1,0:T(8,128)(2,1)S(1)} %assemble.1.mine), channel_id=1, source_target_pairs={{0,4},{4,0},{1,5},{5,1},{2,6},{6,2},{3,7},{7,3},{8,12},{12,8},{9,1... | collective-permute-start | bytes 6291464 | tf_op jit(solution)/shard_map/ppermute | solution.py:99

commit v9 on v8

--- a/solution.py
+++ b/solution.py
@@ -149,7 +149,7 @@
     )(*far(fv, fo, wv, wo))
 
 
-def project_kernel(mine, other, xv, vv, xo, vo, out, whole, late, sems):
+def project_kernel(mine, other, xv, vv, xo, vo, keep, give, whole, late, sems):
     c = lax.axis_index("c")
     read = pltpu.make_async_copy(xo, late, sems.at[0])
     read.start()
@@ -172,7 +172,10 @@
             read.wait()
         projected = dot(x[...], whole[f].reshape(D, R)).astype(jnp.bfloat16)
         term = dot(projected, v[...], TN).astype(jnp.bfloat16)
-        out[:, :, f * cols : (f + 1) * cols] = term.reshape(out.shape[0], out.shape[1], cols)
+        term = term.reshape(2, *keep.shape[:2], cols)
+        lanes = slice(f * cols, (f + 1) * cols)
+        keep[:, :, lanes] = jnp.where(c == 0, term[0], term[1])
+        give[:, :, lanes] = jnp.where(c == 0, term[1], term[0])
 
 
 def projected_terms(mine, other, xv, vv, xo, vo, sizes):
@@ -183,11 +186,12 @@
     return pl.pallas_call(
         project_kernel,
         out_shape=(
-            jax.ShapeDtypeStruct((nx * nc, nzh * nzl, 2 * cols), jnp.bfloat16),
+            jax.ShapeDtypeStruct((nx, nzh * nzl, 2 * cols), jnp.bfloat16),
+            jax.ShapeDtypeStruct((nx, nzh * nzl, 2 * cols), jnp.bfloat16),
             pltpu.VMEM(shape, jnp.bfloat16),
         ),
         in_specs=[VMEM] * 4 + [HBM, VMEM],
-        out_specs=(VMEM, VMEM),
+        out_specs=(VMEM,) * 3,
         scratch_shapes=[pltpu.VMEM(xo.shape, xo.dtype), pltpu.SemaphoreType.DMA((1,))],
         name="project",
         compiler_params=params(12),
@@ -195,25 +199,25 @@
     )(mine, other, *near(xv, vv), *far(xo), *near(vo))
 
 
-def summed_kernel(t, out):
-    out[...] = jnp.sum(t[...].astype(jnp.float32), axis=0).reshape(out.shape)
-
-
-def summed(t, nzh):
-    _, nz, width = t.shape
-    return pl.pallas_call(
-        summed_kernel,
-        out_shape=jax.ShapeDtypeStruct((nz // nzh, nzh, width), jnp.float32),
-        in_specs=[VMEM],
+def paired_kernel(keep, get, out):
+    total = keep[...].astype(jnp.float32) + get[...].astype(jnp.float32)
+    out[...] = total.astype(jnp.bfloat16)
+
+
+def paired(keep, get):
+    return pl.pallas_call(
+        paired_kernel,
+        out_shape=jax.ShapeDtypeStruct(keep.shape, jnp.bfloat16),
+        in_specs=[VMEM, VMEM],
         out_specs=VMEM,
-        name="summed",
+        name="paired",
         compiler_params=params(2),
-        cost_estimate=cost(t.size, 600_000),
-    )(t)
+        cost_estimate=cost(keep.size, 800_000),
+    )(keep, get)
 
 
 def shared_kernel(t, fv, sv, fo, so, out):
-    total = jnp.sum(t[...], axis=0)
+    total = jnp.sum(t[...].astype(jnp.float32), axis=0)
     tiles = total.shape[1] // LANES
     first = 0.9 * jnp.concatenate([fv[...], fo[...]], axis=0)
     high = first.astype(jnp.bfloat16)
@@ -474,7 +478,7 @@
     nzh, nzl = nz // NZL, NZL
     sizes = nzh, nzl, nx, nc
     ny = lax.axis_size("tp")
-    over_xy, over_xc, over_y = plane_groups(nx, nc, ny)
+    over_xy, _, over_y = plane_groups(nx, nc, ny)
     over_block = block_groups(nz, nx, nc, ny)
     _, cols = weight_value.shape
 
@@ -490,15 +494,14 @@
     get = swapped(w, "z", 2)
     w0 = jnp.concatenate([w[:, :, 1:], get[:, :, 1:]])
 
-    terms, factors = projected_terms(
+    keep, give, factors = projected_terms(
         f, other, normed_input, value_cotangent, layer_cotangent, gated_output, sizes
     )
-    t = exchange(terms, PLANE, over_xc)
-    t = summed(t, nzh)
+    across = moved(give, "c", 1)
+    t = paired(keep, across)
+    t = exchange(t.reshape(nx * nzl, nzh, 2 * cols), ALL, over_block)
     w1 = moved(w0, "x", 1)
     w3 = moved(w0, "x", nx - 1)
-    t = exchange(t, "z", near_z(nz))
-
     narrow = (cols // LANES, LANES)
     state = [s.reshape(narrow) for s in (first_value, second_value, first_output, second_output)]
     t = shared(t, *state)

time: 225 us -> 218 us (0.969)
  blocking collectives: 138 us -> 126 us
  starting transfers between devices: 29.5 us -> 33.9 us
    all_to_all x7 -> x6, blocking collectives: 135 us -> 123 us  [exchange(): lax.all_to_all(blocks, axes, split_axis=0, concat_axis=0, axis_index_grou...]
    all_to_all x1, starting transfers between devices: 5.72 us -> 8.07 us  [exchange(): lax.all_to_all(blocks, axes, split_axis=0, concat_axis=0, axis_index_grou...]
    ppermute x5 -> x6, starting transfers between devices: 19.4 us -> 21.6 us  [moved(): return lax.ppermute(block, axis, [(i, (i + by) % n) for i in range(n)])]
    ppermute x5 -> x6, waiting for transfers between devices: 22.1 us -> 23.2 us  [moved(): return lax.ppermute(block, axis, [(i, (i + by) % n) for i in range(n)])]
  transfers between devices with their start and end apart: 8 -> 9, of which waited for: 5 -> 6; matrix products, arithmetic and copies ran while one was open for 0% -> 0% of each run, Pallas kernels for 1% -> 1%
where the time goes in v9:
time: 218 us
  blocking collectives  126 us (58%)
  waiting for transfers between devices  45 us (21%)
  starting transfers between devices  33.9 us (16%)
  Pallas kernels  11.2 us (5%)
    all_to_all x6, blocking collectives, exchange(): lax.all_to_all(blocks, axes, split_axis=0, concat_axis=0, axis_index_grou...  123 us
    ppermute x6, waiting for transfers between devices, moved(): return lax.ppermute(block, axis, [(i, (i + by) % n) for i in range(n)])  23.2 us
    ppermute x2, waiting for transfers between devices, swapped(): lax.ppermute(block, axis, [(i, i ^ bit) for i in range(lax.axis_size(axis...  21.8 us
    ppermute x6, starting transfers between devices, moved(): return lax.ppermute(block, axis, [(i, (i + by) % n) for i in range(n)])  21.6 us
    all_to_all x1, starting transfers between devices, exchange(): lax.all_to_all(blocks, axes, split_axis=0, concat_axis=0, axis_index_grou...  8.07 us
  transfers between devices with their start and end apart: 9, of which 6 were waited for; matrix products, arithmetic and copies ran while one was open for 0% of the time, Pallas kernels for 1%

profile of v9, /device:TPU:1, one launch (start us, length us, event | category | flops | bytes accessed | tf_op | source)
XLA Modules:
  0.0 217.6 jit_solution(7477974922225335178)
XLA Ops:
  0.7 1.1 packed.1
  1.8 45.6 %all_to_all.35 = bf16[8,9,8,128]{3,2,1,0:T(8,128)(2,1)S(1)} all-to-all(bf16[8,9,8,128]{3,2,1,0:T(8,128)(2,1)S(1)} %packed.1), channel_id=1, replica_groups={{640,768,896,0,128,256,384,512},{672,800,928,32,160,288,416,544},{704,8..., dimensions={0} | all-to-all | bytes 294912 | tf_op jit(solution)/shard_map/all_to_all | solution.py:86
  47.4 8.2 %all_to_all.36 = bf16[4,8,8,128]{3,2,1,0:T(8,128)(2,1)S(1)} all-to-all(bf16[4,8,8,128]{3,2,1,0:T(8,128)(2,1)S(1)} %broadcast_in_dim.14), channel_id=1, replica_groups={{32,0,64,96},{160,128,192,224},{288,256,320,352},{416,384,448,480},{544..., dimensions={0} | all-to-all | bytes 131072 | tf_op jit(solution)/shard_map/all_to_all | solution.py:86
  55.6 0.2 broadcast_in_dim.15
  55.9 16.9 %all_to_all.37.mine = bf16[16,4,8,8,128]{4,3,2,1,0:T(8,128)(2,1)S(1)} all-to-all(bf16[16,4,8,8,128]{4,3,2,1,0:T(8,128)(2,1)S(1)} %broadcast_in_dim.15), channel_id=1, replica_groups={{18,19,16,17,26,27,24,25,2,3,0,1,10,11,8,9},{22,23,20,21,30,31,28,29,6,..., dimensions={0} | all-to-all | bytes 2097152 | tf_op jit(solution)/shard_map/all_to_all | solution.py:86
  72.8 6.8 %collective-permute-start = (bf16[16,4,8,8,128]{4,3,2,1,0:T(8,128)(2,1)S(1)}, bf16[16,4,8,8,128]{4,3,2,1,0:T(8,128)(2,1)S(1)}, u32[]{:S(2)}, u32[]{:S(2)}) collective-permute-start(bf16[16,4,8,8,128]{4,3,2,1,0:T(8,128)(2,1)S(1)} %all_to_all.37.mine), channel_id=1, source_target_pairs={{0,4},{4,0},{1,5},{5,1},{2,6},{6,2},{3,7},{7,3},{8,12},{12,8},{9,1... | collective-permute-start | bytes 3145736 | tf_op jit(solution)/shard_map/ppermute | solution.py:99
  79.7 2.3 %collective-permute-done.other = bf16[16,4,8,8,128]{4,3,2,1,0:T(8,128)(2,1)S(1)} collective-permute-done((bf16[16,4,8,8,128]{4,3,2,1,0:T(8,128)(2,1)S(1)}, bf16[16,4,8,8,128]{4,3,2,1,0:T(8,128)(2,1)S(1)}, u32[]{:S(2)}, u32[]{:S(2)}) %collective-permute-start) | collective-permute-done | bytes 1048608 | tf_op jit(solution)/shard_map/ppermute | solution.py:99
  82.0 3.4 %project.1 = (bf16[4,32,1024]{2,1,0:T(8,128)(2,1)S(1)}, bf16[4,32,1024]{2,1,0:T(8,128)(2,1)S(1)}, bf16[2,8,4,4,2,8,256]{6,5,4,3,2,1,0:T(8,128)(2,1)S(1)}) custom-call(bf16[16,4,8,8,128]{4,3,2,1,0:T(8,128)(2,1)S(1)} %all_to_all.37.mine, bf16[16,4,8,8,128]{4,3,2,1,0:T(8,128)(2,1)S(1)} %collective-permute-done.other, bf16[512,2048]{1,0:T(8,128)(2,1)S(1)} %copy-done, ...), custom_call_target="tpu_custom_call" | custom-call | flops 1342177280 | bytes 10000000 | tf_op jit(solution)/shard_map/project/pallas_call | solution.py:186
  85.4 2.3 %collective-permute-start.1 = (bf16[4,32,1024]{2,1,0:T(8,128)(2,1)S(1)}, bf16[4,32,1024]{2,1,0:T(8,128)(2,1)S(1)}, u32[]{:S(2)}, u32[]{:S(2)}) collective-permute-start(bf16[4,32,1024]{2,1,0:T(8,128)(2,1)S(1)} %get-tuple-element.27), channel_id=1, source_target_pairs={{0,4},{4,0},{1,5},{5,1},{2,6},{6,2},{3,7},{7,3},{8,12},{12,8},{9,1... | collective-permute-start | bytes 786440 | tf_op jit(solution)/shard_map/ppermute | solution.py:99
  87.7 1.1 collective-permute-done.1.get
  88.9 0.1 paired.1
  88.9 11.3 %all_to_all.38.t = bf16[16,8,1024]{2,1,0:T(8,128)(2,1)S(1)} all-to-all(bf16[16,8,1024]{2,1,0:T(8,128)(2,1)S(1)} %bitcast.17), channel_id=1, replica_groups={{48,16,80,112,56,24,88,120,32,0,64,96,40,8,72,104},{49,17,81,113,57,25,..., dimensions={0} | all-to-all | bytes 524288 | tf_op jit(solution)/shard_map/all_to_all | solution.py:86
  100.3 34.4 %all_to_all.39.t = bf16[8,11,8,128]{3,2,1,0:T(8,128)(2,1)S(1)} all-to-all(bf16[8,11,8,128]{3,2,1,0:T(8,128)(2,1)S(1)} %shared.1), channel_id=1, replica_groups={{640,768,896,0,128,256,384,512},{672,800,928,32,160,288,416,544},{704,8..., dimensions={0} | all-to-all | bytes 360448 | tf_op jit(solution)/shard_map/all_to_all | solution.py:86
  134.7 0.8 moments.1
  135.5 8.1 %all-to-all-start.5 = ((bf16[16,8,8,128]{3,2,1,0:T(8,128)(2,1)}), bf16[16,8,8,128]{3,2,1,0:T(8,128)(2,1)S(1)}, u32[]{:S(2)}, u32[]{:S(2)}) async-start(bf16[16,8,8,128]{3,2,1,0:T(8,128)(2,1)} %get-tuple-element.28), calls=%async_computation.5 | async-start | bytes 524288 | tf_op jit(solution)/shard_map/all_to_all | solution.py:86
  143.6 2.2 collective-permute-start.2
  145.8 6.0 %collective-permute-done.2 = bf16[8,9,8,128]{3,2,1,0:T(8,128)(2,1)S(1)} collective-permute-done((bf16[8,9,8,128]{3,2,1,0:T(8,128)(2,1)S(1)}, bf16[8,9,8,128]{3,2,1,0:T(8,128)(2,1)S(1)}, u32[]{:S(2)}, u32[]{:S(2)}) %collective-permute-start.2) | collective-permute-done | bytes 147488 | tf_op jit(solution)/shard_map/ppermute | solution.py:103
  151.8 2.0 collective-permute-start.3
  153.9 15.7 %collective-permute-done.3 = bf16[2,8,9,8,128]{4,3,2,1,0:T(8,128)(2,1)S(1)} collective-permute-done((bf16[2,8,9,8,128]{4,3,2,1,0:T(8,128)(2,1)S(1)}, bf16[2,8,9,8,128]{4,3,2,1,0:T(8,128)(2,1)S(1)}, u32[]{:S(2)}, u32[]{:S(2)}) %collective-permute-start.3) | collective-permute-done | bytes 294944 | tf_op jit(solution)/shard_map/ppermute | solution.py:103
  169.7 1.9 collective-permute-start.4
  171.6 4.6 %collective-permute-start.6 = (bf16[4,8,8,8,128]{4,3,2,1,0:T(8,128)(2,1)S(1)}, bf16[4,8,8,8,128]{4,3,2,1,0:T(8,128)(2,1)}, u32[]{:S(2)}, u32[]{:S(2)}) collective-permute-start(bf16[4,8,8,8,128]{4,3,2,1,0:T(8,128)(2,1)S(1)} %pad_maximum_fusion.refs_0_), channel_id=1, source_target_pairs={{0,24},{8,0},{16,8},{24,16},{1,25},{9,1},{17,9},{25,17},{2,26},{10... | collective-permute-start | bytes 1572872 | tf_op jit(solution)/shard_map/ppermute | solution.py:99
  176.2 9.6 %collective-permute-done.4.refs_1_ = bf16[4,8,8,8,128]{4,3,2,1,0:T(8,128)(2,1)S(1)} collective-permute-done((bf16[4,8,8,8,128]{4,3,2,1,0:T(8,128)(2,1)S(1)}, bf16[4,8,8,8,128]{4,3,2,1,0:T(8,128)(2,1)S(1)}, u32[]{:S(2)}, u32[]{:S(2)}) %collective-permute-start.4) | collective-permute-done | bytes 524320 | tf_op jit(solution)/shard_map/ppermute | solution.py:99
  185.8 1.9 collective-permute-start.5
  187.7 3.2 %all_gather.3.d.refs_4_ = bf16[32,8,8,128]{3,2,1,0:T(8,128)(2,1)S(1)} all-gather(bf16[16,8,8,128]{3,2,1,0:T(8,128)(2,1)S(1)} %all-to-all-done.5), channel_id=1, replica_groups=mesh['z'=32,'x'=4,'c'=2,'tp'=4] {'c'}, dimensions={0}, use_global_device_ids=true | all-gather | bytes 786432 | tf_op jit(solution)/shard_map/all_gather | solution.py:516
  190.9 10.2 %collective-permute-done.5.refs_2_ = bf16[4,8,8,8,128]{4,3,2,1,0:T(8,128)(2,1)} collective-permute-done((bf16[4,8,8,8,128]{4,3,2,1,0:T(8,128)(2,1)S(1)}, bf16[4,8,8,8,128]{4,3,2,1,0:T(8,128)(2,1)}, u32[]{:S(2)}, u32[]{:S(2)}) %collective-permute-start.5) | collective-permute-done | bytes 524320 | tf_op jit(solution)/shard_map/ppermute | solution.py:99
  201.1 1.4 assemble.1.mine
  202.5 0.0 copy-start.3
  202.5 4.1 %collective-permute-start.7 = (bf16[8,4,4,8,1024]{4,3,2,1,0:T(8,128)(2,1)S(1)}, bf16[8,4,4,8,1024]{4,3,2,1,0:T(8,128)(2,1)S(1)}, u32[]{:S(2)}, u32[]{:S(2)}) collective-permute-start(bf16[8,4,4,8,1024]{4,3,2,1,0:T(8,128)(2,1)S(1)} %assemble.1.mine), channel_id=1, source_target_pairs={{0,4},{4,0},{1,5},{5,1},{2,6},{6,2},{3,7},{7,3},{8,12},{12,8},{9,1... | collective-permute-start | bytes 6291464 | tf_op jit(solution)/shard_map/ppermute | solution.py:99
  206.6 0.8 gram.1
  207.4 0.6 totals.1
  208.1 6.6 %all_to_all.40.totals = f32[4,8,128]{2,1,0:T(8,128)S(1)} all-to-all(f32[4,8,128]{2,1,0:T(8,128)S(1)} %get-tuple-element.30), channel_id=1, replica_groups={{2,3,0,1},{6,7,4,5},{10,11,8,9},{14,15,12,13},{18,19,16,17},{22,23,20,2..., dimensions={0} | all-to-all | bytes 32768 | tf_op jit(solution)/shard_map/all_to_all | solution.py:86
  214.7 2.9 %final.1 = (bf16[8,4,4,2,8,512]{5,4,3,2,1,0:T(8,128)(2,1)}, bf16[512,2048]{1,0:T(8,128)(2,1)}, f32[8,512]{1,0:T(8,128)}, f32[8,512]{1,0:T(8,128)}, f32[8,512]{1,0:T(8,128)}, /*index=5*/f32[8,512]{1,0:T(8,128)}) custom-call(f32[4,8,128]{2,1,0:T(8,128)S(1)} %all_to_all.40.totals, bf16[2,256,512]{2,1,0:T(8,128)(2,1)S(1)} %get-tuple-element.31.directions, ...), custom_call_target="tpu_custom_call" | custom-call | flops 1073741824 | bytes 10000000 | tf_op jit(solution)/shard_map/final/pallas_call | solution.py:438
  (27 shorter events, 0.2 us)
Async XLA Ops:
  0.6 81.3 %copy-start.2 = (bf16[512,512]{1,0:T(8,128)(2,1)S(1)}, bf16[512,512]{1,0:T(8,128)(2,1)}, u32[]{:S(2)}) copy-start(bf16[512,512]{1,0:T(8,128)(2,1)} %vo.1) | copy-start | bytes 1572868
  0.7 81.3 %copy-start.1 = (bf16[512,512]{1,0:T(8,128)(2,1)S(1)}, bf16[512,512]{1,0:T(8,128)(2,1)}, u32[]{:S(2)}) copy-start(bf16[512,512]{1,0:T(8,128)(2,1)} %vv.1) | copy-start | bytes 1572868
  0.7 81.3 %copy-start = (bf16[512,2048]{1,0:T(8,128)(2,1)S(1)}, bf16[512,2048]{1,0:T(8,128)(2,1)}, u32[]{:S(2)}) copy-start(bf16[512,2048]{1,0:T(8,128)(2,1)} %xv.1) | copy-start | bytes 6291460
  72.8 27.4 %copy-start.5 = (f32[1,512]{1,0:T(1,128)S(1)}, f32[1,512]{1,0:T(1,128)}, u32[]{:S(2)}) copy-start(f32[1,512]{1,0:T(1,128)} %param.20) | copy-start | bytes 6148
  72.8 27.4 %copy-start.6 = (f32[1,512]{1,0:T(1,128)S(1)}, f32[1,512]{1,0:T(1,128)}, u32[]{:S(2)}) copy-start(f32[1,512]{1,0:T(1,128)} %param.21) | copy-start | bytes 6148
  72.8 27.4 %copy-start.7 = (f32[1,512]{1,0:T(1,128)S(1)}, f32[1,512]{1,0:T(1,128)}, u32[]{:S(2)}) copy-start(f32[1,512]{1,0:T(1,128)} %param.22) | copy-start | bytes 6148
  72.8 27.4 %copy-start.8 = (f32[1,512]{1,0:T(1,128)S(1)}, f32[1,512]{1,0:T(1,128)}, u32[]{:S(2)}) copy-start(f32[1,512]{1,0:T(1,128)} %param.23) | copy-start | bytes 6148
  72.8 9.1 %collective-permute-start = (bf16[16,4,8,8,128]{4,3,2,1,0:T(8,128)(2,1)S(1)}, bf16[16,4,8,8,128]{4,3,2,1,0:T(8,128)(2,1)S(1)}, u32[]{:S(2)}, u32[]{:S(2)}) collective-permute-start(bf16[16,4,8,8,128]{4,3,2,1,0:T(8,128)(2,1)S(1)} %all_to_all.37.mine), channel_id=1, source_target_pairs={{0,4},{4,0},{1,5},{5,1},{2,6},{6,2},{3,7},{7,3},{8,12},{12,8},{9,1... | collective-permute-start | bytes 3145736 | tf_op jit(solution)/shard_map/ppermute | solution.py:99
  85.4 3.4 %collective-permute-start.1 = (bf16[4,32,1024]{2,1,0:T(8,128)(2,1)S(1)}, bf16[4,32,1024]{2,1,0:T(8,128)(2,1)S(1)}, u32[]{:S(2)}, u32[]{:S(2)}) collective-permute-start(bf16[4,32,1024]{2,1,0:T(8,128)(2,1)S(1)} %get-tuple-element.27), channel_id=1, source_target_pairs={{0,4},{4,0},{1,5},{5,1},{2,6},{6,2},{3,7},{7,3},{8,12},{12,8},{9,1... | collective-permute-start | bytes 786440 | tf_op jit(solution)/shard_map/ppermute | solution.py:99
  135.5 52.2 %all-to-all-start.5 = ((bf16[16,8,8,128]{3,2,1,0:T(8,128)(2,1)}), bf16[16,8,8,128]{3,2,1,0:T(8,128)(2,1)S(1)}, u32[]{:S(2)}, u32[]{:S(2)}) async-start(bf16[16,8,8,128]{3,2,1,0:T(8,128)(2,1)} %get-tuple-element.28), calls=%async_computation.5 | async-start | bytes 524288 | tf_op jit(solution)/shard_map/all_to_all | solution.py:86
  143.6 8.2 %collective-permute-start.2 = (bf16[8,9,8,128]{3,2,1,0:T(8,128)(2,1)S(1)}, bf16[8,9,8,128]{3,2,1,0:T(8,128)(2,1)S(1)}, u32[]{:S(2)}, u32[]{:S(2)}) collective-permute-start(bf16[8,9,8,128]{3,2,1,0:T(8,128)(2,1)S(1)} %all_to_all.35), channel_id=1, source_target_pairs={{0,32},{32,0},{64,96},{96,64},{128,160},{160,128},{192,224},{224,1... | collective-permute-start | bytes 442376 | tf_op jit(solution)/shard_map/ppermute | solution.py:103
  151.8 17.8 %collective-permute-start.3 = (bf16[2,8,9,8,128]{4,3,2,1,0:T(8,128)(2,1)S(1)}, bf16[2,8,9,8,128]{4,3,2,1,0:T(8,128)(2,1)S(1)}, u32[]{:S(2)}, u32[]{:S(2)}) collective-permute-start(bf16[2,8,9,8,128]{4,3,2,1,0:T(8,128)(2,1)S(1)} %pad_maximum_fusion.1), channel_id=1, source_target_pairs={{0,64},{32,96},{64,0},{96,32},{128,192},{160,224},{192,128},{224,1... | collective-permute-start | bytes 884744 | tf_op jit(solution)/shard_map/ppermute | solution.py:103
  169.7 16.1 %collective-permute-start.4 = (bf16[4,8,8,8,128]{4,3,2,1,0:T(8,128)(2,1)S(1)}, bf16[4,8,8,8,128]{4,3,2,1,0:T(8,128)(2,1)S(1)}, u32[]{:S(2)}, u32[]{:S(2)}) collective-permute-start(bf16[4,8,8,8,128]{4,3,2,1,0:T(8,128)(2,1)S(1)} %pad_maximum_fusion.refs_0_), channel_id=1, source_target_pairs={{0,8},{8,16},{16,24},{24,0},{1,9},{9,17},{17,25},{25,1},{2,10},{10... | collective-permute-start | bytes 1572872 | tf_op jit(solution)/shard_map/ppermute | solution.py:99
  171.6 19.3 %collective-permute-start.6 = (bf16[4,8,8,8,128]{4,3,2,1,0:T(8,128)(2,1)S(1)}, bf16[4,8,8,8,128]{4,3,2,1,0:T(8,128)(2,1)}, u32[]{:S(2)}, u32[]{:S(2)}) collective-permute-start(bf16[4,8,8,8,128]{4,3,2,1,0:T(8,128)(2,1)S(1)} %pad_maximum_fusion.refs_0_), channel_id=1, source_target_pairs={{0,24},{8,0},{16,8},{24,16},{1,25},{9,1},{17,9},{25,17},{2,26},{10... | collective-permute-start | bytes 1572872 | tf_op jit(solution)/shard_map/ppermute | solution.py:99
  185.8 15.3 %collective-permute-start.5 = (bf16[4,8,8,8,128]{4,3,2,1,0:T(8,128)(2,1)S(1)}, bf16[4,8,8,8,128]{4,3,2,1,0:T(8,128)(2,1)}, u32[]{:S(2)}, u32[]{:S(2)}) collective-permute-start(bf16[4,8,8,8,128]{4,3,2,1,0:T(8,128)(2,1)S(1)} %collective-permute-done.4.refs_1_), channel_id=1, source_target_pairs={{0,8},{8,16},{16,24},{24,0},{1,9},{9,17},{17,25},{25,1},{2,10},{10... | collective-permute-start | bytes 1572872 | tf_op jit(solution)/shard_map/ppermute | solution.py:99
  202.5 12.2 %copy-start.3 = (f32[8,512]{1,0:T(8,128)S(1)}, f32[8,512]{1,0:T(8,128)}, u32[]{:S(2)}) copy-start(f32[8,512]{1,0:T(8,128)} %ov.1) | copy-start | bytes 49156
  202.5 12.2 %copy-start.4 = (f32[512,8]{0,1:T(8,128)S(1)}, f32[512,8]{0,1:T(8,128)}, u32[]{:S(2)}) copy-start(f32[512,8]{0,1:T(8,128)} %param.19) | copy-start | bytes 49156
  202.5 12.1 %collective-permute-start.7 = (bf16[8,4,4,8,1024]{4,3,2,1,0:T(8,128)(2,1)S(1)}, bf16[8,4,4,8,1024]{4,3,2,1,0:T(8,128)(2,1)S(1)}, u32[]{:S(2)}, u32[]{:S(2)}) collective-permute-start(bf16[8,4,4,8,1024]{4,3,2,1,0:T(8,128)(2,1)S(1)} %assemble.1.mine), channel_id=1, source_target_pairs={{0,4},{4,0},{1,5},{5,1},{2,6},{6,2},{3,7},{7,3},{8,12},{12,8},{9,1... | collective-permute-start | bytes 6291464 | tf_op jit(solution)/shard_map/ppermute | solution.py:99
